TPU v7x, 512 devices: a whole 4x8x8 slice. The times are simulated.
512 devices in a mesh: sp: 32 (over z, x), tp: 16 (over y, core).
Axes of the slice: x: 4, y: 8, z: 8, core: 2. Of those that a mesh axis runs over, the one named last changes fastest.
Arguments:
- resid: bfloat16 [4096, 2048], P('sp'), may hold values from -8 to 8
- a_val: bfloat16 [4096, 1024], P('sp', 'tp'), may hold values from -8 to 8
- a_gate: bfloat16 [4096, 1024], P('sp', 'tp'), may hold values from -6 to 6
- conv_kernel: bfloat16 [31, 1024], P(None, 'tp'), may hold values from -1 to 1
- conv_bias: float32 [1024], P('tp'), may hold values from -3 to 3
- ln_gain: float32 [1024], P('tp'), may hold values from 0.1 to 1.9
- ln_bias: float32 [1024], P('tp'), may hold values from -3 to 3
- w_out: bfloat16 [1024, 2048], P('tp'), may hold values from -0.1875 to 0.1875
- ffn_gain: float32 [2048], replicated, may hold values from 0.1 to 1.9
- routes: int32 [4096, 4], P('sp'), may hold values from 0 to 31, all different within a row; in each aligned block of 128 rows (0 to 127, 128 to 255, ...) at most 32 rows name the same one
- route_weights: float32 [4096, 4], P('sp'), may hold values from 0.15 to 1.2
- exp_gate: bfloat16 [32, 2048, 4096], P('sp', None, 'tp'), may hold values from -0.125 to 0.125
- exp_up: bfloat16 [32, 2048, 4096], P('sp', None, 'tp'), may hold values from -0.125 to 0.125
- exp_down: bfloat16 [32, 4096, 2048], P('sp', None, 'tp'), may hold values from -0.09375 to 0.09375
- sh_gate: bfloat16 [2048, 512], P(None, 'tp'), may hold values from -0.125 to 0.125
- sh_up: bfloat16 [2048, 512], P(None, 'tp'), may hold values from -0.125 to 0.125
- sh_down: bfloat16 [512, 2048], P(None, 'tp'), may hold values from -0.25 to 0.25
Outputs:
- result: bfloat16 [4096, 2048], P('sp', 'tp')
Inputs may be any that keep to these rules, and one draw needn't show every extreme that they name: `routes`: among the 128 rows of one index of sp, each expert is named at most 32 times, a bound that some block reaches; a row names 4 different experts.
All inputs are finite; a program needn't handle non-finite values.
Results may differ from a plain program's by a relative error of at most 0.007.
Values may be sent and summed in bfloat16 or wider, within the bound.
No kernel may reach another device: no remote copies, remote signals or barrier semaphores. Data moves between devices by JAX's collectives and lax.ppermute only.
A program may use at most 64 MiB of HBM per device.

v0:
```python
import jax
import jax.numpy as jnp
from jax import lax
from jax.sharding import PartitionSpec as P

LN_EPS = 1e-05
RMS_EPS = 1e-06


def shifted(value, axis, by):
    size = lax.axis_size(axis)
    pairs = [(i, i + by) for i in range(size) if 0 <= i + by < size]
    return lax.ppermute(value, axis, pairs)


def sent_to_all(value, axis):
    copies = jnp.broadcast_to(value, (lax.axis_size(axis), *value.shape))
    return lax.all_to_all(copies, axis, split_axis=0, concat_axis=0, tiled=True)


def of_everyone(value, axis):
    return sent_to_all(value, axis).sum(axis=0)


def together(arrays, axis):
    line, at, outs = (jnp.concatenate([a.reshape(-1) for a in arrays]), 0, [])
    so_far = of_everyone(line, axis)
    for a in arrays:
        outs.append(so_far[at : at + a.size].reshape(a.shape))
        at += a.size
    return tuple(outs)


def cut_along(value, dim, size):
    before, after = (value.shape[:dim], value.shape[dim + 1 :])
    return jnp.moveaxis(value.reshape(*before, size, -1, *after), dim, 0)


def summed_on_arrival(value, axis, dim):
    parts = cut_along(value, dim, lax.axis_size(axis))
    arrived = lax.all_to_all(parts, axis, split_axis=0, concat_axis=0, tiled=True)
    return arrived.sum(axis=0)


def laid_out(parts, dim):
    lengths = list(parts.shape[1:])
    lengths[dim] *= parts.shape[0]
    return jnp.moveaxis(parts, 0, dim).reshape(lengths)


def gather_directly(value, axis, dim):
    return laid_out(sent_to_all(value, axis), dim)


def body(
    resid,
    a_val,
    a_gate,
    conv_kernel,
    conv_bias,
    ln_gain,
    ln_bias,
    w_out,
    ffn_gain,
    routes,
    route_weights,
    exp_gate,
    exp_up,
    exp_down,
    sh_gate,
    sh_up,
    sh_down,
):
    tp_count = lax.axis_size("tp")
    tp_place = lax.axis_index("tp")
    sp_count = lax.axis_size("sp")
    tok_rows = resid.shape[0]
    model_width = resid.shape[1]
    col_width = model_width // tp_count
    col_start = tp_place * col_width
    conv_span = conv_kernel.shape[0]
    channels_all = a_val.shape[1] * tp_count
    gated_in = (a_val.astype(jnp.float32) * jax.nn.sigmoid(a_gate.astype(jnp.float32))).astype(
        jnp.bfloat16
    )
    before = shifted(gated_in[tok_rows - (conv_span - 1) :], "sp", 1)
    padded = jnp.concatenate([before, gated_in], axis=0).astype(jnp.float32)
    kernel = conv_kernel.astype(jnp.float32)

    def add_tap(offset, running):
        window_rows = lax.dynamic_slice_in_dim(padded, offset, tok_rows, 0)
        return running + lax.dynamic_slice_in_dim(kernel, offset, 1, 0) * window_rows

    start_sum = jnp.broadcast_to(conv_bias[None, :], gated_in.shape)
    conv_out = lax.fori_loop(0, conv_span, add_tap, start_sum)
    row_sums = together((jnp.sum(conv_out, axis=1), jnp.sum(conv_out * conv_out, axis=1)), "tp")
    channel_mean = row_sums[0] / channels_all
    channel_var = row_sums[1] / channels_all - channel_mean * channel_mean
    scaled = (conv_out - channel_mean[:, None]) * lax.rsqrt(
        channel_var[:, None] + LN_EPS
    ) * ln_gain[None, :] + ln_bias[None, :]
    mixed_out = jax.nn.silu(scaled).astype(jnp.bfloat16)
    partial_proj = jnp.dot(mixed_out, w_out, preferred_element_type=jnp.float32)
    projected = summed_on_arrival(partial_proj, "tp", 1)
    resid_cols = lax.dynamic_slice_in_dim(resid, col_start, col_width, 1)
    middle_cols = (resid_cols.astype(jnp.float32) + projected).astype(jnp.bfloat16)
    share_f = middle_cols.astype(jnp.float32)
    squares = of_everyone(jnp.sum(share_f * share_f, axis=1), "tp")
    gain_cols = lax.dynamic_slice_in_dim(ffn_gain, col_start, col_width, 0)
    inverse = lax.rsqrt(squares[:, None] / model_width + RMS_EPS)
    normed_cols = (share_f * inverse * gain_cols[None, :]).astype(jnp.bfloat16)
    normed = gather_directly(normed_cols, "tp", 1)
    shared_gate = jnp.dot(normed, sh_gate, preferred_element_type=jnp.float32)
    shared_up = jnp.dot(normed, sh_up, preferred_element_type=jnp.float32)
    shared_hidden = (jax.nn.silu(shared_gate) * shared_up).astype(jnp.bfloat16)
    weight_rows = sh_down
    shared = jnp.dot(
        lax.all_gather(shared_hidden, "tp", axis=1, tiled=True),
        weight_rows,
        preferred_element_type=jnp.float32,
    )
    top_count = routes.shape[1]
    local_experts = exp_gate.shape[0]
    experts_all = local_experts * sp_count
    capacity = max(2 * tok_rows * top_count // experts_all, tp_count)
    pair_count = tok_rows * top_count
    chosen = routes.reshape(pair_count)
    one_hot = (chosen[:, None] == jnp.arange(experts_all, dtype=jnp.int32)[None, :]).astype(
        jnp.int32
    )
    earlier = jnp.cumsum(one_hot, axis=0) - one_hot
    place_in = jnp.sum(earlier * one_hot, axis=1)
    slot_of = chosen * capacity + place_in
    owner_ids = (
        jnp.zeros((experts_all * capacity,), jnp.int32)
        .at[slot_of]
        .set(jnp.arange(pair_count, dtype=jnp.int32) + 1)
    )
    owner_grid = owner_ids.reshape(sp_count, local_experts, capacity)
    part_slots = capacity // tp_count
    own_owners = lax.dynamic_slice_in_dim(owner_grid, tp_place * part_slots, part_slots, 2)
    source_row = jnp.maximum(own_owners - 1, 0) // top_count
    taken = normed[source_row.reshape(-1)].reshape(own_owners.shape + (model_width,))
    landed = lax.all_to_all(
        jnp.where((own_owners > 0)[..., None], taken, jnp.zeros((), jnp.bfloat16)),
        "sp",
        split_axis=0,
        concat_axis=0,
        tiled=True,
    )
    arrived = lax.all_gather(landed, "tp", axis=2, tiled=True)
    gate_part = jnp.einsum("sxcd,xdf->sxcf", arrived, exp_gate, preferred_element_type=jnp.float32)
    up_part = jnp.einsum("sxcd,xdf->sxcf", arrived, exp_up, preferred_element_type=jnp.float32)
    expert_hidden = (jax.nn.silu(gate_part) * up_part).astype(jnp.bfloat16)
    weight_rows = exp_down
    expert_sum = jnp.einsum(
        "sxcf,xfd->sxcd",
        lax.all_gather(expert_hidden, "tp", axis=3, tiled=True),
        weight_rows,
        preferred_element_type=jnp.float32,
    )
    expert_out = expert_sum.astype(jnp.bfloat16)
    returned = lax.all_to_all(expert_out, "sp", split_axis=0, concat_axis=0, tiled=True)
    flat_out = returned.reshape(experts_all * capacity, col_width)
    picked = flat_out[slot_of].astype(jnp.float32).reshape(tok_rows, top_count, col_width)
    routed = jnp.sum(picked * route_weights[:, :, None], axis=1)
    return (middle_cols.astype(jnp.float32) + shared + routed).astype(jnp.bfloat16)


def solution(mesh):
    in_specs = (
        P("sp", None),
        P("sp", "tp"),
        P("sp", "tp"),
        P(None, "tp"),
        P("tp"),
        P("tp"),
        P("tp"),
        P("tp", None),
        P(),
        P("sp", None),
        P("sp", None),
        P("sp", None, "tp"),
        P("sp", None, "tp"),
        P("sp", None, "tp"),
        P(None, "tp"),
        P(None, "tp"),
        P(None, "tp"),
    )
    out_specs = P("sp", "tp")
    return jax.shard_map(body, mesh=mesh, in_specs=in_specs, out_specs=out_specs, check_vma=False)
```

profile of v0, /device:TPU:1, one launch (start us, length us, event | category | flops | bytes accessed | tf_op | source)
XLA Modules:
  0.0 289.1 jit_solution(5192437029576323760)
XLA Ops:
  6.5 0.9 multiply_convert_fusion.1
  7.5 3.9 %collective-permute-start = (bf16[30,64]{0,1:T(8,128)(2,1)S(1)}, bf16[30,64]{0,1:T(8,128)(2,1)S(1)}, u32[]{:S(2)}, u32[]{:S(2)}) collective-permute-start(bf16[30,64]{0,1:T(8,128)(2,1)S(1)} %slice.24), channel_id=1, source_target_pairs={{0,16},{16,32},{32,48},{48,64},{64,80},{80,96},{96,112},{112,128},... | collective-permute-start | bytes 11528 | tf_op jit(solution)/shard_map/ppermute | solution.py:13
  11.4 0.7 convert_element_type.67
  12.1 0.1 collective-permute-done
  12.3 0.7 broadcast_in_dim.20
  13.0 7.4 %while.13 = (s32[]{:T(128)}, f32[128,64]{1,0:T(8,128)S(1)}, f32[31,64]{1,0:T(8,128)S(1)}, f32[158,64]{0,1:T(8,128)S(1)}, s32[]{:T(128)}) while((s32[]{:T(128)}, f32[128,64]{1,0:T(8,128)S(1)}, f32[31,64]{1,0:T(8,128)S(1)}, f32[158,64]{0,1:T(8,128)S(1)}, s32[]{:T(128)}) %tuple.33), condition=%wide.region_1.0_spmd, body=%wide.region_0.0_spmd.sunk | while | flops 16386 | bytes 230221 | solution.py:95
  20.5 0.6 broadcast_in_dim.21
  21.2 8.6 %all-to-all-start = ((f32[16,1,256]{2,1,0:T(1,128)}), f32[16,1,256]{2,1,0:T(1,128)S(1)}, u32[]{:S(2)}, u32[]{:S(2)}) async-start(f32[16,1,256]{2,1,0:T(1,128)} %broadcast_in_dim.21), calls=%async_computation | async-start | bytes 32768 | tf_op jit(solution)/shard_map/all_to_all | solution.py:18
  29.9 7.3 %all-to-all-done = f32[16,1,256]{2,1,0:T(1,128)S(1)} async-done(((f32[16,1,256]{2,1,0:T(1,128)}), f32[16,1,256]{2,1,0:T(1,128)S(1)}, u32[]{:S(2)}, u32[]{:S(2)}) %all-to-all-start) | async-done | bytes 16416 | tf_op jit(solution)/shard_map/all_to_all | solution.py:18
  37.2 1.4 convolution_bitcast_fusion
  38.6 1.1 copy.143
  39.7 3.8 %all-to-all-start.1 = ((f32[16,128,128]{2,1,0:T(8,128)}), f32[16,128,128]{2,1,0:T(8,128)S(1)}, u32[]{:S(2)}, u32[]{:S(2)}) async-start(f32[16,128,128]{2,1,0:T(8,128)} %bitcast.117), calls=%async_computation.1 | async-start | bytes 2097152 | tf_op jit(solution)/shard_map/all_to_all | solution.py:41
  43.5 0.1 copy.103
  43.8 0.1 eq.25
  43.9 0.1 copy.102
  44.1 1.2 reduce-window.6
  45.3 0.2 slice_reduce_fusion
  45.6 0.1 fusion.39
  45.7 25.9 %all-to-all-done.1 = f32[16,128,128]{2,1,0:T(8,128)S(1)} async-done(((f32[16,128,128]{2,1,0:T(8,128)}), f32[16,128,128]{2,1,0:T(8,128)S(1)}, u32[]{:S(2)}, u32[]{:S(2)}) %all-to-all-start.1) | async-done | bytes 1048608 | tf_op jit(solution)/shard_map/all_to_all | solution.py:41
  71.6 0.9 fusion.34
  72.5 0.6 broadcast_in_dim.26
  73.1 3.4 %all-to-all-start.2 = ((f32[16,1,128]{2,1,0:T(1,128)}), f32[16,1,128]{2,1,0:T(1,128)S(1)}, u32[]{:S(2)}, u32[]{:S(2)}) async-start(f32[16,1,128]{2,1,0:T(1,128)} %broadcast_in_dim.26), calls=%async_computation.2 | async-start | bytes 16384 | tf_op jit(solution)/shard_map/all_to_all | solution.py:18
  76.6 0.8 dynamic_slice.24
  77.3 6.2 %all-to-all-done.2 = f32[16,1,128]{2,1,0:T(1,128)S(1)} async-done(((f32[16,1,128]{2,1,0:T(1,128)}), f32[16,1,128]{2,1,0:T(1,128)S(1)}, u32[]{:S(2)}, u32[]{:S(2)}) %all-to-all-start.2) | async-done | bytes 8224 | tf_op jit(solution)/shard_map/all_to_all | solution.py:18
  83.7 0.9 broadcast_in_dim.27
  84.6 4.0 %all-to-all-start.3 = ((bf16[16,128,128]{2,1,0:T(8,128)(2,1)}), bf16[16,128,128]{2,1,0:T(8,128)(2,1)S(1)}, u32[]{:S(2)}, u32[]{:S(2)}) async-start(bf16[16,128,128]{2,1,0:T(8,128)(2,1)} %broadcast_in_dim.27), calls=%async_computation.3 | async-start | bytes 1048576 | tf_op jit(solution)/shard_map/all_to_all | solution.py:18
  88.6 2.4 scatter_custom_fusion
  91.3 0.1 copy.107
  91.7 14.2 %all-to-all-done.3 = bf16[16,128,128]{2,1,0:T(8,128)(2,1)S(1)} async-done(((bf16[16,128,128]{2,1,0:T(8,128)(2,1)}), bf16[16,128,128]{2,1,0:T(8,128)(2,1)S(1)}, u32[]{:S(2)}, u32[]{:S(2)}) %all-to-all-start.3) | async-done | bytes 524320 | tf_op jit(solution)/shard_map/all_to_all | solution.py:18
  106.0 0.7 gather_fusion
  106.7 0.2 reshape.161
  106.9 0.3 broadcast_select_fusion
  107.2 27.0 %all_to_all.32 = bf16[32,1,2,2048]{3,2,1,0:T(2,128)(2,1)S(1)} all-to-all(bf16[32,1,2,2048]{3,2,1,0:T(2,128)(2,1)S(1)} %broadcast_select_fusion), channel_id=1, replica_groups=mesh['sp'=32,'tp'=16] {'sp'}, dimensions={0} | all-to-all | bytes 524288 | tf_op jit(solution)/shard_map/all_to_all | solution.py:144
  134.2 0.8 copy.110
  135.0 0.2 all-gather.5.cloned.1.call-start
  135.2 35.9 %all-gather.3.cloned.1.call-done = bf16[32,1,32,2048]{3,0,1,2:T(8,128)(2,1)} async-done(((bf16[32,1,2,2048]{3,0,1,2:T(8,128)(2,1)}), bf16[32,1,32,2048]{3,0,1,2:T(8,128)(2,1)}) %all-gather.3.cloned.1.call-update) | async-done | bytes 4194320 | tf_op jit(solution)/shard_map/all_gather | solution.py:151
  171.2 5.2 %fusion.9 = f32[32,1,32,256]{3,2,0,1:T(8,128)S(1)} fusion(bf16[32,1,32,2048]{3,0,1,2:T(8,128)(2,1)} %all-gather.3.cloned.1.call-done, bf16[1,2048,256]{2,1,0:T(8,128)(2,1)S(1)} %copy-done), kind=kOutput, calls=%fused_computation.15 | convolution fusion | flops 1073741824 | bytes 6291456 | tf_op jit(solution)/shard_map/sxcd,xdf->sxcf/dot_general | solution.py:152
  176.4 3.8 %fusion.18 = bf16[32,1,32,256]{3,2,0,1:T(8,128)(2,1)} fusion(bf16[32,1,32,2048]{3,0,1,2:T(8,128)(2,1)S(1)} %copy-done.4, bf16[1,2048,256]{2,1,0:T(8,128)(2,1)S(1)} %copy-done.5, f32[32,1,32,256]{3,2,0,1:T(8,128)S(1)} %fusion.9), kind=kOutput, calls=%fused_computation.19 | convolution fusion | flops 1075314688 | bytes 6815744 | tf_op jit(solution)/shard_map/sxcd,xdf->sxcf/dot_general | solution.py:153
  180.2 0.1 copy.113
  180.4 68.2 %all-gather.5.cloned.1.call-done = bf16[32,1,32,4096]{3,2,0,1:T(8,128)(2,1)} async-done(((bf16[32,1,32,256]{3,2,0,1:T(8,128)(2,1)}), bf16[32,1,32,4096]{3,2,0,1:T(8,128)(2,1)}) %all-gather.5.cloned.1.call-update) | async-done | bytes 8388624 | tf_op jit(solution)/shard_map/all_gather | solution.py:158
  248.6 6.6 %fusion.24 = bf16[32,1,32,128]{3,2,1,0:T(8,128)(2,1)} fusion(bf16[32,1,32,4096]{3,2,0,1:T(8,128)(2,1)} %all-gather.5.cloned.1.call-done, bf16[1,4096,128]{2,1,0:T(8,128)(2,1)} %param.32), kind=kOutput, calls=%fused_computation.21 | convolution fusion | flops 1073872896 | bytes 9699328 | tf_op jit(solution)/shard_map/sxcf,xfd->sxcd/dot_general | solution.py:156
  255.2 6.9 %all-to-all-start.5 = ((bf16[32,1,32,128]{3,2,1,0:T(8,128)(2,1)}), bf16[32,1,32,128]{3,2,1,0:T(8,128)(2,1)S(1)}, u32[]{:S(2)}, u32[]{:S(2)}) async-start(bf16[32,1,32,128]{3,2,1,0:T(8,128)(2,1)} %fusion.24), calls=%async_computation.5 | async-start | bytes 524288 | tf_op jit(solution)/shard_map/all_to_all | solution.py:163
  262.1 0.3 fusion.50
  262.4 0.3 fusion.29
  262.7 17.1 %all_gather.9 = bf16[128,512]{0,1:T(8,128)(2,1)S(1)} all-gather(bf16[128,32]{0,1:T(8,128)(2,1)S(1)} %fusion.29), channel_id=1, replica_groups=mesh['sp'=32,'tp'=16] {'tp'}, dimensions={1}, use_global_device_ids=true | all-gather | bytes 139264 | tf_op jit(solution)/shard_map/all_gather | solution.py:118
  279.8 1.3 gather_fusion.1
  281.2 0.2 fusion.33
  281.4 0.9 fusion.28
  (174 shorter events, 7.8 us)
Async XLA Ops:
  6.5 164.6 %copy-start = (bf16[1,2048,256]{2,1,0:T(8,128)(2,1)S(1)}, bf16[1,2048,256]{2,1,0:T(8,128)(2,1)}, u32[]{:S(2)}) copy-start(bf16[1,2048,256]{2,1,0:T(8,128)(2,1)} %param.30) | copy-start | bytes 3145732
  6.5 37.0 %copy-start.2 = (s32[128,4]{0,1:T(4,128)S(1)}, s32[128,4]{0,1:T(4,128)}, u32[]{:S(2)}) copy-start(s32[128,4]{0,1:T(4,128)} %param.28) | copy-start | bytes 6148
  7.5 4.8 %collective-permute-start = (bf16[30,64]{0,1:T(8,128)(2,1)S(1)}, bf16[30,64]{0,1:T(8,128)(2,1)S(1)}, u32[]{:S(2)}, u32[]{:S(2)}) collective-permute-start(bf16[30,64]{0,1:T(8,128)(2,1)S(1)} %slice.24), channel_id=1, source_target_pairs={{0,16},{16,32},{32,48},{48,64},{64,80},{80,96},{96,112},{112,128},... | collective-permute-start | bytes 11528 | tf_op jit(solution)/shard_map/ppermute | solution.py:13
  21.2 16.0 %all-to-all-start = ((f32[16,1,256]{2,1,0:T(1,128)}), f32[16,1,256]{2,1,0:T(1,128)S(1)}, u32[]{:S(2)}, u32[]{:S(2)}) async-start(f32[16,1,256]{2,1,0:T(1,128)} %broadcast_in_dim.21), calls=%async_computation | async-start | bytes 32768 | tf_op jit(solution)/shard_map/all_to_all | solution.py:18
  39.7 31.9 %all-to-all-start.1 = ((f32[16,128,128]{2,1,0:T(8,128)}), f32[16,128,128]{2,1,0:T(8,128)S(1)}, u32[]{:S(2)}, u32[]{:S(2)}) async-start(f32[16,128,128]{2,1,0:T(8,128)} %bitcast.117), calls=%async_computation.1 | async-start | bytes 2097152 | tf_op jit(solution)/shard_map/all_to_all | solution.py:41
  73.1 10.4 %all-to-all-start.2 = ((f32[16,1,128]{2,1,0:T(1,128)}), f32[16,1,128]{2,1,0:T(1,128)S(1)}, u32[]{:S(2)}, u32[]{:S(2)}) async-start(f32[16,1,128]{2,1,0:T(1,128)} %broadcast_in_dim.26), calls=%async_computation.2 | async-start | bytes 16384 | tf_op jit(solution)/shard_map/all_to_all | solution.py:18
  84.6 21.3 %all-to-all-start.3 = ((bf16[16,128,128]{2,1,0:T(8,128)(2,1)}), bf16[16,128,128]{2,1,0:T(8,128)(2,1)S(1)}, u32[]{:S(2)}, u32[]{:S(2)}) async-start(bf16[16,128,128]{2,1,0:T(8,128)(2,1)} %broadcast_in_dim.27), calls=%async_computation.3 | async-start | bytes 1048576 | tf_op jit(solution)/shard_map/all_to_all | solution.py:18
  88.6 82.6 %all-gather.3.cloned.1.call-start = ((), (), s32[]{:S(2)}) async-start(), calls=%async_computation.6 | async-start | bytes 4456448 | tf_op jit(solution)/shard_map/all_gather | solution.py:151
  135.0 41.4 %copy-start.5 = (bf16[1,2048,256]{2,1,0:T(8,128)(2,1)S(1)}, bf16[1,2048,256]{2,1,0:T(8,128)(2,1)}, u32[]{:S(2)}) copy-start(bf16[1,2048,256]{2,1,0:T(8,128)(2,1)} %param.31) | copy-start | bytes 3145732
  135.0 113.6 %all-gather.5.cloned.1.call-start = ((), (), s32[]{:S(2)}) async-start(), calls=%async_computation.7 | async-start | bytes 8912896 | tf_op jit(solution)/shard_map/all_gather | solution.py:158
  171.2 5.2 %copy-start.4 = (bf16[32,1,32,2048]{3,0,1,2:T(8,128)(2,1)S(1)}, bf16[32,1,32,2048]{3,0,1,2:T(8,128)(2,1)}, u32[]{:S(2)}) copy-start(bf16[32,1,32,2048]{3,0,1,2:T(8,128)(2,1)} %all-gather.3.cloned.1.call-done) | copy-start | bytes 12582916
  176.4 3.8 %copy-start.3 = (f32[128,4]{0,1:T(4,128)S(1)}, f32[128,4]{0,1:T(4,128)}, u32[]{:S(2)}) copy-start(f32[128,4]{0,1:T(4,128)} %param.29) | copy-start | bytes 6148
  180.4 81.8 %copy-start.6 = (bf16[2048,32]{0,1:T(8,128)(2,1)S(1)}, bf16[2048,32]{0,1:T(8,128)(2,1)}, u32[]{:S(2)}) copy-start(bf16[2048,32]{0,1:T(8,128)(2,1)} %param.33) | copy-start | bytes 393220
  180.4 82.0 %copy-start.7 = (bf16[2048,32]{0,1:T(8,128)(2,1)S(1)}, bf16[2048,32]{0,1:T(8,128)(2,1)}, u32[]{:S(2)}) copy-start(bf16[2048,32]{0,1:T(8,128)(2,1)} %param.34) | copy-start | bytes 393220
  180.4 101.0 %copy-start.1 = (bf16[512,128]{1,0:T(8,128)(2,1)S(1)}, bf16[512,128]{1,0:T(8,128)(2,1)}, u32[]{:S(2)}) copy-start(bf16[512,128]{1,0:T(8,128)(2,1)} %param.35) | copy-start | bytes 393220
  255.2 24.6 %all-to-all-start.5 = ((bf16[32,1,32,128]{3,2,1,0:T(8,128)(2,1)}), bf16[32,1,32,128]{3,2,1,0:T(8,128)(2,1)S(1)}, u32[]{:S(2)}, u32[]{:S(2)}) async-start(bf16[32,1,32,128]{3,2,1,0:T(8,128)(2,1)} %fusion.24), calls=%async_computation.5 | async-start | bytes 524288 | tf_op jit(solution)/shard_map/all_to_all | solution.py:163
Sparse Core Ops, SparseCore 0:
  135.1 36.0 all-gather.2
  180.3 68.1 all-gather.4
where the time goes:
time: 290 us; the launch traced here: 289 us
  waiting for transfers between devices  158 us (54%)
  blocking collectives  44.1 us (15%)
  starting transfers between devices  31 us (11%)
  matrix products  18.4 us (6%)
  local copies, waits for them, and re-layouts  17.6 us (6%)
  between operations  13.7 us (5%)
  other arithmetic  5.28 us (2%)
    all_gather x1, waiting for transfers between devices, body(): lax.all_gather(expert_hidden, 'tp', axis=3, tiled=True)  68.2 us
    all_gather x1, waiting for transfers between devices, body(): arrived = lax.all_gather(landed, 'tp', axis=2, tiled=True)  35.9 us
    all_to_all x3, waiting for transfers between devices, sent_to_all(): return lax.all_to_all(copies, axis, split_axis=0, concat_axis=0, tiled=True)  27.7 us
    all_to_all x1, blocking collectives, body(): lax.all_to_all(jnp.where((own_owners > 0)[..., None], taken, jnp.zeros(()...  27 us
    all_to_all x1, waiting for transfers between devices, summed_on_arrival(): lax.all_to_all(parts, axis, split_axis=0, concat_axis=0, tiled=True)  25.9 us
    all_gather x1, blocking collectives, body(): lax.all_gather(shared_hidden, 'tp', axis=1, tiled=True)  17.1 us
    all_to_all x3, starting transfers between devices, sent_to_all(): return lax.all_to_all(copies, axis, split_axis=0, concat_axis=0, tiled=True)  16.1 us
    all_to_all x1, starting transfers between devices, body(): lax.all_to_all(expert_out, 'sp', split_axis=0, concat_axis=0, tiled=True)  6.89 us
  transfers between devices with their start and end apart: 8, of which 7 were waited for; matrix products, arithmetic and copies ran while one was open for 3% of the time, Pallas kernels for 0%

commit v1 on v0

v1 whole, which is shorter than its diff:
```python
import jax
import jax.numpy as jnp
from jax import lax
from jax.experimental import pallas as pl
from jax.experimental.pallas import tpu as pltpu
from jax.sharding import PartitionSpec as P

LN_EPS = 1e-05
RMS_EPS = 1e-06
LANES = 128
F32 = jnp.float32
BF16 = jnp.bfloat16


def rounded(value):
    return lax.reduce_precision(value, exponent_bits=8, mantissa_bits=7)


def in_three(value):
    high = rounded(value)
    mid = rounded(value - high)
    low = value - high - mid
    return high.astype(BF16), mid.astype(BF16), low.astype(BF16)


def silu(v):
    return v / (1.0 + jnp.exp(-v))


def front_kernel(span, packed, wcol, resid, slots, middle_out, send_out, win, conv):
    peers, rows, _ = packed.shape
    tok_rows = resid.shape[0]
    half = packed.shape[2] // 2
    channels = peers * half
    for pair in range(peers // 2):
        one, two = packed[2 * pair], packed[2 * pair + 1]
        at = pair * LANES
        left = jnp.concatenate([one[:, :half], two[:, :half]], axis=1)
        right = jnp.concatenate([one[:, half:], two[:, half:]], axis=1)
        win[0, :, at : at + LANES] = left.astype(F32)
        win[1, :, at : at + LANES] = right.astype(F32)

    def vector(first):
        high, mid, low = (win[1, first + i : first + i + 1, :] for i in range(3))
        return high + mid + low

    conv_rows = 64

    def one_block(i, _):
        cols = pl.ds(pl.multiple_of(i * LANES, LANES), LANES)
        taps = win[1, 0:span, cols]
        b = sum(win[1, span + n : span + n + 1, cols] for n in range(3))
        for r in range(0, tok_rows, conv_rows):
            acc = jnp.broadcast_to(b, (conv_rows, LANES))
            for j in range(span):
                acc = acc + taps[j : j + 1, :] * win[0, r + j : r + j + conv_rows, cols]
            conv[r : r + conv_rows, cols] = acc
        return 0

    lax.fori_loop(0, channels // LANES, one_block, 0)
    gain = vector(span + 3)
    shift = vector(span + 6)
    for r in range(0, tok_rows, 64):
        c = conv[r : r + 64, :]
        mean = jnp.sum(c, axis=1, keepdims=True) * (1.0 / channels)
        var = jnp.sum(c * c, axis=1, keepdims=True) * (1.0 / channels) - mean * mean
        scaled = (c - mean) * lax.rsqrt(var + LN_EPS) * gain + shift
        mixed = silu(scaled).astype(BF16)
        proj = jnp.dot(mixed, wcol[...], preferred_element_type=F32)
        middle_out[r : r + 64, :] = (resid[r : r + 64, :].astype(F32) + proj).astype(BF16)
    middle = middle_out[...]
    block = 256
    for r in range(0, send_out.shape[0], block):
        ids = lax.broadcasted_iota(jnp.int32, (block, tok_rows), 0) + r
        hit = ids == slots[0:1, :]
        for k in range(1, slots.shape[0]):
            hit = hit | (ids == slots[k : k + 1, :])
        pick = jnp.where(hit, 1.0, 0.0).astype(BF16)
        send_out[r : r + block, :] = jnp.dot(pick, middle, preferred_element_type=F32).astype(BF16)


def front(span, packed, wcol, resid, slots, slot_count):
    tok_rows, cols = resid.shape
    channels = packed.shape[0] * packed.shape[2] // 2

    def kernel(*refs):
        front_kernel(span, *refs)

    return pl.pallas_call(
        kernel,
        out_shape=(
            jax.ShapeDtypeStruct((tok_rows, cols), BF16),
            jax.ShapeDtypeStruct((slot_count, cols), BF16),
        ),
        scratch_shapes=[
            pltpu.VMEM((2, packed.shape[1], channels), F32),
            pltpu.VMEM((tok_rows, channels), F32),
        ],
        name="front",
    )(packed, wcol, resid, slots)


def hidden_kernel(width, rows_in, gain, wg, wu, out):
    pieces = rows_in.shape[0]
    squares = jnp.zeros((rows_in.shape[1], LANES), F32)
    for t in range(pieces):
        x = rows_in[t].astype(F32)
        squares = squares + x * x
    mean = jnp.sum(squares, axis=1, keepdims=True) / width
    inverse = lax.rsqrt(mean + RMS_EPS)
    normed = jnp.concatenate(
        [(rows_in[t].astype(F32) * inverse * gain[t : t + 1, :]).astype(BF16) for t in range(pieces)],
        axis=1,
    )
    g = jnp.dot(normed, wg[...], preferred_element_type=F32)
    u = jnp.dot(normed, wu[...], preferred_element_type=F32)
    out[...] = (silu(g) * u).astype(BF16)


def hidden_units(rows_in, gain, wg, wu):
    pieces, rows, lanes = rows_in.shape
    width, units = wg.shape
    block = 256

    def kernel(*refs):
        hidden_kernel(width, *refs)

    return pl.pallas_call(
        kernel,
        grid=(rows // block,),
        in_specs=[
            pl.BlockSpec((pieces, block, lanes), lambda i: (0, i, 0)),
            pl.BlockSpec((pieces, lanes), lambda i: (0, 0)),
            pl.BlockSpec((width, units), lambda i: (0, 0)),
            pl.BlockSpec((width, units), lambda i: (0, 0)),
        ],
        out_specs=pl.BlockSpec((block, units), lambda i: (i, 0)),
        out_shape=jax.ShapeDtypeStruct((rows, units), BF16),
        name="hidden",
    )(rows_in, gain, wg, wu)


def down_kernel(hidden, wd, out):
    whole = jnp.concatenate([hidden[t] for t in range(hidden.shape[0])], axis=1)
    out[...] = jnp.dot(whole, wd[...], preferred_element_type=F32).astype(BF16)


def down(hidden, wd):
    pieces, rows, units = hidden.shape
    block = 256
    return pl.pallas_call(
        down_kernel,
        grid=(rows // block,),
        in_specs=[
            pl.BlockSpec((pieces, block, units), lambda i: (0, i, 0)),
            pl.BlockSpec(wd.shape, lambda i: (0, 0)),
        ],
        out_specs=pl.BlockSpec((block, wd.shape[1]), lambda i: (i, 0)),
        out_shape=jax.ShapeDtypeStruct((rows, wd.shape[1]), BF16),
        name="down",
    )(hidden, wd)


def combine_kernel(returned, slots, weights, middle, shared, out):
    shape = (slots.shape[0], returned.shape[0])
    ids = lax.broadcasted_iota(jnp.int32, shape, 1)
    table = jnp.zeros(shape, F32)
    for k in range(slots.shape[1]):
        table = jnp.where(ids == slots[:, k : k + 1], weights[:, k : k + 1], table)
    routed = jnp.zeros(out.shape, F32)
    for _ in range(3):
        part = table.astype(BF16)
        routed = routed + jnp.dot(part, returned[...], preferred_element_type=F32)
        table = table - part.astype(F32)
    out[...] = (middle[...].astype(F32) + shared[...] + routed).astype(BF16)


def combine(returned, slots, weights, middle, shared):
    return pl.pallas_call(
        combine_kernel,
        out_shape=jax.ShapeDtypeStruct(middle.shape, BF16),
        name="combine",
    )(returned, slots, weights, middle, shared)


def body(
    resid,
    a_val,
    a_gate,
    conv_kernel,
    conv_bias,
    ln_gain,
    ln_bias,
    w_out,
    ffn_gain,
    routes,
    route_weights,
    exp_gate,
    exp_up,
    exp_down,
    sh_gate,
    sh_up,
    sh_down,
):
    tp_count = lax.axis_size("tp")
    tp_place = lax.axis_index("tp")
    sp_count = lax.axis_size("sp")
    tok_rows, model_width = resid.shape
    col_width = model_width // tp_count
    span = conv_kernel.shape[0]
    top_count = routes.shape[1]
    experts_all = exp_gate.shape[0] * sp_count
    capacity = max(2 * tok_rows * top_count // experts_all, tp_count)
    pair_count = tok_rows * top_count
    slot_count = experts_all * capacity

    w_parts = jnp.moveaxis(w_out.reshape(w_out.shape[0], tp_count, col_width), 1, 0)
    wcol = lax.all_to_all(w_parts, "tp", split_axis=0, concat_axis=0, tiled=True)
    wcol = wcol.reshape(w_out.shape[0] * tp_count, col_width)

    gated = (a_val.astype(F32) * jax.nn.sigmoid(a_gate.astype(F32))).astype(BF16)
    halo = span - 1
    pairs = [(i, i + 1) for i in range(sp_count - 1)]
    before = lax.ppermute(gated[tok_rows - halo :], "sp", pairs)
    rows = -(-(halo + tok_rows) // 16) * 16
    vectors = [p[None, :] for v in (conv_bias, ln_gain, ln_bias) for p in in_three(v)]
    right = jnp.concatenate([conv_kernel, *vectors], axis=0)
    right = jnp.pad(right, ((0, rows - right.shape[0]), (0, 0)))
    left = jnp.concatenate([before, gated], axis=0)
    left = jnp.pad(left, ((0, rows - left.shape[0]), (0, 0)))
    packed = lax.all_gather(jnp.concatenate([left, right], axis=1), "tp")

    chosen = routes.reshape(pair_count)
    one_hot = (chosen[:, None] == jnp.arange(experts_all, dtype=jnp.int32)[None, :]).astype(BF16)
    order = jnp.arange(pair_count, dtype=jnp.int32)
    below = (order[:, None] > order[None, :]).astype(BF16)
    earlier = jnp.dot(below, one_hot, preferred_element_type=F32)
    place_in = jnp.sum(earlier * one_hot.astype(F32), axis=1).astype(jnp.int32)
    slots = (chosen * capacity + place_in).reshape(tok_rows, top_count)

    resid_cols = lax.dynamic_slice_in_dim(resid, tp_place * col_width, col_width, 1)
    middle, send = front(span, packed, wcol, resid_cols, slots.T, slot_count)

    landed = lax.all_to_all(
        send.reshape(sp_count, slot_count // sp_count, col_width),
        "sp",
        split_axis=0,
        concat_axis=0,
        tiled=True,
    ).reshape(slot_count, col_width)
    gain = ffn_gain.reshape(tp_count, col_width)
    arrived = lax.all_gather(landed, "tp")
    hidden = hidden_units(arrived, gain, exp_gate[0], exp_up[0])

    middle_late, landed_late = lax.optimization_barrier((middle, landed[:1]))
    middle_all = lax.all_gather(middle_late, "tp")
    middle_f = jnp.moveaxis(middle_all, 0, 1).reshape(tok_rows, model_width).astype(F32)
    squares = jnp.sum(middle_f * middle_f, axis=1, keepdims=True)
    inverse = lax.rsqrt(squares / model_width + RMS_EPS)
    normed = (middle_f * inverse * ffn_gain[None, :]).astype(BF16)
    shared_gate = jnp.dot(normed, sh_gate, preferred_element_type=F32)
    shared_up = jnp.dot(normed, sh_up, preferred_element_type=F32)
    shared_hidden = (jax.nn.silu(shared_gate) * shared_up).astype(BF16)

    hidden_all = lax.all_gather(hidden, "tp")
    shared_late, _ = lax.optimization_barrier((shared_hidden, hidden[:1]))
    shared = jnp.dot(
        lax.all_gather(shared_late, "tp", axis=1, tiled=True),
        sh_down,
        preferred_element_type=F32,
    )
    hidden_all, shared = lax.optimization_barrier((hidden_all, shared))

    expert_out = down(hidden_all, exp_down[0])
    returned = lax.all_to_all(
        expert_out.reshape(sp_count, slot_count // sp_count, col_width),
        "sp",
        split_axis=0,
        concat_axis=0,
        tiled=True,
    ).reshape(slot_count, col_width)
    return combine(returned, slots, route_weights, middle, shared)


def solution(mesh):
    in_specs = (
        P("sp", None),
        P("sp", "tp"),
        P("sp", "tp"),
        P(None, "tp"),
        P("tp"),
        P("tp"),
        P("tp"),
        P("tp", None),
        P(),
        P("sp", None),
        P("sp", None),
        P("sp", None, "tp"),
        P("sp", None, "tp"),
        P("sp", None, "tp"),
        P(None, "tp"),
        P(None, "tp"),
        P(None, "tp"),
    )
    out_specs = P("sp", "tp")
    return jax.shard_map(body, mesh=mesh, in_specs=in_specs, out_specs=out_specs, check_vma=False)
```

time: 290 us -> 223 us (0.77)
  waiting for transfers between devices: 158 us -> 70.9 us
  blocking collectives: 44.1 us -> 78.9 us
  Pallas kernels: 0 us -> 20.9 us
  matrix products: 18.4 us -> 2.44 us
  starting transfers between devices: 31 us -> 22.1 us
  local copies, waits for them, and re-layouts: 17.6 us -> 8.73 us
    all_gather x2, waiting for transfers between devices: 104 us -> 60 us  [the longest x1 39.2 us: body(): arrived = lax.all_gather(landed, 'tp')]
    all_to_all x5 -> x2, waiting for transfers between devices: 53.6 us -> 10.9 us  [the longest x1 10.9 us: body(): lax.all_to_all(expert_out.reshape(sp_count, slot_count // sp_count, col_w...]
    all_gather x1 -> x3, blocking collectives: 17.1 us -> 54.5 us  [the longest x1 20.4 us: body(): packed = lax.all_gather(jnp.concatenate([left, right], axis=1), 'tp')]
    pallas_call x0 -> x4, Pallas kernels: none -> 20.9 us  [the longest x1 6.69 us: hidden_units(): pl.pallas_call(kernel, grid=(rows // block,), in_specs=[pl.BlockSpec((pie...]
    dot_general x7 -> x4, matrix products: 18.4 us -> 2.44 us  [the longest x1 1.11 us: body(): shared_up = jnp.dot(normed, sh_up, preferred_element_type=F32)]
    all_to_all x5 -> x2, starting transfers between devices: 26.8 us -> 18.1 us  [the longest x1 9.9 us: body(): lax.all_to_all(expert_out.reshape(sp_count, slot_count // sp_count, col_w...]
    dynamic_slice x64 -> x1, local copies, waits for them, and re-layouts: 6.32 us -> 0.63 us  [body(): lax.dynamic_slice_in_dim(resid, tp_place * col_width, col_width, 1)]
    unnamed x19, local copies, waits for them, and re-layouts: 0.35 us -> 3.76 us
  transfers between devices with their start and end apart: 8 -> 5, of which waited for: 7 -> 3; matrix products, arithmetic and copies ran while one was open for 3% -> 6% of each run, Pallas kernels for 0% -> 0%
where the time goes in v1:
time: 223 us; the launch traced here: 222 us
  blocking collectives  78.9 us (35%)
  waiting for transfers between devices  70.9 us (32%)
  starting transfers between devices  22.1 us (10%)
  Pallas kernels  20.9 us (9%)
  between operations  13.6 us (6%)
  local copies, waits for them, and re-layouts  8.73 us (4%)
  other arithmetic  4.22 us (2%)
  matrix products  2.44 us (1%)
    all_gather x1, waiting for transfers between devices, body(): arrived = lax.all_gather(landed, 'tp')  39.2 us
    all_to_all x1, blocking collectives, body(): lax.all_to_all(send.reshape(sp_count, slot_count // sp_count, col_width),...  24.3 us
    all_gather x1, waiting for transfers between devices, body(): hidden_all = lax.all_gather(hidden, 'tp')  20.7 us
    all_gather x1, blocking collectives, body(): packed = lax.all_gather(jnp.concatenate([left, right], axis=1), 'tp')  20.4 us
    all_gather x1, blocking collectives, body(): middle_all = lax.all_gather(middle_late, 'tp')  18.4 us
    all_gather x1, blocking collectives, body(): lax.all_gather(shared_late, 'tp', axis=1, tiled=True)  15.7 us
    all_to_all x1, waiting for transfers between devices, body(): lax.all_to_all(expert_out.reshape(sp_count, slot_count // sp_count, col_w...  10.9 us
    all_to_all x1, starting transfers between devices, body(): lax.all_to_all(expert_out.reshape(sp_count, slot_count // sp_count, col_w...  9.9 us
  transfers between devices with their start and end apart: 5, of which 3 were waited for; matrix products, arithmetic and copies ran while one was open for 6% of the time, Pallas kernels for 0%

profile of v1, /device:TPU:1, one launch (start us, length us, event | category | flops | bytes accessed | tf_op | source)
XLA Modules:
  0.0 221.8 jit_solution(2855925693692652073)
XLA Ops:
  6.5 0.8 multiply_convert_fusion
  7.4 3.9 %collective-permute-start = (bf16[30,64]{0,1:T(8,128)(2,1)S(1)}, bf16[30,64]{0,1:T(8,128)(2,1)S(1)}, u32[]{:S(2)}, u32[]{:S(2)}) collective-permute-start(bf16[30,64]{0,1:T(8,128)(2,1)S(1)} %slice.6), channel_id=1, source_target_pairs={{0,16},{16,32},{32,48},{48,64},{64,80},{80,96},{96,112},{112,128},... | collective-permute-start | bytes 11528 | tf_op jit(solution)/shard_map/ppermute | solution.py:224
  11.4 1.7 bitcast_bitcast_fusion
  13.1 8.2 %all-to-all-start = ((bf16[16,64,128]{2,1,0:T(8,128)(2,1)}), bf16[16,64,128]{2,1,0:T(8,128)(2,1)S(1)}, u32[]{:S(2)}, u32[]{:S(2)}) async-start(bf16[16,64,128]{2,1,0:T(8,128)(2,1)} %bitcast_bitcast_fusion), calls=%async_computation | async-start | bytes 524288 | tf_op jit(solution)/shard_map/all_to_all | solution.py:218
  21.3 0.8 copy.72
  22.1 0.7 broadcast_multiply_fusion
  22.8 0.7 fusion.14
  23.5 0.7 fusion.18
  24.1 0.7 fusion.22
  24.8 0.1 eq.15
  24.9 0.3 fusion
  25.2 0.6 constant_dynamic-slice_fusion.refs_2_
  25.8 0.1 copy.61
  25.9 0.1 copy.62
  26.0 0.1 copy.63
  26.1 0.1 copy.64
  26.3 0.1 copy.65
  26.4 0.1 copy.66
  26.5 0.1 copy.67
  26.6 0.1 copy.68
  26.7 0.1 copy.69
  26.8 0.8 copy.60
  27.6 0.1 convert_element_type.88
  27.8 0.1 copy.73
  27.9 0.7 copy.74.refs_3_
  28.6 0.1 concatenate.10
  28.8 0.1 copy.70
  28.9 20.4 %all-gather = bf16[2560,128]{1,0:T(8,128)(2,1)} all-gather(bf16[160,128]{1,0:T(8,128)(2,1)S(1)} %copy.70), channel_id=2, replica_groups=mesh['sp'=32,'tp'=16] {'tp'}, dimensions={0}, use_global_device_ids=true | all-gather | bytes 696320 | tf_op jit(solution)/shard_map/all_gather | solution.py:231
  49.3 0.7 copy-done.2
  50.0 5.6 %front.1 = (bf16[128,128]{1,0:T(8,128)(2,1)}, bf16[1024,128]{1,0:T(8,128)(2,1)}) custom-call(bf16[16,160,128]{2,1,0:T(8,128)(2,1)} %bitcast.56, bf16[1024,128]{1,0:T(8,128)(2,1)} %bitcast.61, bf16[128,128]{1,0:T(8,128)(2,1)} %constant_dynamic-slice_fusion.refs_2_, s32[4,128]{1,0:T(4,128)} %copy.74.refs_3_), custom_call_target="tpu_custom_call" | custom-call | tf_op jit(solution)/shard_map/front/pallas_call | solution.py:89
  55.6 24.3 %all_to_all.15 = bf16[32,32,128]{2,1,0:T(8,128)(2,1)} all-to-all(bf16[32,32,128]{2,1,0:T(8,128)(2,1)} %bitcast.65), channel_id=1, replica_groups=mesh['sp'=32,'tp'=16] {'sp'}, dimensions={0} | all-to-all | bytes 524288 | tf_op jit(solution)/shard_map/all_to_all | solution.py:244
  80.0 39.2 %all-gather.6.cloned.1.call-done.refs_0_ = bf16[16,1024,128]{2,1,0:T(8,128)(2,1)} async-done(((bf16[1,1024,128]{2,1,0:T(8,128)(2,1)}), bf16[16,1024,128]{2,1,0:T(8,128)(2,1)}) %all-gather.6.cloned.1.call-update) | async-done | bytes 4194320 | tf_op jit(solution)/shard_map/all_gather | solution.py:252
  119.3 6.7 %hidden.1 = bf16[1024,256]{1,0:T(8,128)(2,1)} custom-call(bf16[16,1024,128]{2,1,0:T(8,128)(2,1)} %all-gather.6.cloned.1.call-done.refs_0_, f32[16,128]{1,0:T(8,128)} %bitcast.66, bf16[2048,256]{1,0:T(8,128)(2,1)} %bitcast.62, bf16[2048,256]{1,0:T(8,128)(2,1)} %bitcast.63), custom_call_target="tpu_custom_call" | custom-call | tf_op jit(solution)/shard_map/hidden/pallas_call | solution.py:128
  126.0 18.4 %all-gather.2 = bf16[2048,128]{1,0:T(8,128)(2,1)S(1)} all-gather(bf16[128,128]{1,0:T(8,128)(2,1)} %get-tuple-element.10.middle), channel_id=4, replica_groups=mesh['sp'=32,'tp'=16] {'tp'}, dimensions={0}, use_global_device_ids=true | all-gather | bytes 557056 | tf_op jit(solution)/shard_map/all_gather | solution.py:256
  144.5 0.3 copy.75
  144.9 0.2 multiply_reduce_fusion
  145.1 0.3 fusion.3
  145.4 0.2 fusion.24
  145.6 1.1 fusion.1
  146.8 15.7 %all_gather.31 = bf16[128,512]{0,1:T(8,128)(2,1)S(1)} all-gather(bf16[128,32]{0,1:T(8,128)(2,1)S(1)} %fusion.1), channel_id=1, replica_groups=mesh['sp'=32,'tp'=16] {'tp'}, dimensions={1}, use_global_device_ids=true | all-gather | bytes 139264 | tf_op jit(solution)/shard_map/all_gather | solution.py:268
  162.5 0.9 fusion.23.shared
  163.3 20.7 %all-gather.8.cloned.1.call-done = bf16[16384,256]{1,0:T(8,128)(2,1)} async-done(((bf16[1024,256]{1,0:T(8,128)(2,1)}), bf16[16384,256]{1,0:T(8,128)(2,1)}) %all-gather.8.cloned.1.call-update) | async-done | bytes 8388624 | tf_op jit(solution)/shard_map/all_gather | solution.py:265
  184.1 6.4 %down.1 = bf16[1024,128]{1,0:T(8,128)(2,1)} custom-call(bf16[16,1024,256]{2,1,0:T(8,128)(2,1)} %bitcast.54, bf16[4096,128]{1,0:T(8,128)(2,1)} %bitcast.57), custom_call_target="tpu_custom_call" | custom-call | tf_op jit(solution)/shard_map/down/pallas_call | solution.py:151
  190.4 9.9 %all-to-all-start.2 = ((bf16[32,32,128]{2,1,0:T(8,128)(2,1)}), bf16[32,32,128]{2,1,0:T(8,128)(2,1)S(1)}, u32[]{:S(2)}, u32[]{:S(2)}) async-start(bf16[32,32,128]{2,1,0:T(8,128)(2,1)} %bitcast.58), calls=%async_computation.2 | async-start | bytes 524288 | tf_op jit(solution)/shard_map/all_to_all | solution.py:275
  200.4 0.7 copy.76.weights
  201.1 10.9 %all-to-all-done.2 = bf16[32,32,128]{2,1,0:T(8,128)(2,1)S(1)} async-done(((bf16[32,32,128]{2,1,0:T(8,128)(2,1)}), bf16[32,32,128]{2,1,0:T(8,128)(2,1)S(1)}, u32[]{:S(2)}, u32[]{:S(2)}) %all-to-all-start.2) | async-done | bytes 262176 | tf_op jit(solution)/shard_map/all_to_all | solution.py:275
  212.0 0.7 copy-done.1
  212.7 2.3 %combine.1 = bf16[128,128]{1,0:T(8,128)(2,1)} custom-call(bf16[1024,128]{1,0:T(8,128)(2,1)} %bitcast.59, s32[128,4]{1,0:T(8,128)} %copy-done.3, f32[128,4]{1,0:T(8,128)} %copy.76.weights, bf16[128,128]{1,0:T(8,128)(2,1)} %get-tuple-element.10.middle, f32[128,128]{1,0:T(8,128)} %fusion.23.shared), custom_call_target="tpu_custom_call" | custom-call | tf_op jit(solution)/shard_map/combine/pallas_call | solution.py:179
  (27 shorter events, 0.4 us)
Async XLA Ops:
  6.5 18.6 %copy-start = (bf16[128,2048]{1,0:T(8,128)(2,1)S(1)}, bf16[128,2048]{1,0:T(8,128)(2,1)}, u32[]{:S(2)}) copy-start(bf16[128,2048]{1,0:T(8,128)(2,1)} %param.17) | copy-start | bytes 1572868
  7.4 21.3 %collective-permute-start = (bf16[30,64]{0,1:T(8,128)(2,1)S(1)}, bf16[30,64]{0,1:T(8,128)(2,1)S(1)}, u32[]{:S(2)}, u32[]{:S(2)}) collective-permute-start(bf16[30,64]{0,1:T(8,128)(2,1)S(1)} %slice.6), channel_id=1, source_target_pairs={{0,16},{16,32},{32,48},{48,64},{64,80},{80,96},{96,112},{112,128},... | collective-permute-start | bytes 11528 | tf_op jit(solution)/shard_map/ppermute | solution.py:224
  13.1 132.0 %copy-start.6 = (f32[2048]{0:T(1024)S(1)}, f32[2048]{0:T(1024)}, u32[]{:S(2)}) copy-start(f32[2048]{0:T(1024)} %param.25) | copy-start | bytes 24580
  13.1 36.2 %all-to-all-start = ((bf16[16,64,128]{2,1,0:T(8,128)(2,1)}), bf16[16,64,128]{2,1,0:T(8,128)(2,1)S(1)}, u32[]{:S(2)}, u32[]{:S(2)}) async-start(bf16[16,64,128]{2,1,0:T(8,128)(2,1)} %bitcast_bitcast_fusion), calls=%async_computation | async-start | bytes 524288 | tf_op jit(solution)/shard_map/all_to_all | solution.py:218
  21.3 98.0 %all-gather.6.cloned.1.call-start = ((), (), s32[]{:S(2)}) async-start(), calls=%async_computation.3 | async-start | bytes 4456448 | tf_op jit(solution)/shard_map/all_gather | solution.py:252
  27.9 117.7 %copy-start.3 = (s32[128,4]{1,0:T(8,128)}, s32[128,4]{1,0:T(8,128)S(1)}, u32[]{:S(2)}) copy-start(s32[128,4]{1,0:T(8,128)S(1)} %add.31.slots) | copy-start | bytes 6148
  27.9 117.5 %copy-start.5 = (bf16[2048,32]{0,1:T(8,128)(2,1)S(1)}, bf16[2048,32]{0,1:T(8,128)(2,1)}, u32[]{:S(2)}) copy-start(bf16[2048,32]{0,1:T(8,128)(2,1)} %param.31) | copy-start | bytes 393220
  49.3 0.7 copy-start.2
  50.0 112.4 %copy-start.4 = (bf16[512,128]{1,0:T(8,128)(2,1)S(1)}, bf16[512,128]{1,0:T(8,128)(2,1)}, u32[]{:S(2)}) copy-start(bf16[512,128]{1,0:T(8,128)(2,1)} %param.33) | copy-start | bytes 393220
  80.0 104.1 %all-gather.8.cloned.1.call-start = ((), (), s32[]{:S(2)}) async-start(), calls=%async_computation.4 | async-start | bytes 8912896 | tf_op jit(solution)/shard_map/all_gather | solution.py:265
  144.5 55.8 %copy-start.7 = (f32[128,4]{0,1:T(4,128)S(1)}, f32[128,4]{0,1:T(4,128)}, u32[]{:S(2)}) copy-start(f32[128,4]{0,1:T(4,128)} %param.27) | copy-start | bytes 6148
  190.4 21.6 %all-to-all-start.2 = ((bf16[32,32,128]{2,1,0:T(8,128)(2,1)}), bf16[32,32,128]{2,1,0:T(8,128)(2,1)S(1)}, u32[]{:S(2)}, u32[]{:S(2)}) async-start(bf16[32,32,128]{2,1,0:T(8,128)(2,1)} %bitcast.58), calls=%async_computation.2 | async-start | bytes 524288 | tf_op jit(solution)/shard_map/all_to_all | solution.py:275
  212.0 0.7 copy-start.1
Sparse Core Ops, SparseCore 0:
  80.1 39.1 all-gather.5
  126.1 57.9 all-gather.7

commit v2 on v1

v2 whole, which is shorter than its diff:
```python
import jax
import jax.numpy as jnp
from jax import lax
from jax.experimental import pallas as pl
from jax.experimental.pallas import tpu as pltpu
from jax.sharding import PartitionSpec as P

LN_EPS = 1e-05
RMS_EPS = 1e-06
LANES = 128
F32 = jnp.float32
BF16 = jnp.bfloat16


def silu(v):
    return v / (1.0 + jnp.exp(-v))


def pack_kernel(before, a_val, a_gate, taps, bias, gain, shift, w_out, out, win, params):
    peers, _, lanes = out.shape
    halo, half = before.shape
    rows = win.shape[0]
    win[...] = jnp.zeros(win.shape, F32)
    params[...] = jnp.zeros(params.shape, F32)
    gate = 1.0 / (1.0 + jnp.exp(-a_gate[...].astype(F32)))
    win[0:halo, :] = before[...].astype(F32)
    win[halo : halo + a_val.shape[0], :] = a_val[...].astype(F32) * gate
    span = taps.shape[0]
    params[0:span, :] = taps[...].astype(F32)
    for n, vector in enumerate((bias, gain, shift)):
        rest = vector[...]
        for part in range(3):
            kept = rest.astype(BF16).astype(F32)
            at = span + 3 * n + part
            params[at : at + 1, :] = kept
            rest = rest - kept

    def folded(v):
        n = v.shape[0] // 2
        return jnp.concatenate([v[0:n, :], v[n : 2 * n, :]], axis=1).astype(BF16)

    head, tail = folded(win[...]), folded(params[...])
    top = rows // 2
    low = top + tail.shape[0]
    for t in range(peers):
        out[t, 0:top, :] = head
        out[t, top:low, :] = tail
        out[t, low : low + w_out.shape[0], :] = w_out[:, t * lanes : (t + 1) * lanes]


PARAM_ROWS = 64


def window_rows(span, tok_rows):
    return -(-(span - 1 + tok_rows) // 32) * 32


def pack(before, a_val, a_gate, taps, bias, gain, shift, w_out, peers):
    rows = window_rows(taps.shape[0], a_val.shape[0])
    lanes = w_out.shape[1] // peers
    total = rows // 2 + PARAM_ROWS // 2 + w_out.shape[0]
    return pl.pallas_call(
        pack_kernel,
        out_shape=jax.ShapeDtypeStruct((peers, total, lanes), BF16),
        scratch_shapes=[
            pltpu.VMEM((rows, a_val.shape[1]), F32),
            pltpu.VMEM((PARAM_ROWS, a_val.shape[1]), F32),
        ],
        name="pack",
    )(before, a_val, a_gate, taps, bias, gain, shift, w_out)


def routing_kernel(capacity, routes, slots_out, pick_out):
    tok_rows, top_count = routes.shape
    experts = pick_out.shape[1] // capacity
    ids = lax.broadcasted_iota(jnp.int32, (tok_rows, experts), 1)
    hits = [ids == routes[:, k : k + 1] for k in range(top_count)]
    named = sum(jnp.where(h, 1.0, 0.0) for h in hits).astype(BF16)
    square = (tok_rows, tok_rows)
    below = lax.broadcasted_iota(jnp.int32, square, 0) > lax.broadcasted_iota(jnp.int32, square, 1)
    earlier = jnp.dot(jnp.where(below, 1.0, 0.0).astype(BF16), named, preferred_element_type=F32)
    wide = lax.broadcasted_iota(jnp.int32, pick_out.shape, 1)
    lane = lax.broadcasted_iota(jnp.int32, slots_out.shape, 1)
    slots = jnp.zeros(slots_out.shape, jnp.int32)
    pick = jnp.zeros(pick_out.shape, F32)
    for k in range(top_count):
        place = jnp.sum(jnp.where(hits[k], earlier, 0.0), axis=1, keepdims=True).astype(jnp.int32)
        slot = routes[:, k : k + 1] * capacity + place
        slots = jnp.where(lane == k, slot, slots)
        pick = jnp.where(wide == slot, 1.0, pick)
    slots_out[...] = slots
    pick_out[...] = pick.astype(BF16)


def routing(routes, capacity, slot_count):
    tok_rows, top_count = routes.shape

    def kernel(*refs):
        routing_kernel(capacity, *refs)

    return pl.pallas_call(
        kernel,
        out_shape=(
            jax.ShapeDtypeStruct((tok_rows, top_count), jnp.int32),
            jax.ShapeDtypeStruct((tok_rows, slot_count), BF16),
        ),
        name="routing",
    )(routes)


def table_kernel(slots, weights, out):
    shape = out.shape[1:]
    ids = lax.broadcasted_iota(jnp.int32, shape, 1)
    table = jnp.zeros(shape, F32)
    for k in range(slots.shape[1]):
        table = jnp.where(ids == slots[:, k : k + 1], weights[:, k : k + 1], table)
    for n in range(out.shape[0]):
        part = table.astype(BF16)
        out[n] = part
        table = table - part.astype(F32)


def weight_table(slots, weights, slot_count):
    return pl.pallas_call(
        table_kernel,
        out_shape=jax.ShapeDtypeStruct((3, slots.shape[0], slot_count), BF16),
        name="table",
    )(slots, weights)


def front_kernel(span, packed, resid, pick, middle_out, send_out, win, params, conv):
    peers = packed.shape[0]
    tok_rows = resid.shape[0]
    half = LANES // 2
    channels = peers * half
    top = win.shape[0] // 2
    fold = PARAM_ROWS // 2
    for pair in range(peers // 2):
        at = slice(pair * LANES, (pair + 1) * LANES)
        one, two = packed[2 * pair, 0 : top + fold, :], packed[2 * pair + 1, 0 : top + fold, :]
        left = jnp.concatenate([one[:, :half], two[:, :half]], axis=1).astype(F32)
        right = jnp.concatenate([one[:, half:], two[:, half:]], axis=1).astype(F32)
        win[0:top, at], win[top : 2 * top, at] = left[0:top], right[0:top]
        params[0:fold, at], params[fold : 2 * fold, at] = left[top:], right[top:]

    def vector(first, cols=slice(None)):
        return sum(params[first + i : first + i + 1, cols] for i in range(3))

    conv_rows = 64

    def one_block(i, _):
        cols = pl.ds(pl.multiple_of(i * LANES, LANES), LANES)
        taps = params[0:span, cols]
        b = vector(span, cols)
        for r in range(0, tok_rows, conv_rows):
            acc = jnp.broadcast_to(b, (conv_rows, LANES))
            for j in range(span):
                acc = acc + taps[j : j + 1, :] * win[r + j : r + j + conv_rows, cols]
            conv[r : r + conv_rows, cols] = acc
        return 0

    lax.fori_loop(0, channels // LANES, one_block, 0)
    gain = vector(span + 3)
    shift = vector(span + 6)
    wcol = packed[:, top + fold :, :].reshape(channels, packed.shape[2])
    for r in range(0, tok_rows, 64):
        c = conv[r : r + 64, :]
        mean = jnp.sum(c, axis=1, keepdims=True) * (1.0 / channels)
        var = jnp.sum(c * c, axis=1, keepdims=True) * (1.0 / channels) - mean * mean
        scaled = (c - mean) * lax.rsqrt(var + LN_EPS) * gain + shift
        mixed = silu(scaled).astype(BF16)
        proj = jnp.dot(mixed, wcol, preferred_element_type=F32)
        middle_out[r : r + 64, :] = (resid[r : r + 64, :].astype(F32) + proj).astype(BF16)
    middle = middle_out[...]
    dims = (((0,), (0,)), ((), ()))
    send_out[...] = lax.dot_general(pick[...], middle, dims, preferred_element_type=F32).astype(BF16)


def front(span, packed, resid, pick):
    tok_rows, cols = resid.shape
    channels = packed.shape[0] * LANES // 2

    def kernel(*refs):
        front_kernel(span, *refs)

    return pl.pallas_call(
        kernel,
        out_shape=(
            jax.ShapeDtypeStruct((tok_rows, cols), BF16),
            jax.ShapeDtypeStruct((pick.shape[1], cols), BF16),
        ),
        scratch_shapes=[
            pltpu.VMEM((window_rows(span, tok_rows), channels), F32),
            pltpu.VMEM((PARAM_ROWS, channels), F32),
            pltpu.VMEM((tok_rows, channels), F32),
        ],
        name="front",
    )(packed, resid, pick)


def hidden_kernel(width, rows_in, gain, wg, wu, out):
    pieces = rows_in.shape[0]
    squares = jnp.zeros((rows_in.shape[1], LANES), F32)
    for t in range(pieces):
        x = rows_in[t].astype(F32)
        squares = squares + x * x
    mean = jnp.sum(squares, axis=1, keepdims=True) / width
    inverse = lax.rsqrt(mean + RMS_EPS)
    normed = jnp.concatenate(
        [(rows_in[t].astype(F32) * inverse * gain[t : t + 1, :]).astype(BF16) for t in range(pieces)],
        axis=1,
    )
    g = jnp.dot(normed, wg[...], preferred_element_type=F32)
    u = jnp.dot(normed, wu[...], preferred_element_type=F32)
    out[...] = (silu(g) * u).astype(BF16)


def hidden_units(rows_in, gain, wg, wu):
    pieces, rows, lanes = rows_in.shape
    width, units = wg.shape
    block = 256

    def kernel(*refs):
        hidden_kernel(width, *refs)

    return pl.pallas_call(
        kernel,
        grid=(rows // block,),
        in_specs=[
            pl.BlockSpec((pieces, block, lanes), lambda i: (0, i, 0)),
            pl.BlockSpec((pieces, lanes), lambda i: (0, 0)),
            pl.BlockSpec((width, units), lambda i: (0, 0)),
            pl.BlockSpec((width, units), lambda i: (0, 0)),
        ],
        out_specs=pl.BlockSpec((block, units), lambda i: (i, 0)),
        out_shape=jax.ShapeDtypeStruct((rows, units), BF16),
        name="hidden",
    )(rows_in, gain, wg, wu)


def down_kernel(hidden, wd, out):
    whole = jnp.concatenate([hidden[t] for t in range(hidden.shape[0])], axis=1)
    out[...] = jnp.dot(whole, wd[...], preferred_element_type=F32).astype(BF16)


def down(hidden, wd):
    pieces, rows, units = hidden.shape
    block = 256
    return pl.pallas_call(
        down_kernel,
        grid=(rows // block,),
        in_specs=[
            pl.BlockSpec((pieces, block, units), lambda i: (0, i, 0)),
            pl.BlockSpec(wd.shape, lambda i: (0, 0)),
        ],
        out_specs=pl.BlockSpec((block, wd.shape[1]), lambda i: (i, 0)),
        out_shape=jax.ShapeDtypeStruct((rows, wd.shape[1]), BF16),
        name="down",
    )(hidden, wd)


def combine_kernel(returned, table, middle, shared, out):
    total = middle[...].astype(F32) + shared[...]
    rows = returned[...]
    for n in range(table.shape[0]):
        total = total + jnp.dot(table[n], rows, preferred_element_type=F32)
    out[...] = total.astype(BF16)


def combine(returned, table, middle, shared):
    return pl.pallas_call(
        combine_kernel,
        out_shape=jax.ShapeDtypeStruct(middle.shape, BF16),
        name="combine",
    )(returned, table, middle, shared)


def body(
    resid,
    a_val,
    a_gate,
    conv_kernel,
    conv_bias,
    ln_gain,
    ln_bias,
    w_out,
    ffn_gain,
    routes,
    route_weights,
    exp_gate,
    exp_up,
    exp_down,
    sh_gate,
    sh_up,
    sh_down,
):
    tp_count = lax.axis_size("tp")
    tp_place = lax.axis_index("tp")
    sp_count = lax.axis_size("sp")
    tok_rows, model_width = resid.shape
    col_width = model_width // tp_count
    span = conv_kernel.shape[0]
    top_count = routes.shape[1]
    experts_all = exp_gate.shape[0] * sp_count
    capacity = max(2 * tok_rows * top_count // experts_all, tp_count)
    slot_count = experts_all * capacity

    halo = span - 1
    late_val, late_gate = a_val[tok_rows - halo :].astype(F32), a_gate[tok_rows - halo :].astype(F32)
    pairs = [(i, i + 1) for i in range(sp_count - 1)]
    before = lax.ppermute((late_val * jax.nn.sigmoid(late_gate)).astype(BF16), "sp", pairs)

    vectors = [v[None, :] for v in (conv_bias, ln_gain, ln_bias)]
    packed = pack(before, a_val, a_gate, conv_kernel, *vectors, w_out, tp_count)
    spread = lax.all_to_all(packed, "tp", split_axis=0, concat_axis=0, tiled=True)

    routes_late, _ = lax.optimization_barrier((routes, packed[0, :1]))
    slots, pick = routing(routes_late, capacity, slot_count)

    resid_cols = lax.dynamic_slice_in_dim(resid, tp_place * col_width, col_width, 1)
    middle, send = front(span, spread, resid_cols, pick)

    landed = lax.all_to_all(
        send.reshape(sp_count, slot_count // sp_count, col_width),
        "sp",
        split_axis=0,
        concat_axis=0,
        tiled=True,
    ).reshape(slot_count, col_width)
    slots_late, weights_late, _ = lax.optimization_barrier((slots, route_weights, middle[:1]))
    table = weight_table(slots_late, weights_late, slot_count)
    landed, table = lax.optimization_barrier((landed, table))
    gain = ffn_gain.reshape(tp_count, col_width)
    arrived = lax.all_gather(landed, "tp")
    hidden = hidden_units(arrived, gain, exp_gate[0], exp_up[0])

    middle_late, landed_late = lax.optimization_barrier((middle, landed[:1]))
    middle_all = lax.all_gather(middle_late, "tp")
    middle_f = jnp.moveaxis(middle_all, 0, 1).reshape(tok_rows, model_width).astype(F32)
    squares = jnp.sum(middle_f * middle_f, axis=1, keepdims=True)
    inverse = lax.rsqrt(squares / model_width + RMS_EPS)
    normed = (middle_f * inverse * ffn_gain[None, :]).astype(BF16)
    shared_gate = jnp.dot(normed, sh_gate, preferred_element_type=F32)
    shared_up = jnp.dot(normed, sh_up, preferred_element_type=F32)
    shared_hidden = (jax.nn.silu(shared_gate) * shared_up).astype(BF16)

    hidden_all = lax.all_gather(hidden, "tp")
    shared_late, _ = lax.optimization_barrier((shared_hidden, hidden[:1]))
    shared_all = lax.all_gather(shared_late, "tp", axis=1, tiled=True)
    hidden_all, shared_all = lax.optimization_barrier((hidden_all, shared_all))

    expert_out = down(hidden_all, exp_down[0])
    returned = lax.all_to_all(
        expert_out.reshape(sp_count, slot_count // sp_count, col_width),
        "sp",
        split_axis=0,
        concat_axis=0,
        tiled=True,
    ).reshape(slot_count, col_width)
    shared_all, _ = lax.optimization_barrier((shared_all, expert_out[:1]))
    shared = jnp.dot(shared_all, sh_down, preferred_element_type=F32)
    return combine(returned, table, middle, shared)


def solution(mesh):
    in_specs = (
        P("sp", None),
        P("sp", "tp"),
        P("sp", "tp"),
        P(None, "tp"),
        P("tp"),
        P("tp"),
        P("tp"),
        P("tp", None),
        P(),
        P("sp", None),
        P("sp", None),
        P("sp", None, "tp"),
        P("sp", None, "tp"),
        P("sp", None, "tp"),
        P(None, "tp"),
        P(None, "tp"),
        P(None, "tp"),
    )
    out_specs = P("sp", "tp")
    return jax.shard_map(body, mesh=mesh, in_specs=in_specs, out_specs=out_specs, check_vma=False)
```

time: 223 us -> 220 us (0.987)
  blocking collectives: 78.9 us -> 34 us
  waiting for transfers between devices: 70.9 us -> 96.5 us
  starting transfers between devices: 22.1 us -> 37.3 us
  Pallas kernels: 20.9 us -> 27.3 us
  other arithmetic: 4.22 us -> 0.65 us
    all_to_all x1 -> x2, waiting for transfers between devices: 0.01 us -> 25.3 us  [the longest x1 17 us: body(): lax.all_to_all(packed, 'tp', split_axis=0, concat_axis=0, tiled=True)]
    all_to_all x1 -> x0, blocking collectives: 24.3 us -> none  [body(): lax.all_to_all(send.reshape(sp_count, slot_count // sp_count, col_width),...]
    all_gather x2 -> x1, blocking collectives: 36.1 us -> 15.6 us  [body(): shared_all = lax.all_gather(shared_late, 'tp', axis=1, tiled=True)]
    all_to_all x1 -> x2, starting transfers between devices: 8.2 us -> 23.4 us  [the longest x1 14.6 us: body(): lax.all_to_all(send.reshape(sp_count, slot_count // sp_count, col_width),...]
    pallas_call x0 -> x3, Pallas kernels: none -> 6.65 us  [the longest x1 2.36 us: weight_table(): pl.pallas_call(table_kernel, out_shape=jax.ShapeDtypeStruct((3, slots.sha...]
    optimization_barrier x0 -> x2, local copies, waits for them, and re-layouts: none -> 2.86 us  [the longest x1 1.45 us: body(): routes_late, _ = lax.optimization_barrier((routes, packed[0, :1]))]
    all_gather x1, waiting for transfers between devices: 39.2 us -> 36.8 us  [body(): arrived = lax.all_gather(landed, 'tp')]
    transpose x2 -> x0, local copies, waits for them, and re-layouts: 2.37 us -> none  [the longest x1 1.71 us: body(): jnp.moveaxis(w_out.reshape(w_out.shape[0], tp_count, col_width), 1, 0)]
  transfers between devices with their start and end apart: 5 -> 6, of which waited for: 3 -> 6; matrix products, arithmetic and copies ran while one was open for 6% -> 3% of each run, Pallas kernels for 0% -> 2%
where the time goes in v2:
time: 220 us; the launch traced here: 219 us
  waiting for transfers between devices  96.5 us (44%)
  starting transfers between devices  37.3 us (17%)
  blocking collectives  34 us (15%)
  Pallas kernels  27.3 us (12%)
  between operations  13.6 us (6%)
  local copies, waits for them, and re-layouts  8.45 us (4%)
    all_gather x1, waiting for transfers between devices, body(): arrived = lax.all_gather(landed, 'tp')  36.8 us
    all_gather x1, waiting for transfers between devices, body(): hidden_all = lax.all_gather(hidden, 'tp')  22.7 us
    all_gather x1, blocking collectives, body(): middle_all = lax.all_gather(middle_late, 'tp')  18.4 us
    all_to_all x1, waiting for transfers between devices, body(): lax.all_to_all(packed, 'tp', split_axis=0, concat_axis=0, tiled=True)  17 us
    all_gather x1, blocking collectives, body(): shared_all = lax.all_gather(shared_late, 'tp', axis=1, tiled=True)  15.6 us
    all_to_all x1, starting transfers between devices, body(): lax.all_to_all(send.reshape(sp_count, slot_count // sp_count, col_width),...  14.6 us
    all_to_all x1, waiting for transfers between devices, body(): lax.all_to_all(expert_out.reshape(sp_count, slot_count // sp_count, col_w...  10.8 us
    all_to_all x1, starting transfers between devices, body(): lax.all_to_all(expert_out.reshape(sp_count, slot_count // sp_count, col_w...  9.9 us
  transfers between devices with their start and end apart: 6, of which 6 were waited for; matrix products, arithmetic and copies ran while one was open for 3% of the time, Pallas kernels for 2%

profile of v2, /device:TPU:1, one launch (start us, length us, event | category | flops | bytes accessed | tf_op | source)
XLA Modules:
  0.0 219.0 jit_solution(3912464500542240573)
XLA Ops:
  6.5 0.0 copy-start
  6.5 0.9 copy.24.a_val
  7.4 0.0 copy-start.4
  7.4 0.8 copy.25.a_gate
  8.3 0.0 copy-start.5
  8.3 3.9 %collective-permute-start = (bf16[30,64]{1,0:T(8,128)(2,1)S(1)}, bf16[30,64]{1,0:T(8,128)(2,1)S(1)}, u32[]{:S(2)}, u32[]{:S(2)}) collective-permute-start(bf16[30,64]{1,0:T(8,128)(2,1)S(1)} %multiply_convert_fusion), channel_id=1, source_target_pairs={{0,16},{16,32},{32,48},{48,64},{64,80},{80,96},{96,112},{112,128},... | collective-permute-start | bytes 11528 | tf_op jit(solution)/shard_map/ppermute | solution.py:311
  12.2 0.8 collective-permute-done.before
  13.0 0.0 copy-done.4
  13.0 0.0 copy-done.5
  13.0 0.6 copy-done.11
  13.6 2.1 pack.1
  15.7 8.8 %all-to-all-start = ((bf16[16,176,128]{2,1,0:T(8,128)(2,1)}), bf16[16,176,128]{2,1,0:T(8,128)(2,1)S(1)}, u32[]{:S(2)}, u32[]{:S(2)}) async-start(bf16[16,176,128]{2,1,0:T(8,128)(2,1)} %pack.1), calls=%async_computation | async-start | bytes 1441792 | tf_op jit(solution)/shard_map/all_to_all | solution.py:315
  24.5 1.4 copy.28.refs_0_
  25.9 2.2 %routing.1 = (s32[128,4]{1,0:T(8,128)}, bf16[128,1024]{1,0:T(8,128)(2,1)}) custom-call(s32[128,4]{1,0:T(8,128)} %copy.28.refs_0_), custom_call_target="tpu_custom_call" | custom-call | tf_op jit(solution)/shard_map/routing/pallas_call | solution.py:101
  28.1 0.0 copy-done
  28.2 0.6 constant_dynamic-slice_fusion.refs_1_
  28.8 17.0 %all-to-all-done.refs_0_ = bf16[16,176,128]{2,1,0:T(8,128)(2,1)S(1)} async-done(((bf16[16,176,128]{2,1,0:T(8,128)(2,1)}), bf16[16,176,128]{2,1,0:T(8,128)(2,1)S(1)}, u32[]{:S(2)}, u32[]{:S(2)}) %all-to-all-start) | async-done | bytes 720928 | tf_op jit(solution)/shard_map/all_to_all | solution.py:315
  45.8 0.9 copy-done.1
  46.7 5.4 %front.1 = (bf16[128,128]{1,0:T(8,128)(2,1)}, bf16[1024,128]{1,0:T(8,128)(2,1)}) custom-call(bf16[16,176,128]{2,1,0:T(8,128)(2,1)} %copy-done.1, bf16[128,128]{1,0:T(8,128)(2,1)} %constant_dynamic-slice_fusion.refs_1_, bf16[128,1024]{1,0:T(8,128)(2,1)} %get-tuple-element.15.refs_2_), custom_call_target="tpu_custom_call" | custom-call | tf_op jit(solution)/shard_map/front/pallas_call | solution.py:186
  52.1 14.6 %all-to-all-start.1 = ((bf16[32,32,128]{2,1,0:T(8,128)(2,1)}), bf16[32,32,128]{2,1,0:T(8,128)(2,1)S(1)}, u32[]{:S(2)}, u32[]{:S(2)}) async-start(bf16[32,32,128]{2,1,0:T(8,128)(2,1)} %bitcast.39), calls=%async_computation.1 | async-start | bytes 524288 | tf_op jit(solution)/shard_map/all_to_all | solution.py:323
  66.7 0.0 all-gather.6.cloned.1.call-start
  66.8 1.4 copy.29.weights
  68.2 2.4 %table.1 = bf16[3,128,1024]{2,1,0:T(8,128)(2,1)} custom-call(s32[128,4]{1,0:T(8,128)} %get-tuple-element.18.slots, f32[128,4]{1,0:T(8,128)} %copy.29.weights), custom_call_target="tpu_custom_call" | custom-call | tf_op jit(solution)/shard_map/table/pallas_call | solution.py:124
  70.5 8.3 %all-to-all-done.1 = bf16[32,32,128]{2,1,0:T(8,128)(2,1)S(1)} async-done(((bf16[32,32,128]{2,1,0:T(8,128)(2,1)}), bf16[32,32,128]{2,1,0:T(8,128)(2,1)S(1)}, u32[]{:S(2)}, u32[]{:S(2)}) %all-to-all-start.1) | async-done | bytes 262176 | tf_op jit(solution)/shard_map/all_to_all | solution.py:323
  78.8 0.7 copy-done.2
  79.6 0.0 all-gather.6.cloned.1.call-update
  79.6 0.0 all-gather.8.cloned.1.call-start
  79.6 36.8 %all-gather.6.cloned.1.call-done = bf16[16384,128]{1,0:T(8,128)(2,1)} async-done(((bf16[1024,128]{1,0:T(8,128)(2,1)}), bf16[16384,128]{1,0:T(8,128)(2,1)}) %all-gather.6.cloned.1.call-update) | async-done | bytes 4194320 | tf_op jit(solution)/shard_map/all_gather | solution.py:334
  116.5 6.7 %hidden.1 = bf16[1024,256]{1,0:T(8,128)(2,1)} custom-call(bf16[16,1024,128]{2,1,0:T(8,128)(2,1)} %bitcast.32, f32[16,128]{1,0:T(8,128)} %bitcast.40, bf16[2048,256]{1,0:T(8,128)(2,1)} %bitcast.37, bf16[2048,256]{1,0:T(8,128)(2,1)} %bitcast.38), custom_call_target="tpu_custom_call" | custom-call | tf_op jit(solution)/shard_map/hidden/pallas_call | solution.py:226
  123.2 0.0 all-gather.8.cloned.1.call-update
  123.2 0.0 copy-done.6
  123.2 18.4 %all-gather.2 = bf16[2048,128]{1,0:T(8,128)(2,1)S(1)} all-gather(bf16[128,128]{1,0:T(8,128)(2,1)S(1)} %copy-done.6), channel_id=4, replica_groups=mesh['sp'=32,'tp'=16] {'tp'}, dimensions={0}, use_global_device_ids=true | all-gather | bytes 557056 | tf_op jit(solution)/shard_map/all_gather | solution.py:338
  141.6 0.1 bitcast_convert_fusion
  141.7 0.3 copy.30
  142.0 0.2 multiply_reduce_fusion
  142.2 0.0 copy-done.10
  142.2 0.3 fusion.2
  142.6 0.2 fusion.4
  142.8 0.0 copy-done.9
  142.8 0.2 fusion
  143.0 15.6 %all_gather.27 = bf16[128,512]{0,1:T(8,128)(2,1)S(1)} all-gather(bf16[128,32]{0,1:T(8,128)(2,1)S(1)} %fusion), channel_id=1, replica_groups=mesh['sp'=32,'tp'=16] {'tp'}, dimensions={1}, use_global_device_ids=true | all-gather | bytes 139264 | tf_op jit(solution)/shard_map/all_gather | solution.py:349
  158.6 22.7 %all-gather.8.cloned.1.call-done = bf16[16384,256]{1,0:T(8,128)(2,1)} async-done(((bf16[1024,256]{1,0:T(8,128)(2,1)}), bf16[16384,256]{1,0:T(8,128)(2,1)}) %all-gather.8.cloned.1.call-update) | async-done | bytes 8388624 | tf_op jit(solution)/shard_map/all_gather | solution.py:347
  181.3 6.4 %down.1 = bf16[1024,128]{1,0:T(8,128)(2,1)} custom-call(bf16[16,1024,256]{2,1,0:T(8,128)(2,1)} %bitcast.30, bf16[4096,128]{1,0:T(8,128)(2,1)} %bitcast.33), custom_call_target="tpu_custom_call" | custom-call | tf_op jit(solution)/shard_map/down/pallas_call | solution.py:249
  187.7 9.9 %all-to-all-start.2 = ((bf16[32,32,128]{2,1,0:T(8,128)(2,1)}), bf16[32,32,128]{2,1,0:T(8,128)(2,1)S(1)}, u32[]{:S(2)}, u32[]{:S(2)}) async-start(bf16[32,32,128]{2,1,0:T(8,128)(2,1)} %bitcast.34), calls=%async_computation.2 | async-start | bytes 524288 | tf_op jit(solution)/shard_map/all_to_all | solution.py:353
  197.6 0.8 fusion.3.shared
  198.5 10.8 %all-to-all-done.2 = bf16[32,32,128]{2,1,0:T(8,128)(2,1)S(1)} async-done(((bf16[32,32,128]{2,1,0:T(8,128)(2,1)}), bf16[32,32,128]{2,1,0:T(8,128)(2,1)S(1)}, u32[]{:S(2)}, u32[]{:S(2)}) %all-to-all-start.2) | async-done | bytes 262176 | tf_op jit(solution)/shard_map/all_to_all | solution.py:353
  209.3 0.7 copy-done.3
  210.0 2.2 combine.1
  (13 shorter events, 0.0 us)
Async XLA Ops:
  6.5 21.6 %copy-start = (bf16[128,2048]{1,0:T(8,128)(2,1)S(1)}, bf16[128,2048]{1,0:T(8,128)(2,1)}, u32[]{:S(2)}) copy-start(bf16[128,2048]{1,0:T(8,128)(2,1)} %param.17) | copy-start | bytes 1572868
  7.4 5.6 %copy-start.4 = (bf16[128,64]{1,0:T(8,128)(2,1)}, bf16[128,64]{1,0:T(8,128)(2,1)S(1)}, u32[]{:S(2)}) copy-start(bf16[128,64]{1,0:T(8,128)(2,1)S(1)} %copy.24.a_val) | copy-start | bytes 49156
  8.3 4.8 %copy-start.5 = (bf16[128,64]{1,0:T(8,128)(2,1)}, bf16[128,64]{1,0:T(8,128)(2,1)S(1)}, u32[]{:S(2)}) copy-start(bf16[128,64]{1,0:T(8,128)(2,1)S(1)} %copy.25.a_gate) | copy-start | bytes 49156
  8.3 4.7 %collective-permute-start = (bf16[30,64]{1,0:T(8,128)(2,1)S(1)}, bf16[30,64]{1,0:T(8,128)(2,1)S(1)}, u32[]{:S(2)}, u32[]{:S(2)}) collective-permute-start(bf16[30,64]{1,0:T(8,128)(2,1)S(1)} %multiply_convert_fusion), channel_id=1, source_target_pairs={{0,16},{16,32},{32,48},{48,64},{64,80},{80,96},{96,112},{112,128},... | collective-permute-start | bytes 11528 | tf_op jit(solution)/shard_map/ppermute | solution.py:311
  13.0 0.6 copy-start.11
  15.7 126.5 %copy-start.10 = (f32[2048]{0:T(1024)S(1)}, f32[2048]{0:T(1024)}, u32[]{:S(2)}) copy-start(f32[2048]{0:T(1024)} %param.25) | copy-start | bytes 24580
  15.7 30.1 %all-to-all-start = ((bf16[16,176,128]{2,1,0:T(8,128)(2,1)}), bf16[16,176,128]{2,1,0:T(8,128)(2,1)S(1)}, u32[]{:S(2)}, u32[]{:S(2)}) async-start(bf16[16,176,128]{2,1,0:T(8,128)(2,1)} %pack.1), calls=%async_computation | async-start | bytes 1441792 | tf_op jit(solution)/shard_map/all_to_all | solution.py:315
  24.5 118.1 %copy-start.8 = (bf16[2048,32]{0,1:T(8,128)(2,1)S(1)}, bf16[2048,32]{0,1:T(8,128)(2,1)}, u32[]{:S(2)}) copy-start(bf16[2048,32]{0,1:T(8,128)(2,1)} %param.31) | copy-start | bytes 393220
  45.8 0.9 copy-start.1
  46.7 96.1 %copy-start.9 = (bf16[2048,32]{0,1:T(8,128)(2,1)S(1)}, bf16[2048,32]{0,1:T(8,128)(2,1)}, u32[]{:S(2)}) copy-start(bf16[2048,32]{0,1:T(8,128)(2,1)} %param.32) | copy-start | bytes 393220
  52.1 71.1 %copy-start.6 = (bf16[128,128]{1,0:T(8,128)(2,1)S(1)}, bf16[128,128]{1,0:T(8,128)(2,1)}, u32[]{:S(2)}) copy-start(bf16[128,128]{1,0:T(8,128)(2,1)} %get-tuple-element.21.middle) | copy-start | bytes 98308
  52.1 26.8 %all-to-all-start.1 = ((bf16[32,32,128]{2,1,0:T(8,128)(2,1)}), bf16[32,32,128]{2,1,0:T(8,128)(2,1)S(1)}, u32[]{:S(2)}, u32[]{:S(2)}) async-start(bf16[32,32,128]{2,1,0:T(8,128)(2,1)} %bitcast.39), calls=%async_computation.1 | async-start | bytes 524288 | tf_op jit(solution)/shard_map/all_to_all | solution.py:323
  66.7 49.8 %all-gather.6.cloned.1.call-start = ((), (), s32[]{:S(2)}) async-start(), calls=%async_computation.3 | async-start | bytes 4456448 | tf_op jit(solution)/shard_map/all_gather | solution.py:334
  78.8 0.7 copy-start.2
  79.6 101.7 %all-gather.8.cloned.1.call-start = ((), (), s32[]{:S(2)}) async-start(), calls=%async_computation.4 | async-start | bytes 8912896 | tf_op jit(solution)/shard_map/all_gather | solution.py:347
  141.6 56.0 %copy-start.7 = (bf16[512,128]{1,0:T(8,128)(2,1)S(1)}, bf16[512,128]{1,0:T(8,128)(2,1)}, u32[]{:S(2)}) copy-start(bf16[512,128]{1,0:T(8,128)(2,1)} %param.33) | copy-start | bytes 393220
  187.7 21.6 %all-to-all-start.2 = ((bf16[32,32,128]{2,1,0:T(8,128)(2,1)}), bf16[32,32,128]{2,1,0:T(8,128)(2,1)S(1)}, u32[]{:S(2)}, u32[]{:S(2)}) async-start(bf16[32,32,128]{2,1,0:T(8,128)(2,1)} %bitcast.34), calls=%async_computation.2 | async-start | bytes 524288 | tf_op jit(solution)/shard_map/all_to_all | solution.py:353
  209.3 0.7 copy-start.3
Sparse Core Ops, SparseCore 0:
  79.7 36.7 all-gather.5
  123.3 57.9 all-gather.7

commit v3 on v2

--- a/solution.py
+++ b/solution.py
@@ -49,6 +49,8 @@
 
 
 PARAM_ROWS = 64
+FOLDED = 16
+ASIDE = (96, 112)
 
 
 def window_rows(span, tok_rows):
@@ -198,37 +200,38 @@
     )(packed, resid, pick)
 
 
-def hidden_kernel(width, rows_in, gain, wg, wu, out):
-    pieces = rows_in.shape[0]
-    squares = jnp.zeros((rows_in.shape[1], LANES), F32)
-    for t in range(pieces):
-        x = rows_in[t].astype(F32)
-        squares = squares + x * x
+def normed_rows(pieces, width, gain):
+    squares = jnp.zeros(pieces[0].shape, F32)
+    for x in pieces:
+        squares = squares + x.astype(F32) * x.astype(F32)
     mean = jnp.sum(squares, axis=1, keepdims=True) / width
     inverse = lax.rsqrt(mean + RMS_EPS)
-    normed = jnp.concatenate(
-        [(rows_in[t].astype(F32) * inverse * gain[t : t + 1, :]).astype(BF16) for t in range(pieces)],
-        axis=1,
-    )
-    g = jnp.dot(normed, wg[...], preferred_element_type=F32)
-    u = jnp.dot(normed, wu[...], preferred_element_type=F32)
-    out[...] = (silu(g) * u).astype(BF16)
-
-
-def hidden_units(rows_in, gain, wg, wu):
+    cols = [gain[:, n * LANES : (n + 1) * LANES] for n in range(len(pieces))]
+    scaled = [(x.astype(F32) * inverse * c).astype(BF16) for x, c in zip(pieces, cols)]
+    return jnp.concatenate(scaled, axis=1)
+
+
+def gated_units(rows, w_gate, w_up):
+    g = jnp.dot(rows, w_gate, preferred_element_type=F32)
+    u = jnp.dot(rows, w_up, preferred_element_type=F32)
+    return (silu(g) * u).astype(BF16)
+
+
+def hidden_kernel(rows_in, gain, wg, wu, out):
+    rows = normed_rows([rows_in[t] for t in range(rows_in.shape[0])], wg.shape[0], gain)
+    out[...] = gated_units(rows, wg[...], wu[...])
+
+
+def hidden_units(rows_in, gain, wg, wu, blocks):
     pieces, rows, lanes = rows_in.shape
     width, units = wg.shape
-    block = 256
-
-    def kernel(*refs):
-        hidden_kernel(width, *refs)
-
-    return pl.pallas_call(
-        kernel,
-        grid=(rows // block,),
+    block = rows // blocks
+    return pl.pallas_call(
+        hidden_kernel,
+        grid=(blocks,),
         in_specs=[
             pl.BlockSpec((pieces, block, lanes), lambda i: (0, i, 0)),
-            pl.BlockSpec((pieces, lanes), lambda i: (0, 0)),
+            pl.BlockSpec((1, width), lambda i: (0, 0)),
             pl.BlockSpec((width, units), lambda i: (0, 0)),
             pl.BlockSpec((width, units), lambda i: (0, 0)),
         ],
@@ -238,25 +241,94 @@
     )(rows_in, gain, wg, wu)
 
 
-def down_kernel(hidden, wd, out):
+def side_hidden_kernel(one, two, gain, wg, wu, sg, su, one_out, two_out):
+    width, units = wg.shape
+    few = sg.shape[1]
+    slots = one_out.shape[0] - FOLDED
+    rows = normed_rows([one[t] for t in range(one.shape[0])], width, gain)
+    one_out[0:slots, :] = gated_units(rows[0:slots, :], wg[...], wu[...])
+    shared = gated_units(rows[slots:, :], sg[...], su[...])
+    parts = [shared[j * FOLDED : (j + 1) * FOLDED, :].astype(F32) for j in range(units // few)]
+    one_out[slots:, :] = jnp.concatenate(parts, axis=1).astype(BF16)
+    rows = normed_rows([two[t] for t in range(two.shape[0])], width, gain)
+    two_out[...] = gated_units(rows, wg[...], wu[...])
+
+
+def side_hidden(one, two, gain, wg, wu, sg, su, tok_rows):
+    units = wg.shape[1]
+    slots = one.shape[1] - tok_rows
+    return pl.pallas_call(
+        side_hidden_kernel,
+        out_shape=(
+            jax.ShapeDtypeStruct((slots + FOLDED, units), BF16),
+            jax.ShapeDtypeStruct((two.shape[1], units), BF16),
+        ),
+        name="side_hidden",
+    )(one, two, gain, wg, wu, sg, su)
+
+
+def side_down_kernel(one, two, wd, sh_down, out, shared_out):
+    peers, rows, units = one.shape
+    slots = rows - FOLDED
+    few = sh_down.shape[0] // peers
+    folds = units // few
+    whole = jnp.concatenate([one[t, 0:slots, :] for t in range(peers)], axis=1)
+    out[0:slots, :] = jnp.dot(whole, wd[...], preferred_element_type=F32).astype(BF16)
+    whole = jnp.concatenate([two[t] for t in range(peers)], axis=1)
+    out[slots:, :] = jnp.dot(whole, wd[...], preferred_element_type=F32).astype(BF16)
+    shape = (folds * FOLDED, units)
+    own = lax.broadcasted_iota(jnp.int32, shape, 0) // FOLDED == lax.broadcasted_iota(jnp.int32, shape, 1) // few
+    shared = jnp.zeros(shared_out.shape, F32)
+    for t in range(peers):
+        packed = one[t, slots:, :].astype(F32)
+        spread = jnp.where(own, jnp.concatenate([packed] * folds, axis=0), 0.0).astype(BF16)
+        weights = jnp.concatenate([sh_down[t * few : (t + 1) * few, :]] * folds, axis=0)
+        shared = shared + jnp.dot(spread, weights, preferred_element_type=F32)
+    shared_out[...] = shared
+
+
+def side_down(one, two, wd, sh_down, tok_rows):
+    slots = one.shape[1] - FOLDED + two.shape[1]
+    return pl.pallas_call(
+        side_down_kernel,
+        out_shape=(
+            jax.ShapeDtypeStruct((slots, wd.shape[1]), BF16),
+            jax.ShapeDtypeStruct((tok_rows, wd.shape[1]), F32),
+        ),
+        name="side_down",
+    )(one, two, wd, sh_down)
+
+
+def down_kernel(hidden, wd, aside, out):
+    slots = aside.shape[0]
+    block = hidden.shape[1]
+    step = pl.program_id(0)
+
+    @pl.when(step == 0)
+    def _():
+        out[0:slots, :] = aside[...]
+
     whole = jnp.concatenate([hidden[t] for t in range(hidden.shape[0])], axis=1)
-    out[...] = jnp.dot(whole, wd[...], preferred_element_type=F32).astype(BF16)
-
-
-def down(hidden, wd):
+    at = pl.ds(pl.multiple_of(slots + step * block, 16), block)
+    out[at, :] = jnp.dot(whole, wd[...], preferred_element_type=F32).astype(BF16)
+
+
+def down(hidden, wd, aside, blocks):
     pieces, rows, units = hidden.shape
-    block = 256
+    block = rows // blocks
+    total = (aside.shape[0] + rows, wd.shape[1])
     return pl.pallas_call(
         down_kernel,
-        grid=(rows // block,),
+        grid=(blocks,),
         in_specs=[
             pl.BlockSpec((pieces, block, units), lambda i: (0, i, 0)),
             pl.BlockSpec(wd.shape, lambda i: (0, 0)),
+            pl.BlockSpec(aside.shape, lambda i: (0, 0)),
         ],
-        out_specs=pl.BlockSpec((block, wd.shape[1]), lambda i: (i, 0)),
-        out_shape=jax.ShapeDtypeStruct((rows, wd.shape[1]), BF16),
+        out_specs=pl.BlockSpec(total, lambda i: (0, 0)),
+        out_shape=jax.ShapeDtypeStruct(total, BF16),
         name="down",
-    )(hidden, wd)
+    )(hidden, wd, aside)
 
 
 def combine_kernel(returned, table, middle, shared, out):
@@ -330,26 +402,23 @@
     slots_late, weights_late, _ = lax.optimization_barrier((slots, route_weights, middle[:1]))
     table = weight_table(slots_late, weights_late, slot_count)
     landed, table = lax.optimization_barrier((landed, table))
-    gain = ffn_gain.reshape(tp_count, col_width)
-    arrived = lax.all_gather(landed, "tp")
-    hidden = hidden_units(arrived, gain, exp_gate[0], exp_up[0])
-
-    middle_late, landed_late = lax.optimization_barrier((middle, landed[:1]))
-    middle_all = lax.all_gather(middle_late, "tp")
-    middle_f = jnp.moveaxis(middle_all, 0, 1).reshape(tok_rows, model_width).astype(F32)
-    squares = jnp.sum(middle_f * middle_f, axis=1, keepdims=True)
-    inverse = lax.rsqrt(squares / model_width + RMS_EPS)
-    normed = (middle_f * inverse * ffn_gain[None, :]).astype(BF16)
-    shared_gate = jnp.dot(normed, sh_gate, preferred_element_type=F32)
-    shared_up = jnp.dot(normed, sh_up, preferred_element_type=F32)
-    shared_hidden = (jax.nn.silu(shared_gate) * shared_up).astype(BF16)
+    first, aside = ASIDE[0], sum(ASIDE)
+    gain = ffn_gain[None, :]
+    experts = (gain, exp_gate[0], exp_up[0])
+    arrived = lax.all_gather(landed[aside:], "tp")
+    one = lax.all_gather(jnp.concatenate([landed[:first], middle], axis=0), "tp")
+    two = lax.all_gather(landed[first:aside], "tp")
+    one, two = side_hidden(one, two, *experts, sh_gate, sh_up, tok_rows)
+    arrived, one, two = lax.optimization_barrier((arrived, one, two))
+    hidden = hidden_units(arrived, *experts, 3)
 
     hidden_all = lax.all_gather(hidden, "tp")
-    shared_late, _ = lax.optimization_barrier((shared_hidden, hidden[:1]))
-    shared_all = lax.all_gather(shared_late, "tp", axis=1, tiled=True)
-    hidden_all, shared_all = lax.optimization_barrier((hidden_all, shared_all))
-
-    expert_out = down(hidden_all, exp_down[0])
+    one, two, _ = lax.optimization_barrier((one, two, hidden[:1]))
+    side_out, shared = side_down(
+        lax.all_gather(one, "tp"), lax.all_gather(two, "tp"), exp_down[0], sh_down, tok_rows
+    )
+    hidden_all, side_out = lax.optimization_barrier((hidden_all, side_out))
+    expert_out = down(hidden_all, exp_down[0], side_out, 3)
     returned = lax.all_to_all(
         expert_out.reshape(sp_count, slot_count // sp_count, col_width),
         "sp",
@@ -357,8 +426,6 @@
         concat_axis=0,
         tiled=True,
     ).reshape(slot_count, col_width)
-    shared_all, _ = lax.optimization_barrier((shared_all, expert_out[:1]))
-    shared = jnp.dot(shared_all, sh_down, preferred_element_type=F32)
     return combine(returned, table, middle, shared)
 
 

time: 220 us -> 220 us (level)
  blocking collectives: 34 us -> 107 us
  waiting for transfers between devices: 96.5 us -> 27.3 us
  starting transfers between devices: 37.3 us -> 27.2 us
  Pallas kernels: 27.3 us -> 33.1 us
    all_gather x2 -> x4, blocking collectives: 34 us -> 86.9 us  [the longest x1 25.7 us: body(): lax.all_gather(two, 'tp')]
    all_gather x1, waiting for transfers between devices: 36.8 us -> 0.01 us  [body(): arrived = lax.all_gather(landed[aside:], 'tp')]
    all_gather x1, waiting for transfers between devices: 22.7 us -> 1.14 us  [body(): hidden_all = lax.all_gather(hidden, 'tp')]
    all_to_all x0 -> x1, blocking collectives: none -> 20.3 us  [body(): lax.all_to_all(expert_out.reshape(sp_count, slot_count // sp_count, col_w...]
    all_to_all x1 -> x0, waiting for transfers between devices: 10.8 us -> none  [body(): lax.all_to_all(expert_out.reshape(sp_count, slot_count // sp_count, col_w...]
    all_to_all x1 -> x0, starting transfers between devices: 9.9 us -> none  [body(): lax.all_to_all(expert_out.reshape(sp_count, slot_count // sp_count, col_w...]
    pallas_call x2 -> x4, Pallas kernels: 13.1 us -> 18.9 us  [the longest x1 5.84 us: hidden_units(): pl.pallas_call(hidden_kernel, grid=(blocks,), in_specs=[pl.BlockSpec((pie...]
    unnamed x26 -> x18, local copies, waits for them, and re-layouts: 4.64 us -> 6.16 us
  transfers between devices with their start and end apart: 6 -> 5, of which waited for: 6 -> 4; matrix products, arithmetic and copies ran while one was open for 3% -> 3% of each run, Pallas kernels for 2% -> 5%
where the time goes in v3:
time: 220 us; the launch traced here: 219 us
  blocking collectives  107 us (49%)
  Pallas kernels  33.1 us (15%)
  waiting for transfers between devices  27.3 us (12%)
  starting transfers between devices  27.2 us (12%)
  between operations  13.5 us (6%)
  local copies, waits for them, and re-layouts  10.3 us (5%)
    all_gather x1, blocking collectives, body(): lax.all_gather(two, 'tp')  25.7 us
    all_gather x1, blocking collectives, body(): lax.all_gather(one, 'tp')  21.9 us
    all_gather x1, blocking collectives, body(): lax.all_gather(jnp.concatenate([landed[:first], middle], axis=0), 'tp')  20.6 us
    all_to_all x1, blocking collectives, body(): lax.all_to_all(expert_out.reshape(sp_count, slot_count // sp_count, col_w...  20.3 us
    all_gather x1, blocking collectives, body(): two = lax.all_gather(landed[first:aside], 'tp')  18.7 us
    all_to_all x1, waiting for transfers between devices, body(): lax.all_to_all(packed, 'tp', split_axis=0, concat_axis=0, tiled=True)  17.1 us
    all_to_all x1, starting transfers between devices, body(): lax.all_to_all(send.reshape(sp_count, slot_count // sp_count, col_width),...  14.5 us
    all_to_all x1, starting transfers between devices, body(): lax.all_to_all(packed, 'tp', split_axis=0, concat_axis=0, tiled=True)  8.64 us
  transfers between devices with their start and end apart: 5, of which 4 were waited for; matrix products, arithmetic and copies ran while one was open for 3% of the time, Pallas kernels for 5%

profile of v3, /device:TPU:1, one launch (start us, length us, event | category | flops | bytes accessed | tf_op | source)
XLA Modules:
  0.0 219.4 jit_solution(10529634868633127272)
XLA Ops:
  6.5 0.0 copy-start
  6.5 0.0 copy-start.4
  6.5 0.9 copy.18.a_val
  7.4 0.0 copy-start.2
  7.4 0.8 copy.19.a_gate
  8.3 0.0 copy-start.3
  8.3 3.9 %collective-permute-start = (bf16[30,64]{1,0:T(8,128)(2,1)S(1)}, bf16[30,64]{1,0:T(8,128)(2,1)S(1)}, u32[]{:S(2)}, u32[]{:S(2)}) collective-permute-start(bf16[30,64]{1,0:T(8,128)(2,1)S(1)} %multiply_convert_fusion), channel_id=1, source_target_pairs={{0,16},{16,32},{32,48},{48,64},{64,80},{80,96},{96,112},{112,128},... | collective-permute-start | bytes 11528 | tf_op jit(solution)/shard_map/ppermute | solution.py:383
  12.3 0.8 collective-permute-done.before
  13.0 0.0 copy-start.6
  13.0 0.0 copy-done.2
  13.0 0.0 copy-done.3
  13.0 0.6 copy-done.6
  13.6 2.1 pack.1
  15.7 8.6 %all-to-all-start = ((bf16[16,176,128]{2,1,0:T(8,128)(2,1)}), bf16[16,176,128]{2,1,0:T(8,128)(2,1)S(1)}, u32[]{:S(2)}, u32[]{:S(2)}) async-start(bf16[16,176,128]{2,1,0:T(8,128)(2,1)} %pack.1), calls=%async_computation | async-start | bytes 1441792 | tf_op jit(solution)/shard_map/all_to_all | solution.py:387
  24.4 1.4 copy.22.refs_0_
  25.8 2.2 %routing.1 = (s32[128,4]{1,0:T(8,128)}, bf16[128,1024]{1,0:T(8,128)(2,1)}) custom-call(s32[128,4]{1,0:T(8,128)} %copy.22.refs_0_), custom_call_target="tpu_custom_call" | custom-call | tf_op jit(solution)/shard_map/routing/pallas_call | solution.py:103
  28.0 0.0 copy-done
  28.0 0.6 constant_dynamic-slice_fusion.refs_1_
  28.6 17.1 %all-to-all-done.refs_0_ = bf16[16,176,128]{2,1,0:T(8,128)(2,1)S(1)} async-done(((bf16[16,176,128]{2,1,0:T(8,128)(2,1)}), bf16[16,176,128]{2,1,0:T(8,128)(2,1)S(1)}, u32[]{:S(2)}, u32[]{:S(2)}) %all-to-all-start) | async-done | bytes 720928 | tf_op jit(solution)/shard_map/all_to_all | solution.py:387
  45.7 0.0 copy-start.1
  45.7 0.9 copy-done.1
  46.6 5.4 %front.1 = (bf16[128,128]{1,0:T(8,128)(2,1)}, bf16[1024,128]{1,0:T(8,128)(2,1)}) custom-call(bf16[16,176,128]{2,1,0:T(8,128)(2,1)} %copy-done.1, bf16[128,128]{1,0:T(8,128)(2,1)} %constant_dynamic-slice_fusion.refs_1_, bf16[128,1024]{1,0:T(8,128)(2,1)} %get-tuple-element.24.refs_2_), custom_call_target="tpu_custom_call" | custom-call | tf_op jit(solution)/shard_map/front/pallas_call | solution.py:188
  52.0 14.5 %all-to-all-start.1 = ((bf16[32,32,128]{2,1,0:T(8,128)(2,1)}), bf16[32,32,128]{2,1,0:T(8,128)(2,1)S(1)}, u32[]{:S(2)}, u32[]{:S(2)}) async-start(bf16[32,32,128]{2,1,0:T(8,128)(2,1)} %bitcast.34), calls=%async_computation.1 | async-start | bytes 524288 | tf_op jit(solution)/shard_map/all_to_all | solution.py:395
  66.5 0.0 all-gather.9.cloned.1.call-start
  66.5 1.4 copy.23.weights
  67.9 2.4 %table.1 = bf16[3,128,1024]{2,1,0:T(8,128)(2,1)} custom-call(s32[128,4]{1,0:T(8,128)} %get-tuple-element.27.slots, f32[128,4]{1,0:T(8,128)} %copy.23.weights), custom_call_target="tpu_custom_call" | custom-call | tf_op jit(solution)/shard_map/table/pallas_call | solution.py:126
  70.3 8.3 %all-to-all-done.1 = bf16[32,32,128]{2,1,0:T(8,128)(2,1)S(1)} async-done(((bf16[32,32,128]{2,1,0:T(8,128)(2,1)}), bf16[32,32,128]{2,1,0:T(8,128)(2,1)S(1)}, u32[]{:S(2)}, u32[]{:S(2)}) %all-to-all-start.1) | async-done | bytes 262176 | tf_op jit(solution)/shard_map/all_to_all | solution.py:395
  78.6 0.7 slice.20
  79.3 0.0 all-gather.9.cloned.1.call-update
  79.3 0.0 all-gather.11.cloned.1.call-start
  79.4 1.9 copy.24.sg
  81.3 0.0 copy-done.4
  81.3 1.0 copy.25.su
  82.3 0.8 pad_maximum_fusion
  83.1 18.7 %all-gather.2 = bf16[1792,128]{1,0:T(8,128)(2,1)} all-gather(bf16[112,128]{1,0:T(8,128)(2,1)S(1)} %slice.22), channel_id=4, replica_groups=mesh['sp'=32,'tp'=16] {'tp'}, dimensions={0}, use_global_device_ids=true | all-gather | bytes 487424 | tf_op jit(solution)/shard_map/all_gather | solution.py:410
  101.7 20.6 %all-gather.1 = bf16[3584,128]{1,0:T(8,128)(2,1)} all-gather(bf16[224,128]{1,0:T(8,128)(2,1)S(1)} %pad_maximum_fusion), channel_id=3, replica_groups=mesh['sp'=32,'tp'=16] {'tp'}, dimensions={0}, use_global_device_ids=true | all-gather | bytes 974848 | tf_op jit(solution)/shard_map/all_gather | solution.py:409
  122.4 4.0 %side_hidden.1 = (bf16[112,256]{1,0:T(8,128)(2,1)}, bf16[112,256]{1,0:T(8,128)(2,1)}) custom-call(bf16[16,224,128]{2,1,0:T(8,128)(2,1)} %bitcast.26, bf16[16,112,128]{2,1,0:T(8,128)(2,1)} %bitcast.28, f32[1,2048]{1,0:T(1,128)} %bitcast.35, bf16[2048,256]{1,0:T(8,128)(2,1)} %bitcast.20, bf16[2048,256]{1,0:T(8,128)(2,1)} %bitcast.22, ...), custom_call_target="tpu_custom_call" | custom-call | tf_op jit(solution)/shard_map/side_hidden/pallas_call | solution.py:260
  126.4 0.0 copy-start.5
  126.4 5.8 %hidden.1 = bf16[816,256]{1,0:T(8,128)(2,1)} custom-call(bf16[16,816,128]{2,1,0:T(8,128)(2,1)} %bitcast.27, f32[1,2048]{1,0:T(1,128)} %bitcast.36, bf16[2048,256]{1,0:T(8,128)(2,1)} %bitcast.21, bf16[2048,256]{1,0:T(8,128)(2,1)} %bitcast.23), custom_call_target="tpu_custom_call" | custom-call | tf_op jit(solution)/shard_map/hidden/pallas_call | solution.py:229
  132.3 0.0 all-gather.11.cloned.1.call-update
  132.3 21.9 %all-gather.4 = bf16[1792,256]{1,0:T(8,128)(2,1)} all-gather(bf16[112,256]{1,0:T(8,128)(2,1)} %get-tuple-element.36), channel_id=6, replica_groups=mesh['sp'=32,'tp'=16] {'tp'}, dimensions={0}, use_global_device_ids=true | all-gather | bytes 974848 | tf_op jit(solution)/shard_map/all_gather | solution.py:418
  154.2 0.0 copy-done.5
  154.2 25.7 %all-gather.5 = bf16[1792,256]{1,0:T(8,128)(2,1)} all-gather(bf16[112,256]{1,0:T(8,128)(2,1)S(1)} %copy-done.5), channel_id=7, replica_groups=mesh['sp'=32,'tp'=16] {'tp'}, dimensions={0}, use_global_device_ids=true | all-gather | bytes 974848 | tf_op jit(solution)/shard_map/all_gather | solution.py:418
  179.9 3.3 %side_down.1 = (bf16[208,128]{1,0:T(8,128)(2,1)}, f32[128,128]{1,0:T(8,128)}) custom-call(bf16[16,112,256]{2,1,0:T(8,128)(2,1)} %bitcast.24, bf16[16,112,256]{2,1,0:T(8,128)(2,1)} %bitcast.25, bf16[4096,128]{1,0:T(8,128)(2,1)} %bitcast.18, bf16[512,128]{1,0:T(8,128)(2,1)} %sh_down.1), custom_call_target="tpu_custom_call" | custom-call | tf_op jit(solution)/shard_map/side_down/pallas_call | solution.py:292
  183.2 1.1 all-gather.11.cloned.1.call-done
  184.3 5.7 %down.1 = bf16[1024,128]{1,0:T(8,128)(2,1)} custom-call(bf16[16,816,256]{2,1,0:T(8,128)(2,1)} %bitcast.17, bf16[4096,128]{1,0:T(8,128)(2,1)} %bitcast.19, bf16[208,128]{1,0:T(8,128)(2,1)} %get-tuple-element.40.aside), custom_call_target="tpu_custom_call" | custom-call | tf_op jit(solution)/shard_map/down/pallas_call | solution.py:320
  190.1 20.3 %all_to_all.15 = bf16[32,32,128]{2,1,0:T(8,128)(2,1)} all-to-all(bf16[32,32,128]{2,1,0:T(8,128)(2,1)} %bitcast.29), channel_id=1, replica_groups=mesh['sp'=32,'tp'=16] {'sp'}, dimensions={0} | all-to-all | bytes 524288 | tf_op jit(solution)/shard_map/all_to_all | solution.py:422
  210.4 2.2 combine.1
  (4 shorter events, 0.0 us)
Async XLA Ops:
  6.5 21.5 %copy-start = (bf16[128,2048]{1,0:T(8,128)(2,1)S(1)}, bf16[128,2048]{1,0:T(8,128)(2,1)}, u32[]{:S(2)}) copy-start(bf16[128,2048]{1,0:T(8,128)(2,1)} %param.17) | copy-start | bytes 1572868
  6.5 74.8 %copy-start.4 = (bf16[2048,32]{0,1:T(8,128)(2,1)S(1)}, bf16[2048,32]{0,1:T(8,128)(2,1)}, u32[]{:S(2)}) copy-start(bf16[2048,32]{0,1:T(8,128)(2,1)} %param.32) | copy-start | bytes 393220
  7.4 5.6 %copy-start.2 = (bf16[128,64]{1,0:T(8,128)(2,1)}, bf16[128,64]{1,0:T(8,128)(2,1)S(1)}, u32[]{:S(2)}) copy-start(bf16[128,64]{1,0:T(8,128)(2,1)S(1)} %copy.18.a_val) | copy-start | bytes 49156
  8.3 4.8 %copy-start.3 = (bf16[128,64]{1,0:T(8,128)(2,1)}, bf16[128,64]{1,0:T(8,128)(2,1)S(1)}, u32[]{:S(2)}) copy-start(bf16[128,64]{1,0:T(8,128)(2,1)S(1)} %copy.19.a_gate) | copy-start | bytes 49156
  8.3 4.7 %collective-permute-start = (bf16[30,64]{1,0:T(8,128)(2,1)S(1)}, bf16[30,64]{1,0:T(8,128)(2,1)S(1)}, u32[]{:S(2)}, u32[]{:S(2)}) collective-permute-start(bf16[30,64]{1,0:T(8,128)(2,1)S(1)} %multiply_convert_fusion), channel_id=1, source_target_pairs={{0,16},{16,32},{32,48},{48,64},{64,80},{80,96},{96,112},{112,128},... | collective-permute-start | bytes 11528 | tf_op jit(solution)/shard_map/ppermute | solution.py:383
  13.0 0.6 copy-start.6
  15.7 30.0 %all-to-all-start = ((bf16[16,176,128]{2,1,0:T(8,128)(2,1)}), bf16[16,176,128]{2,1,0:T(8,128)(2,1)S(1)}, u32[]{:S(2)}, u32[]{:S(2)}) async-start(bf16[16,176,128]{2,1,0:T(8,128)(2,1)} %pack.1), calls=%async_computation | async-start | bytes 1441792 | tf_op jit(solution)/shard_map/all_to_all | solution.py:387
  45.7 0.9 copy-start.1
  52.0 26.6 %all-to-all-start.1 = ((bf16[32,32,128]{2,1,0:T(8,128)(2,1)}), bf16[32,32,128]{2,1,0:T(8,128)(2,1)S(1)}, u32[]{:S(2)}, u32[]{:S(2)}) async-start(bf16[32,32,128]{2,1,0:T(8,128)(2,1)} %bitcast.34), calls=%async_computation.1 | async-start | bytes 524288 | tf_op jit(solution)/shard_map/all_to_all | solution.py:395
  66.5 59.9 %all-gather.9.cloned.1.call-start = ((), (), s32[]{:S(2)}) async-start(), calls=%async_computation.3 | async-start | bytes 3551232 | tf_op jit(solution)/shard_map/all_gather | solution.py:408
  79.3 105.0 %all-gather.11.cloned.1.call-start = ((), (), s32[]{:S(2)}) async-start(), calls=%async_computation.4 | async-start | bytes 7102464 | tf_op jit(solution)/shard_map/all_gather | solution.py:415
  126.4 27.8 %copy-start.5 = (bf16[112,256]{1,0:T(8,128)(2,1)S(1)}, bf16[112,256]{1,0:T(8,128)(2,1)}, u32[]{:S(2)}) copy-start(bf16[112,256]{1,0:T(8,128)(2,1)} %get-tuple-element.37) | copy-start | bytes 172036
Sparse Core Ops, SparseCore 0:
  79.4 35.7 all-gather.8
  132.4 51.8 all-gather.10

commit v4 on v3

--- a/solution.py
+++ b/solution.py
@@ -16,8 +16,8 @@
     return v / (1.0 + jnp.exp(-v))
 
 
-def pack_kernel(before, a_val, a_gate, taps, bias, gain, shift, w_out, out, win, params):
-    peers, _, lanes = out.shape
+def pack_kernel(before, a_val, a_gate, taps, bias, gain, shift, out, win, params):
+    peers = out.shape[0]
     halo, half = before.shape
     rows = win.shape[0]
     win[...] = jnp.zeros(win.shape, F32)
@@ -41,57 +41,57 @@
 
     head, tail = folded(win[...]), folded(params[...])
     top = rows // 2
-    low = top + tail.shape[0]
     for t in range(peers):
         out[t, 0:top, :] = head
-        out[t, top:low, :] = tail
-        out[t, low : low + w_out.shape[0], :] = w_out[:, t * lanes : (t + 1) * lanes]
+        out[t, top:, :] = tail
 
 
 PARAM_ROWS = 64
 FOLDED = 16
-ASIDE = (96, 112)
+DOWN_BLOCKS = 3
+ASIDE = (64, 96)
 
 
 def window_rows(span, tok_rows):
     return -(-(span - 1 + tok_rows) // 32) * 32
 
 
-def pack(before, a_val, a_gate, taps, bias, gain, shift, w_out, peers):
+def pack(before, a_val, a_gate, taps, bias, gain, shift, peers):
     rows = window_rows(taps.shape[0], a_val.shape[0])
-    lanes = w_out.shape[1] // peers
-    total = rows // 2 + PARAM_ROWS // 2 + w_out.shape[0]
+    total = (rows + PARAM_ROWS) // 2
     return pl.pallas_call(
         pack_kernel,
-        out_shape=jax.ShapeDtypeStruct((peers, total, lanes), BF16),
+        out_shape=jax.ShapeDtypeStruct((peers, total, LANES), BF16),
         scratch_shapes=[
             pltpu.VMEM((rows, a_val.shape[1]), F32),
             pltpu.VMEM((PARAM_ROWS, a_val.shape[1]), F32),
         ],
         name="pack",
-    )(before, a_val, a_gate, taps, bias, gain, shift, w_out)
+    )(before, a_val, a_gate, taps, bias, gain, shift)
 
 
 def routing_kernel(capacity, routes, slots_out, pick_out):
     tok_rows, top_count = routes.shape
-    experts = pick_out.shape[1] // capacity
+    slot_count = pick_out.shape[0]
+    experts = slot_count // capacity
     ids = lax.broadcasted_iota(jnp.int32, (tok_rows, experts), 1)
     hits = [ids == routes[:, k : k + 1] for k in range(top_count)]
     named = sum(jnp.where(h, 1.0, 0.0) for h in hits).astype(BF16)
     square = (tok_rows, tok_rows)
     below = lax.broadcasted_iota(jnp.int32, square, 0) > lax.broadcasted_iota(jnp.int32, square, 1)
     earlier = jnp.dot(jnp.where(below, 1.0, 0.0).astype(BF16), named, preferred_element_type=F32)
-    wide = lax.broadcasted_iota(jnp.int32, pick_out.shape, 1)
+    wide = lax.broadcasted_iota(jnp.int32, (tok_rows, slot_count), 1)
     lane = lax.broadcasted_iota(jnp.int32, slots_out.shape, 1)
     slots = jnp.zeros(slots_out.shape, jnp.int32)
-    pick = jnp.zeros(pick_out.shape, F32)
+    pick = jnp.zeros(wide.shape, F32)
     for k in range(top_count):
         place = jnp.sum(jnp.where(hits[k], earlier, 0.0), axis=1, keepdims=True).astype(jnp.int32)
         slot = routes[:, k : k + 1] * capacity + place
         slots = jnp.where(lane == k, slot, slots)
         pick = jnp.where(wide == slot, 1.0, pick)
     slots_out[...] = slots
-    pick_out[...] = pick.astype(BF16)
+    for at in range(0, slot_count, tok_rows):
+        pick_out[at : at + tok_rows, :] = pick[:, at : at + tok_rows].T.astype(BF16)
 
 
 def routing(routes, capacity, slot_count):
@@ -104,7 +104,7 @@
         kernel,
         out_shape=(
             jax.ShapeDtypeStruct((tok_rows, top_count), jnp.int32),
-            jax.ShapeDtypeStruct((tok_rows, slot_count), BF16),
+            jax.ShapeDtypeStruct((slot_count, tok_rows), BF16),
         ),
         name="routing",
     )(routes)
@@ -130,7 +130,7 @@
     )(slots, weights)
 
 
-def front_kernel(span, packed, resid, pick, middle_out, send_out, win, params, conv):
+def front_kernel(span, packed, wcol, resid, pick, middle_out, send_out, win, params, conv):
     peers = packed.shape[0]
     tok_rows = resid.shape[0]
     half = LANES // 2
@@ -164,21 +164,19 @@
     lax.fori_loop(0, channels // LANES, one_block, 0)
     gain = vector(span + 3)
     shift = vector(span + 6)
-    wcol = packed[:, top + fold :, :].reshape(channels, packed.shape[2])
     for r in range(0, tok_rows, 64):
         c = conv[r : r + 64, :]
         mean = jnp.sum(c, axis=1, keepdims=True) * (1.0 / channels)
         var = jnp.sum(c * c, axis=1, keepdims=True) * (1.0 / channels) - mean * mean
         scaled = (c - mean) * lax.rsqrt(var + LN_EPS) * gain + shift
         mixed = silu(scaled).astype(BF16)
-        proj = jnp.dot(mixed, wcol, preferred_element_type=F32)
+        proj = jnp.dot(mixed, wcol[...], preferred_element_type=F32)
         middle_out[r : r + 64, :] = (resid[r : r + 64, :].astype(F32) + proj).astype(BF16)
     middle = middle_out[...]
-    dims = (((0,), (0,)), ((), ()))
-    send_out[...] = lax.dot_general(pick[...], middle, dims, preferred_element_type=F32).astype(BF16)
-
-
-def front(span, packed, resid, pick):
+    send_out[...] = jnp.dot(pick[...], middle, preferred_element_type=F32).astype(BF16)
+
+
+def front(span, packed, wcol, resid, pick):
     tok_rows, cols = resid.shape
     channels = packed.shape[0] * LANES // 2
 
@@ -189,7 +187,7 @@
         kernel,
         out_shape=(
             jax.ShapeDtypeStruct((tok_rows, cols), BF16),
-            jax.ShapeDtypeStruct((pick.shape[1], cols), BF16),
+            jax.ShapeDtypeStruct((pick.shape[0], cols), BF16),
         ),
         scratch_shapes=[
             pltpu.VMEM((window_rows(span, tok_rows), channels), F32),
@@ -197,7 +195,7 @@
             pltpu.VMEM((tok_rows, channels), F32),
         ],
         name="front",
-    )(packed, resid, pick)
+    )(packed, wcol, resid, pick)
 
 
 def normed_rows(pieces, width, gain):
@@ -217,12 +215,24 @@
     return (silu(g) * u).astype(BF16)
 
 
-def hidden_kernel(rows_in, gain, wg, wu, out):
+def hidden_kernel(rows_in, gain, wg, wu, aside_out, out):
+    step = pl.program_id(0)
+    block = rows_in.shape[1]
+    aside = aside_out.shape[0]
     rows = normed_rows([rows_in[t] for t in range(rows_in.shape[0])], wg.shape[0], gain)
-    out[...] = gated_units(rows, wg[...], wu[...])
-
-
-def hidden_units(rows_in, gain, wg, wu, blocks):
+    units = gated_units(rows, wg[...], wu[...])
+
+    @pl.when(step == 0)
+    def _():
+        aside_out[...] = units[0:aside, :]
+        out[0 : block - aside, :] = units[aside:, :]
+
+    @pl.when(step > 0)
+    def _():
+        out[pl.ds(pl.multiple_of(step * block - aside, 16), block), :] = units
+
+
+def hidden_units(rows_in, gain, wg, wu, blocks, aside):
     pieces, rows, lanes = rows_in.shape
     width, units = wg.shape
     block = rows // blocks
@@ -235,36 +245,36 @@
             pl.BlockSpec((width, units), lambda i: (0, 0)),
             pl.BlockSpec((width, units), lambda i: (0, 0)),
         ],
-        out_specs=pl.BlockSpec((block, units), lambda i: (i, 0)),
-        out_shape=jax.ShapeDtypeStruct((rows, units), BF16),
+        out_specs=[
+            pl.BlockSpec((aside, units), lambda i: (0, 0)),
+            pl.BlockSpec((rows - aside, units), lambda i: (0, 0)),
+        ],
+        out_shape=(
+            jax.ShapeDtypeStruct((aside, units), BF16),
+            jax.ShapeDtypeStruct((rows - aside, units), BF16),
+        ),
         name="hidden",
     )(rows_in, gain, wg, wu)
 
 
-def side_hidden_kernel(one, two, gain, wg, wu, sg, su, one_out, two_out):
+def side_hidden_kernel(one, gain, wg, wu, sg, su, out):
     width, units = wg.shape
     few = sg.shape[1]
-    slots = one_out.shape[0] - FOLDED
+    slots = out.shape[0] - FOLDED
     rows = normed_rows([one[t] for t in range(one.shape[0])], width, gain)
-    one_out[0:slots, :] = gated_units(rows[0:slots, :], wg[...], wu[...])
+    out[0:slots, :] = gated_units(rows[0:slots, :], wg[...], wu[...])
     shared = gated_units(rows[slots:, :], sg[...], su[...])
     parts = [shared[j * FOLDED : (j + 1) * FOLDED, :].astype(F32) for j in range(units // few)]
-    one_out[slots:, :] = jnp.concatenate(parts, axis=1).astype(BF16)
-    rows = normed_rows([two[t] for t in range(two.shape[0])], width, gain)
-    two_out[...] = gated_units(rows, wg[...], wu[...])
-
-
-def side_hidden(one, two, gain, wg, wu, sg, su, tok_rows):
-    units = wg.shape[1]
+    out[slots:, :] = jnp.concatenate(parts, axis=1).astype(BF16)
+
+
+def side_hidden(one, gain, wg, wu, sg, su, tok_rows):
     slots = one.shape[1] - tok_rows
     return pl.pallas_call(
         side_hidden_kernel,
-        out_shape=(
-            jax.ShapeDtypeStruct((slots + FOLDED, units), BF16),
-            jax.ShapeDtypeStruct((two.shape[1], units), BF16),
-        ),
+        out_shape=jax.ShapeDtypeStruct((slots + FOLDED, wg.shape[1]), BF16),
         name="side_hidden",
-    )(one, two, gain, wg, wu, sg, su)
+    )(one, gain, wg, wu, sg, su)
 
 
 def side_down_kernel(one, two, wd, sh_down, out, shared_out):
@@ -377,20 +387,24 @@
     capacity = max(2 * tok_rows * top_count // experts_all, tp_count)
     slot_count = experts_all * capacity
 
+    w_parts = jnp.moveaxis(w_out.reshape(w_out.shape[0], tp_count, col_width), 1, 0)
+    wcol = lax.all_to_all(w_parts, "tp", split_axis=0, concat_axis=0, tiled=True)
+    wcol = wcol.reshape(w_out.shape[0] * tp_count, col_width)
+
     halo = span - 1
     late_val, late_gate = a_val[tok_rows - halo :].astype(F32), a_gate[tok_rows - halo :].astype(F32)
     pairs = [(i, i + 1) for i in range(sp_count - 1)]
     before = lax.ppermute((late_val * jax.nn.sigmoid(late_gate)).astype(BF16), "sp", pairs)
 
     vectors = [v[None, :] for v in (conv_bias, ln_gain, ln_bias)]
-    packed = pack(before, a_val, a_gate, conv_kernel, *vectors, w_out, tp_count)
+    packed = pack(before, a_val, a_gate, conv_kernel, *vectors, tp_count)
     spread = lax.all_to_all(packed, "tp", split_axis=0, concat_axis=0, tiled=True)
 
     routes_late, _ = lax.optimization_barrier((routes, packed[0, :1]))
     slots, pick = routing(routes_late, capacity, slot_count)
 
     resid_cols = lax.dynamic_slice_in_dim(resid, tp_place * col_width, col_width, 1)
-    middle, send = front(span, spread, resid_cols, pick)
+    middle, send = front(span, spread, wcol, resid_cols, pick)
 
     landed = lax.all_to_all(
         send.reshape(sp_count, slot_count // sp_count, col_width),
@@ -402,23 +416,22 @@
     slots_late, weights_late, _ = lax.optimization_barrier((slots, route_weights, middle[:1]))
     table = weight_table(slots_late, weights_late, slot_count)
     landed, table = lax.optimization_barrier((landed, table))
-    first, aside = ASIDE[0], sum(ASIDE)
+    first = ASIDE[0]
     gain = ffn_gain[None, :]
     experts = (gain, exp_gate[0], exp_up[0])
-    arrived = lax.all_gather(landed[aside:], "tp")
+    arrived = lax.all_gather(landed[first:], "tp")
     one = lax.all_gather(jnp.concatenate([landed[:first], middle], axis=0), "tp")
-    two = lax.all_gather(landed[first:aside], "tp")
-    one, two = side_hidden(one, two, *experts, sh_gate, sh_up, tok_rows)
-    arrived, one, two = lax.optimization_barrier((arrived, one, two))
-    hidden = hidden_units(arrived, *experts, 3)
+    one = side_hidden(one, *experts, sh_gate, sh_up, tok_rows)
+    arrived, one = lax.optimization_barrier((arrived, one))
+    two, hidden = hidden_units(arrived, *experts, 4, ASIDE[1])
 
     hidden_all = lax.all_gather(hidden, "tp")
-    one, two, _ = lax.optimization_barrier((one, two, hidden[:1]))
+    one, two = lax.optimization_barrier((one, two))
     side_out, shared = side_down(
         lax.all_gather(one, "tp"), lax.all_gather(two, "tp"), exp_down[0], sh_down, tok_rows
     )
     hidden_all, side_out = lax.optimization_barrier((hidden_all, side_out))
-    expert_out = down(hidden_all, exp_down[0], side_out, 3)
+    expert_out = down(hidden_all, exp_down[0], side_out, DOWN_BLOCKS)
     returned = lax.all_to_all(
         expert_out.reshape(sp_count, slot_count // sp_count, col_width),
         "sp",

time: 220 us -> 219 us (level)
  blocking collectives: 107 us -> 87.4 us
  waiting for transfers between devices: 27.3 us -> 41 us
  local copies, waits for them, and re-layouts: 10.3 us -> 12.8 us
  starting transfers between devices: 27.2 us -> 29.6 us
    all_gather x1 -> x0, blocking collectives: 18.7 us -> none  [body(): two = lax.all_gather(landed[first:aside], 'tp')]
    all_to_all x0 -> x1, starting transfers between devices: none -> 10.2 us  [body(): lax.all_to_all(w_parts, 'tp', split_axis=0, concat_axis=0, tiled=True)]
    all_gather x1, waiting for transfers between devices: 0.01 us -> 7.91 us  [body(): arrived = lax.all_gather(landed[first:], 'tp')]
    all_to_all x1, waiting for transfers between devices: 17.1 us -> 10.9 us  [body(): lax.all_to_all(packed, 'tp', split_axis=0, concat_axis=0, tiled=True)]
    all_gather x1, waiting for transfers between devices: 1.14 us -> 7.03 us  [body(): hidden_all = lax.all_gather(hidden, 'tp')]
    all_to_all x0 -> x1, waiting for transfers between devices: none -> 5.36 us  [body(): lax.all_to_all(w_parts, 'tp', split_axis=0, concat_axis=0, tiled=True)]
    all_to_all x1, starting transfers between devices: 8.64 us -> 3.46 us  [body(): lax.all_to_all(packed, 'tp', split_axis=0, concat_axis=0, tiled=True)]
    all_gather x1, blocking collectives: 25.7 us -> 23.1 us  [body(): lax.all_gather(two, 'tp')]
  transfers between devices with their start and end apart: 5 -> 6, of which waited for: 4 -> 6; matrix products, arithmetic and copies ran while one was open for 3% -> 4% of each run, Pallas kernels for 5% -> 6%
where the time goes in v4:
time: 219 us; the launch traced here: 218 us
  blocking collectives  87.4 us (40%)
  waiting for transfers between devices  41 us (19%)
  Pallas kernels  33.2 us (15%)
  starting transfers between devices  29.6 us (14%)
  between operations  13.5 us (6%)
  local copies, waits for them, and re-layouts  12.8 us (6%)
    all_gather x1, blocking collectives, body(): lax.all_gather(two, 'tp')  23.1 us
    all_gather x1, blocking collectives, body(): lax.all_gather(jnp.concatenate([landed[:first], middle], axis=0), 'tp')  21.7 us
    all_to_all x1, blocking collectives, body(): lax.all_to_all(expert_out.reshape(sp_count, slot_count // sp_count, col_w...  21.4 us
    all_gather x1, blocking collectives, body(): lax.all_gather(one, 'tp')  21.2 us
    all_to_all x1, starting transfers between devices, body(): lax.all_to_all(send.reshape(sp_count, slot_count // sp_count, col_width),...  14.4 us
    all_to_all x1, waiting for transfers between devices, body(): lax.all_to_all(packed, 'tp', split_axis=0, concat_axis=0, tiled=True)  10.9 us
    all_to_all x1, starting transfers between devices, body(): lax.all_to_all(w_parts, 'tp', split_axis=0, concat_axis=0, tiled=True)  10.2 us
    all_to_all x1, waiting for transfers between devices, body(): lax.all_to_all(send.reshape(sp_count, slot_count // sp_count, col_width),...  8.92 us
  transfers between devices with their start and end apart: 6, of which 6 were waited for; matrix products, arithmetic and copies ran while one was open for 4% of the time, Pallas kernels for 6%

profile of v4, /device:TPU:1, one launch (start us, length us, event | category | flops | bytes accessed | tf_op | source)
XLA Modules:
  0.0 218.3 jit_solution(8250106362194727658)
XLA Ops:
  6.5 0.0 copy-start
  6.5 1.8 bitcast_bitcast_fusion
  8.3 10.2 %all-to-all-start.1 = ((bf16[16,64,128]{2,1,0:T(8,128)(2,1)}), bf16[16,64,128]{2,1,0:T(8,128)(2,1)S(1)}, u32[]{:S(2)}, u32[]{:S(2)}) async-start(bf16[16,64,128]{2,1,0:T(8,128)(2,1)} %bitcast_bitcast_fusion), calls=%async_computation.1 | async-start | bytes 524288 | tf_op jit(solution)/shard_map/all_to_all | solution.py:391
  18.5 0.8 copy.18.a_val
  19.3 0.0 copy-start.3
  19.3 0.8 copy.19.a_gate
  20.1 0.0 copy-start.4
  20.2 1.6 collective-permute-start
  21.8 0.8 collective-permute-done.before
  22.5 0.0 copy-start.5
  22.5 0.0 copy-done.3
  22.5 0.0 copy-done.4
  22.5 0.6 copy-done.5
  23.1 1.7 pack.1
  24.9 5.4 %all-to-all-done.1 = bf16[16,64,128]{2,1,0:T(8,128)(2,1)S(1)} async-done(((bf16[16,64,128]{2,1,0:T(8,128)(2,1)}), bf16[16,64,128]{2,1,0:T(8,128)(2,1)S(1)}, u32[]{:S(2)}, u32[]{:S(2)}) %all-to-all-start.1) | async-done | bytes 262176 | tf_op jit(solution)/shard_map/all_to_all | solution.py:391
  30.2 0.0 copy-start.2
  30.2 3.5 %all-to-all-start = ((bf16[16,112,128]{2,1,0:T(8,128)(2,1)}), bf16[16,112,128]{2,1,0:T(8,128)(2,1)S(1)}, u32[]{:S(2)}, u32[]{:S(2)}) async-start(bf16[16,112,128]{2,1,0:T(8,128)(2,1)} %pack.1), calls=%async_computation | async-start | bytes 917504 | tf_op jit(solution)/shard_map/all_to_all | solution.py:401
  33.7 1.4 copy.23.refs_0_
  35.1 2.3 %routing.1 = (s32[128,4]{1,0:T(8,128)}, bf16[1024,128]{1,0:T(8,128)(2,1)}) custom-call(s32[128,4]{1,0:T(8,128)} %copy.23.refs_0_), custom_call_target="tpu_custom_call" | custom-call | tf_op jit(solution)/shard_map/routing/pallas_call | solution.py:103
  37.4 0.0 copy-done
  37.4 0.6 constant_dynamic-slice_fusion.refs_2_
  38.0 10.9 %all-to-all-done.refs_0_ = bf16[16,112,128]{2,1,0:T(8,128)(2,1)S(1)} async-done(((bf16[16,112,128]{2,1,0:T(8,128)(2,1)}), bf16[16,112,128]{2,1,0:T(8,128)(2,1)S(1)}, u32[]{:S(2)}, u32[]{:S(2)}) %all-to-all-start) | async-done | bytes 458784 | tf_op jit(solution)/shard_map/all_to_all | solution.py:401
  48.9 0.0 copy-done.2
  48.9 0.8 copy-done.1
  49.7 5.4 %front.1 = (bf16[128,128]{1,0:T(8,128)(2,1)}, bf16[1024,128]{1,0:T(8,128)(2,1)}) custom-call(bf16[16,112,128]{2,1,0:T(8,128)(2,1)} %copy-done.1, bf16[1024,128]{1,0:T(8,128)(2,1)} %bitcast.38, bf16[128,128]{1,0:T(8,128)(2,1)} %constant_dynamic-slice_fusion.refs_2_, bf16[1024,128]{1,0:T(8,128)(2,1)} %get-tuple-element.23.refs_3_), custom_call_target="tpu_custom_call" | custom-call | tf_op jit(solution)/shard_map/front/pallas_call | solution.py:186
  55.1 14.4 %all-to-all-start.2 = ((bf16[32,32,128]{2,1,0:T(8,128)(2,1)}), bf16[32,32,128]{2,1,0:T(8,128)(2,1)S(1)}, u32[]{:S(2)}, u32[]{:S(2)}) async-start(bf16[32,32,128]{2,1,0:T(8,128)(2,1)} %bitcast.40), calls=%async_computation.2 | async-start | bytes 524288 | tf_op jit(solution)/shard_map/all_to_all | solution.py:409
  69.5 0.0 all-gather.8.cloned.1.call-start
  69.5 1.4 copy.24.weights
  70.9 2.3 %table.1 = bf16[3,128,1024]{2,1,0:T(8,128)(2,1)} custom-call(s32[128,4]{1,0:T(8,128)} %get-tuple-element.26.slots, f32[128,4]{1,0:T(8,128)} %copy.24.weights), custom_call_target="tpu_custom_call" | custom-call | tf_op jit(solution)/shard_map/table/pallas_call | solution.py:126
  73.2 8.9 %all-to-all-done.2 = bf16[32,32,128]{2,1,0:T(8,128)(2,1)S(1)} async-done(((bf16[32,32,128]{2,1,0:T(8,128)(2,1)}), bf16[32,32,128]{2,1,0:T(8,128)(2,1)S(1)}, u32[]{:S(2)}, u32[]{:S(2)}) %all-to-all-start.2) | async-done | bytes 262176 | tf_op jit(solution)/shard_map/all_to_all | solution.py:409
  82.1 0.7 slice.16
  82.8 0.0 all-gather.8.cloned.1.call-update
  82.8 0.0 all-gather.10.cloned.1.call-start
  82.9 1.9 copy.25.sg
  84.8 1.9 copy.26.su
  86.7 0.8 pad_maximum_fusion
  87.5 21.7 %all-gather.1 = bf16[3072,128]{1,0:T(8,128)(2,1)} all-gather(bf16[192,128]{1,0:T(8,128)(2,1)S(1)} %pad_maximum_fusion), channel_id=3, replica_groups=mesh['sp'=32,'tp'=16] {'tp'}, dimensions={0}, use_global_device_ids=true | all-gather | bytes 835584 | tf_op jit(solution)/shard_map/all_gather | solution.py:423
  109.2 3.7 %side_hidden.1 = bf16[80,256]{1,0:T(8,128)(2,1)} custom-call(bf16[16,192,128]{2,1,0:T(8,128)(2,1)} %bitcast.33, f32[1,2048]{1,0:T(1,128)} %bitcast.41, bf16[2048,256]{1,0:T(8,128)(2,1)} %bitcast.27, bf16[2048,256]{1,0:T(8,128)(2,1)} %bitcast.29, bf16[2048,32]{1,0:T(8,128)(2,1)} %copy.25.sg, bf16[2048,32]{1,0:T(8,128)(2,1)} %copy.26.su), custom_call_target="tpu_custom_call" | custom-call | tf_op jit(solution)/shard_map/side_hidden/pallas_call | solution.py:273
  112.9 7.9 %all-gather.8.cloned.1.call-done = bf16[15360,128]{1,0:T(8,128)(2,1)} async-done(((bf16[960,128]{1,0:T(8,128)(2,1)}), bf16[15360,128]{1,0:T(8,128)(2,1)}) %all-gather.8.cloned.1.call-update) | async-done | bytes 3932176 | tf_op jit(solution)/shard_map/all_gather | solution.py:422
  120.8 6.7 %hidden.1 = (bf16[96,256]{1,0:T(8,128)(2,1)}, bf16[864,256]{1,0:T(8,128)(2,1)}) custom-call(bf16[16,960,128]{2,1,0:T(8,128)(2,1)} %bitcast.31, f32[1,2048]{1,0:T(1,128)} %bitcast.42, bf16[2048,256]{1,0:T(8,128)(2,1)} %bitcast.28, bf16[2048,256]{1,0:T(8,128)(2,1)} %bitcast.30), custom_call_target="tpu_custom_call" | custom-call | tf_op jit(solution)/shard_map/hidden/pallas_call | solution.py:239
  127.5 0.0 all-gather.10.cloned.1.call-update
  127.5 21.2 %all-gather.3 = bf16[1280,256]{1,0:T(8,128)(2,1)} all-gather(bf16[80,256]{1,0:T(8,128)(2,1)} %side_hidden.1), channel_id=5, replica_groups=mesh['sp'=32,'tp'=16] {'tp'}, dimensions={0}, use_global_device_ids=true | all-gather | bytes 696320 | tf_op jit(solution)/shard_map/all_gather | solution.py:431
  148.6 23.1 %all-gather.4 = bf16[1536,256]{1,0:T(8,128)(2,1)} all-gather(bf16[96,256]{1,0:T(8,128)(2,1)} %get-tuple-element.35), channel_id=6, replica_groups=mesh['sp'=32,'tp'=16] {'tp'}, dimensions={0}, use_global_device_ids=true | all-gather | bytes 835584 | tf_op jit(solution)/shard_map/all_gather | solution.py:431
  171.8 3.2 %side_down.1 = (bf16[160,128]{1,0:T(8,128)(2,1)}, f32[128,128]{1,0:T(8,128)}) custom-call(bf16[16,80,256]{2,1,0:T(8,128)(2,1)} %bitcast.34, bf16[16,96,256]{2,1,0:T(8,128)(2,1)} %bitcast.32, bf16[4096,128]{1,0:T(8,128)(2,1)} %bitcast.25, bf16[512,128]{1,0:T(8,128)(2,1)} %sh_down.1), custom_call_target="tpu_custom_call" | custom-call | tf_op jit(solution)/shard_map/side_down/pallas_call | solution.py:302
  174.9 7.0 %all-gather.10.cloned.1.call-done = bf16[13824,256]{1,0:T(8,128)(2,1)} async-done(((bf16[864,256]{1,0:T(8,128)(2,1)}), bf16[13824,256]{1,0:T(8,128)(2,1)}) %all-gather.10.cloned.1.call-update) | async-done | bytes 7077904 | tf_op jit(solution)/shard_map/all_gather | solution.py:428
  182.0 5.9 %down.1 = bf16[1024,128]{1,0:T(8,128)(2,1)} custom-call(bf16[16,864,256]{2,1,0:T(8,128)(2,1)} %bitcast.24, bf16[4096,128]{1,0:T(8,128)(2,1)} %bitcast.26, bf16[160,128]{1,0:T(8,128)(2,1)} %get-tuple-element.38.aside), custom_call_target="tpu_custom_call" | custom-call | tf_op jit(solution)/shard_map/down/pallas_call | solution.py:330
  187.9 21.4 %all_to_all.20 = bf16[32,32,128]{2,1,0:T(8,128)(2,1)} all-to-all(bf16[32,32,128]{2,1,0:T(8,128)(2,1)} %bitcast.35), channel_id=1, replica_groups=mesh['sp'=32,'tp'=16] {'sp'}, dimensions={0} | all-to-all | bytes 524288 | tf_op jit(solution)/shard_map/all_to_all | solution.py:435
  209.3 2.2 combine.1
  (3 shorter events, 0.0 us)
Async XLA Ops:
  6.5 30.8 %copy-start = (bf16[128,2048]{1,0:T(8,128)(2,1)S(1)}, bf16[128,2048]{1,0:T(8,128)(2,1)}, u32[]{:S(2)}) copy-start(bf16[128,2048]{1,0:T(8,128)(2,1)} %param.17) | copy-start | bytes 1572868
  8.3 21.9 %all-to-all-start.1 = ((bf16[16,64,128]{2,1,0:T(8,128)(2,1)}), bf16[16,64,128]{2,1,0:T(8,128)(2,1)S(1)}, u32[]{:S(2)}, u32[]{:S(2)}) async-start(bf16[16,64,128]{2,1,0:T(8,128)(2,1)} %bitcast_bitcast_fusion), calls=%async_computation.1 | async-start | bytes 524288 | tf_op jit(solution)/shard_map/all_to_all | solution.py:391
  19.3 3.2 %copy-start.3 = (bf16[128,64]{1,0:T(8,128)(2,1)}, bf16[128,64]{1,0:T(8,128)(2,1)S(1)}, u32[]{:S(2)}) copy-start(bf16[128,64]{1,0:T(8,128)(2,1)S(1)} %copy.18.a_val) | copy-start | bytes 49156
  20.1 2.4 %copy-start.4 = (bf16[128,64]{1,0:T(8,128)(2,1)}, bf16[128,64]{1,0:T(8,128)(2,1)S(1)}, u32[]{:S(2)}) copy-start(bf16[128,64]{1,0:T(8,128)(2,1)S(1)} %copy.19.a_gate) | copy-start | bytes 49156
  20.2 2.3 %collective-permute-start = (bf16[30,64]{1,0:T(8,128)(2,1)S(1)}, bf16[30,64]{1,0:T(8,128)(2,1)S(1)}, u32[]{:S(2)}, u32[]{:S(2)}) collective-permute-start(bf16[30,64]{1,0:T(8,128)(2,1)S(1)} %multiply_convert_fusion), channel_id=1, source_target_pairs={{0,16},{16,32},{32,48},{48,64},{64,80},{80,96},{96,112},{112,128},... | collective-permute-start | bytes 11528 | tf_op jit(solution)/shard_map/ppermute | solution.py:397
  22.5 0.6 copy-start.5
  30.2 18.7 %copy-start.2 = (bf16[16,64,128]{2,1,0:T(8,128)(2,1)}, bf16[16,64,128]{2,1,0:T(8,128)(2,1)S(1)}, u32[]{:S(2)}) copy-start(bf16[16,64,128]{2,1,0:T(8,128)(2,1)S(1)} %all-to-all-done.1) | copy-start | bytes 786436
  30.2 18.7 %all-to-all-start = ((bf16[16,112,128]{2,1,0:T(8,128)(2,1)}), bf16[16,112,128]{2,1,0:T(8,128)(2,1)S(1)}, u32[]{:S(2)}, u32[]{:S(2)}) async-start(bf16[16,112,128]{2,1,0:T(8,128)(2,1)} %pack.1), calls=%async_computation | async-start | bytes 917504 | tf_op jit(solution)/shard_map/all_to_all | solution.py:401
  48.9 0.8 copy-start.1
  55.1 27.0 %all-to-all-start.2 = ((bf16[32,32,128]{2,1,0:T(8,128)(2,1)}), bf16[32,32,128]{2,1,0:T(8,128)(2,1)S(1)}, u32[]{:S(2)}, u32[]{:S(2)}) async-start(bf16[32,32,128]{2,1,0:T(8,128)(2,1)} %bitcast.40), calls=%async_computation.2 | async-start | bytes 524288 | tf_op jit(solution)/shard_map/all_to_all | solution.py:409
  69.5 51.3 %all-gather.8.cloned.1.call-start = ((), (), s32[]{:S(2)}) async-start(), calls=%async_computation.4 | async-start | bytes 4177920 | tf_op jit(solution)/shard_map/all_gather | solution.py:422
  82.8 99.1 %all-gather.10.cloned.1.call-start = ((), (), s32[]{:S(2)}) async-start(), calls=%async_computation.5 | async-start | bytes 7520256 | tf_op jit(solution)/shard_map/all_gather | solution.py:428
Sparse Core Ops, SparseCore 0:
  83.0 37.7 all-gather.7
  127.6 54.3 all-gather.9

commit v5 on v4

--- a/solution.py
+++ b/solution.py
@@ -16,8 +16,8 @@
     return v / (1.0 + jnp.exp(-v))
 
 
-def pack_kernel(before, a_val, a_gate, taps, bias, gain, shift, out, win, params):
-    peers = out.shape[0]
+def pack_kernel(before, a_val, a_gate, taps, bias, gain, shift, w_out, out, win, params):
+    peers, _, lanes = out.shape
     halo, half = before.shape
     rows = win.shape[0]
     win[...] = jnp.zeros(win.shape, F32)
@@ -41,33 +41,35 @@
 
     head, tail = folded(win[...]), folded(params[...])
     top = rows // 2
+    low = top + tail.shape[0]
     for t in range(peers):
         out[t, 0:top, :] = head
-        out[t, top:, :] = tail
+        out[t, top:low, :] = tail
+        out[t, low : low + w_out.shape[0], :] = w_out[:, t * lanes : (t + 1) * lanes]
 
 
 PARAM_ROWS = 64
 FOLDED = 16
-DOWN_BLOCKS = 3
-ASIDE = (64, 96)
+ASIDE = (96, 112)
 
 
 def window_rows(span, tok_rows):
     return -(-(span - 1 + tok_rows) // 32) * 32
 
 
-def pack(before, a_val, a_gate, taps, bias, gain, shift, peers):
+def pack(before, a_val, a_gate, taps, bias, gain, shift, w_out, peers):
     rows = window_rows(taps.shape[0], a_val.shape[0])
-    total = (rows + PARAM_ROWS) // 2
+    lanes = w_out.shape[1] // peers
+    total = rows // 2 + PARAM_ROWS // 2 + w_out.shape[0]
     return pl.pallas_call(
         pack_kernel,
-        out_shape=jax.ShapeDtypeStruct((peers, total, LANES), BF16),
+        out_shape=jax.ShapeDtypeStruct((peers, total, lanes), BF16),
         scratch_shapes=[
             pltpu.VMEM((rows, a_val.shape[1]), F32),
             pltpu.VMEM((PARAM_ROWS, a_val.shape[1]), F32),
         ],
         name="pack",
-    )(before, a_val, a_gate, taps, bias, gain, shift)
+    )(before, a_val, a_gate, taps, bias, gain, shift, w_out)
 
 
 def routing_kernel(capacity, routes, slots_out, pick_out):
@@ -130,7 +132,7 @@
     )(slots, weights)
 
 
-def front_kernel(span, packed, wcol, resid, pick, middle_out, send_out, win, params, conv):
+def front_kernel(span, packed, resid, pick, middle_out, send_out, win, params, conv):
     peers = packed.shape[0]
     tok_rows = resid.shape[0]
     half = LANES // 2
@@ -164,19 +166,20 @@
     lax.fori_loop(0, channels // LANES, one_block, 0)
     gain = vector(span + 3)
     shift = vector(span + 6)
+    wcol = packed[:, top + fold :, :].reshape(channels, packed.shape[2])
     for r in range(0, tok_rows, 64):
         c = conv[r : r + 64, :]
         mean = jnp.sum(c, axis=1, keepdims=True) * (1.0 / channels)
         var = jnp.sum(c * c, axis=1, keepdims=True) * (1.0 / channels) - mean * mean
         scaled = (c - mean) * lax.rsqrt(var + LN_EPS) * gain + shift
         mixed = silu(scaled).astype(BF16)
-        proj = jnp.dot(mixed, wcol[...], preferred_element_type=F32)
+        proj = jnp.dot(mixed, wcol, preferred_element_type=F32)
         middle_out[r : r + 64, :] = (resid[r : r + 64, :].astype(F32) + proj).astype(BF16)
     middle = middle_out[...]
     send_out[...] = jnp.dot(pick[...], middle, preferred_element_type=F32).astype(BF16)
 
 
-def front(span, packed, wcol, resid, pick):
+def front(span, packed, resid, pick):
     tok_rows, cols = resid.shape
     channels = packed.shape[0] * LANES // 2
 
@@ -195,7 +198,7 @@
             pltpu.VMEM((tok_rows, channels), F32),
         ],
         name="front",
-    )(packed, wcol, resid, pick)
+    )(packed, resid, pick)
 
 
 def normed_rows(pieces, width, gain):
@@ -309,36 +312,25 @@
     )(one, two, wd, sh_down)
 
 
-def down_kernel(hidden, wd, aside, out):
-    slots = aside.shape[0]
-    block = hidden.shape[1]
-    step = pl.program_id(0)
-
-    @pl.when(step == 0)
-    def _():
-        out[0:slots, :] = aside[...]
-
+def down_kernel(hidden, wd, out):
     whole = jnp.concatenate([hidden[t] for t in range(hidden.shape[0])], axis=1)
-    at = pl.ds(pl.multiple_of(slots + step * block, 16), block)
-    out[at, :] = jnp.dot(whole, wd[...], preferred_element_type=F32).astype(BF16)
-
-
-def down(hidden, wd, aside, blocks):
+    out[...] = jnp.dot(whole, wd[...], preferred_element_type=F32).astype(BF16)
+
+
+def down(hidden, wd, blocks):
     pieces, rows, units = hidden.shape
     block = rows // blocks
-    total = (aside.shape[0] + rows, wd.shape[1])
     return pl.pallas_call(
         down_kernel,
         grid=(blocks,),
         in_specs=[
             pl.BlockSpec((pieces, block, units), lambda i: (0, i, 0)),
             pl.BlockSpec(wd.shape, lambda i: (0, 0)),
-            pl.BlockSpec(aside.shape, lambda i: (0, 0)),
         ],
-        out_specs=pl.BlockSpec(total, lambda i: (0, 0)),
-        out_shape=jax.ShapeDtypeStruct(total, BF16),
+        out_specs=pl.BlockSpec((block, wd.shape[1]), lambda i: (i, 0)),
+        out_shape=jax.ShapeDtypeStruct((rows, wd.shape[1]), BF16),
         name="down",
-    )(hidden, wd, aside)
+    )(hidden, wd)
 
 
 def combine_kernel(returned, table, middle, shared, out):
@@ -387,24 +379,20 @@
     capacity = max(2 * tok_rows * top_count // experts_all, tp_count)
     slot_count = experts_all * capacity
 
-    w_parts = jnp.moveaxis(w_out.reshape(w_out.shape[0], tp_count, col_width), 1, 0)
-    wcol = lax.all_to_all(w_parts, "tp", split_axis=0, concat_axis=0, tiled=True)
-    wcol = wcol.reshape(w_out.shape[0] * tp_count, col_width)
-
     halo = span - 1
     late_val, late_gate = a_val[tok_rows - halo :].astype(F32), a_gate[tok_rows - halo :].astype(F32)
     pairs = [(i, i + 1) for i in range(sp_count - 1)]
     before = lax.ppermute((late_val * jax.nn.sigmoid(late_gate)).astype(BF16), "sp", pairs)
 
     vectors = [v[None, :] for v in (conv_bias, ln_gain, ln_bias)]
-    packed = pack(before, a_val, a_gate, conv_kernel, *vectors, tp_count)
+    packed = pack(before, a_val, a_gate, conv_kernel, *vectors, w_out, tp_count)
     spread = lax.all_to_all(packed, "tp", split_axis=0, concat_axis=0, tiled=True)
 
     routes_late, _ = lax.optimization_barrier((routes, packed[0, :1]))
     slots, pick = routing(routes_late, capacity, slot_count)
 
     resid_cols = lax.dynamic_slice_in_dim(resid, tp_place * col_width, col_width, 1)
-    middle, send = front(span, spread, wcol, resid_cols, pick)
+    middle, send = front(span, spread, resid_cols, pick)
 
     landed = lax.all_to_all(
         send.reshape(sp_count, slot_count // sp_count, col_width),
@@ -423,7 +411,7 @@
     one = lax.all_gather(jnp.concatenate([landed[:first], middle], axis=0), "tp")
     one = side_hidden(one, *experts, sh_gate, sh_up, tok_rows)
     arrived, one = lax.optimization_barrier((arrived, one))
-    two, hidden = hidden_units(arrived, *experts, 4, ASIDE[1])
+    two, hidden = hidden_units(arrived, *experts, 2, ASIDE[1])
 
     hidden_all = lax.all_gather(hidden, "tp")
     one, two = lax.optimization_barrier((one, two))
@@ -431,7 +419,7 @@
         lax.all_gather(one, "tp"), lax.all_gather(two, "tp"), exp_down[0], sh_down, tok_rows
     )
     hidden_all, side_out = lax.optimization_barrier((hidden_all, side_out))
-    expert_out = down(hidden_all, exp_down[0], side_out, DOWN_BLOCKS)
+    expert_out = jnp.concatenate([side_out, down(hidden_all, exp_down[0], 3)], axis=0)
     returned = lax.all_to_all(
         expert_out.reshape(sp_count, slot_count // sp_count, col_width),
         "sp",

time: 219 us -> 215 us (0.982)
  blocking collectives: 87.4 us -> 90.4 us
  local copies, waits for them, and re-layouts: 12.8 us -> 10.3 us
  waiting for transfers between devices: 41 us -> 38.5 us
  starting transfers between devices: 29.6 us -> 27.2 us
    all_to_all x1 -> x0, starting transfers between devices: 10.2 us -> none  [body(): lax.all_to_all(w_parts, 'tp', split_axis=0, concat_axis=0, tiled=True)]
    all_to_all x1, waiting for transfers between devices: 10.9 us -> 17 us  [body(): lax.all_to_all(packed, 'tp', split_axis=0, concat_axis=0, tiled=True)]
    all_to_all x1 -> x0, waiting for transfers between devices: 5.36 us -> none  [body(): lax.all_to_all(w_parts, 'tp', split_axis=0, concat_axis=0, tiled=True)]
    all_to_all x1, starting transfers between devices: 3.46 us -> 8.64 us  [body(): lax.all_to_all(packed, 'tp', split_axis=0, concat_axis=0, tiled=True)]
    all_gather x1, waiting for transfers between devices: 7.03 us -> 4.23 us  [body(): hidden_all = lax.all_gather(hidden, 'tp')]
    ppermute x1, starting transfers between devices: 1.56 us -> 3.93 us  [body(): lax.ppermute((late_val * jax.nn.sigmoid(late_gate)).astype(BF16), 'sp', p...]
    unnamed x16 -> x18, local copies, waits for them, and re-layouts: 6.86 us -> 6.15 us
  transfers between devices with their start and end apart: 6 -> 5, of which waited for: 6 -> 5; matrix products, arithmetic and copies ran while one was open for 4% -> 3% of each run, Pallas kernels for 6% -> 5%
where the time goes in v5:
time: 215 us; the launch traced here: 214 us
  blocking collectives  90.4 us (42%)
  waiting for transfers between devices  38.5 us (18%)
  Pallas kernels  32.9 us (15%)
  starting transfers between devices  27.2 us (13%)
  between operations  13.5 us (6%)
  local copies, waits for them, and re-layouts  10.3 us (5%)
    all_gather x1, blocking collectives, body(): lax.all_gather(two, 'tp')  24.3 us
    all_gather x1, blocking collectives, body(): lax.all_gather(jnp.concatenate([landed[:first], middle], axis=0), 'tp')  22.4 us
    all_gather x1, blocking collectives, body(): lax.all_gather(one, 'tp')  22 us
    all_to_all x1, blocking collectives, body(): lax.all_to_all(expert_out.reshape(sp_count, slot_count // sp_count, col_w...  21.6 us
    all_to_all x1, waiting for transfers between devices, body(): lax.all_to_all(packed, 'tp', split_axis=0, concat_axis=0, tiled=True)  17 us
    all_to_all x1, starting transfers between devices, body(): lax.all_to_all(send.reshape(sp_count, slot_count // sp_count, col_width),...  14.5 us
    all_to_all x1, starting transfers between devices, body(): lax.all_to_all(packed, 'tp', split_axis=0, concat_axis=0, tiled=True)  8.64 us
    all_to_all x1, waiting for transfers between devices, body(): lax.all_to_all(send.reshape(sp_count, slot_count // sp_count, col_width),...  8.33 us
  transfers between devices with their start and end apart: 5, of which 5 were waited for; matrix products, arithmetic and copies ran while one was open for 3% of the time, Pallas kernels for 5%

profile of v5, /device:TPU:1, one launch (start us, length us, event | category | flops | bytes accessed | tf_op | source)
XLA Modules:
  0.0 214.4 jit_solution(8598298125614828327)
XLA Ops:
  6.5 0.0 copy-start
  6.5 0.0 copy-start.4
  6.5 0.9 copy.18.a_val
  7.4 0.0 copy-start.2
  7.4 0.8 copy.19.a_gate
  8.3 0.0 copy-start.3
  8.3 3.9 %collective-permute-start = (bf16[30,64]{1,0:T(8,128)(2,1)S(1)}, bf16[30,64]{1,0:T(8,128)(2,1)S(1)}, u32[]{:S(2)}, u32[]{:S(2)}) collective-permute-start(bf16[30,64]{1,0:T(8,128)(2,1)S(1)} %multiply_convert_fusion), channel_id=1, source_target_pairs={{0,16},{16,32},{32,48},{48,64},{64,80},{80,96},{96,112},{112,128},... | collective-permute-start | bytes 11528 | tf_op jit(solution)/shard_map/ppermute | solution.py:385
  12.3 0.8 collective-permute-done.before
  13.0 0.0 copy-start.6
  13.0 0.0 copy-done.2
  13.0 0.0 copy-done.3
  13.0 0.6 copy-done.6
  13.6 2.1 pack.1
  15.7 8.6 %all-to-all-start = ((bf16[16,176,128]{2,1,0:T(8,128)(2,1)}), bf16[16,176,128]{2,1,0:T(8,128)(2,1)S(1)}, u32[]{:S(2)}, u32[]{:S(2)}) async-start(bf16[16,176,128]{2,1,0:T(8,128)(2,1)} %pack.1), calls=%async_computation | async-start | bytes 1441792 | tf_op jit(solution)/shard_map/all_to_all | solution.py:389
  24.4 1.4 copy.22.refs_0_
  25.8 2.3 %routing.1 = (s32[128,4]{1,0:T(8,128)}, bf16[1024,128]{1,0:T(8,128)(2,1)}) custom-call(s32[128,4]{1,0:T(8,128)} %copy.22.refs_0_), custom_call_target="tpu_custom_call" | custom-call | tf_op jit(solution)/shard_map/routing/pallas_call | solution.py:105
  28.0 0.0 copy-done
  28.0 0.6 constant_dynamic-slice_fusion.refs_1_
  28.7 17.0 %all-to-all-done.refs_0_ = bf16[16,176,128]{2,1,0:T(8,128)(2,1)S(1)} async-done(((bf16[16,176,128]{2,1,0:T(8,128)(2,1)}), bf16[16,176,128]{2,1,0:T(8,128)(2,1)S(1)}, u32[]{:S(2)}, u32[]{:S(2)}) %all-to-all-start) | async-done | bytes 720928 | tf_op jit(solution)/shard_map/all_to_all | solution.py:389
  45.7 0.0 copy-start.1
  45.7 0.9 copy-done.1
  46.6 5.4 %front.1 = (bf16[128,128]{1,0:T(8,128)(2,1)}, bf16[1024,128]{1,0:T(8,128)(2,1)}) custom-call(bf16[16,176,128]{2,1,0:T(8,128)(2,1)} %copy-done.1, bf16[128,128]{1,0:T(8,128)(2,1)} %constant_dynamic-slice_fusion.refs_1_, bf16[1024,128]{1,0:T(8,128)(2,1)} %get-tuple-element.23.refs_2_), custom_call_target="tpu_custom_call" | custom-call | tf_op jit(solution)/shard_map/front/pallas_call | solution.py:189
  52.0 14.5 %all-to-all-start.1 = ((bf16[32,32,128]{2,1,0:T(8,128)(2,1)}), bf16[32,32,128]{2,1,0:T(8,128)(2,1)S(1)}, u32[]{:S(2)}, u32[]{:S(2)}) async-start(bf16[32,32,128]{2,1,0:T(8,128)(2,1)} %bitcast.31), calls=%async_computation.1 | async-start | bytes 524288 | tf_op jit(solution)/shard_map/all_to_all | solution.py:397
  66.5 0.0 all-gather.8.cloned.1.call-start
  66.5 1.4 copy.23.weights
  67.9 2.4 %table.1 = bf16[3,128,1024]{2,1,0:T(8,128)(2,1)} custom-call(s32[128,4]{1,0:T(8,128)} %get-tuple-element.26.slots, f32[128,4]{1,0:T(8,128)} %copy.23.weights), custom_call_target="tpu_custom_call" | custom-call | tf_op jit(solution)/shard_map/table/pallas_call | solution.py:128
  70.3 8.3 %all-to-all-done.1 = bf16[32,32,128]{2,1,0:T(8,128)(2,1)S(1)} async-done(((bf16[32,32,128]{2,1,0:T(8,128)(2,1)}), bf16[32,32,128]{2,1,0:T(8,128)(2,1)S(1)}, u32[]{:S(2)}, u32[]{:S(2)}) %all-to-all-start.1) | async-done | bytes 262176 | tf_op jit(solution)/shard_map/all_to_all | solution.py:397
  78.6 0.7 slice.16
  79.3 0.0 all-gather.8.cloned.1.call-update
  79.4 0.0 all-gather.10.cloned.1.call-start
  79.4 1.9 copy.24.sg
  81.3 0.0 copy-done.4
  81.3 1.0 copy.25.su
  82.3 0.8 pad_maximum_fusion.1
  83.1 22.4 %all-gather.1 = bf16[3584,128]{1,0:T(8,128)(2,1)} all-gather(bf16[224,128]{1,0:T(8,128)(2,1)S(1)} %pad_maximum_fusion.1), channel_id=3, replica_groups=mesh['sp'=32,'tp'=16] {'tp'}, dimensions={0}, use_global_device_ids=true | all-gather | bytes 974848 | tf_op jit(solution)/shard_map/all_gather | solution.py:411
  105.5 3.7 %side_hidden.1 = bf16[112,256]{1,0:T(8,128)(2,1)} custom-call(bf16[16,224,128]{2,1,0:T(8,128)(2,1)} %bitcast.26, f32[1,2048]{1,0:T(1,128)} %bitcast.32, bf16[2048,256]{1,0:T(8,128)(2,1)} %bitcast.19, bf16[2048,256]{1,0:T(8,128)(2,1)} %bitcast.21, bf16[2048,32]{1,0:T(8,128)(2,1)} %copy.24.sg, bf16[2048,32]{1,0:T(8,128)(2,1)} %copy.25.su), custom_call_target="tpu_custom_call" | custom-call | tf_op jit(solution)/shard_map/side_hidden/pallas_call | solution.py:276
  109.2 8.0 %all-gather.8.cloned.1.call-done = bf16[14848,128]{1,0:T(8,128)(2,1)} async-done(((bf16[928,128]{1,0:T(8,128)(2,1)}), bf16[14848,128]{1,0:T(8,128)(2,1)}) %all-gather.8.cloned.1.call-update) | async-done | bytes 3801104 | tf_op jit(solution)/shard_map/all_gather | solution.py:410
  117.3 5.9 %hidden.1 = (bf16[112,256]{1,0:T(8,128)(2,1)}, bf16[816,256]{1,0:T(8,128)(2,1)}) custom-call(bf16[16,928,128]{2,1,0:T(8,128)(2,1)} %bitcast.23, f32[1,2048]{1,0:T(1,128)} %bitcast.33, bf16[2048,256]{1,0:T(8,128)(2,1)} %bitcast.20, bf16[2048,256]{1,0:T(8,128)(2,1)} %bitcast.22), custom_call_target="tpu_custom_call" | custom-call | tf_op jit(solution)/shard_map/hidden/pallas_call | solution.py:242
  123.2 0.0 all-gather.10.cloned.1.call-update
  123.2 22.0 %all-gather.3 = bf16[1792,256]{1,0:T(8,128)(2,1)} all-gather(bf16[112,256]{1,0:T(8,128)(2,1)} %side_hidden.1), channel_id=5, replica_groups=mesh['sp'=32,'tp'=16] {'tp'}, dimensions={0}, use_global_device_ids=true | all-gather | bytes 974848 | tf_op jit(solution)/shard_map/all_gather | solution.py:419
  145.3 24.3 %all-gather.4 = bf16[1792,256]{1,0:T(8,128)(2,1)} all-gather(bf16[112,256]{1,0:T(8,128)(2,1)} %get-tuple-element.35), channel_id=6, replica_groups=mesh['sp'=32,'tp'=16] {'tp'}, dimensions={0}, use_global_device_ids=true | all-gather | bytes 974848 | tf_op jit(solution)/shard_map/all_gather | solution.py:419
  169.6 3.3 %side_down.1 = (bf16[208,128]{1,0:T(8,128)(2,1)}, f32[128,128]{1,0:T(8,128)}) custom-call(bf16[16,112,256]{2,1,0:T(8,128)(2,1)} %bitcast.24, bf16[16,112,256]{2,1,0:T(8,128)(2,1)} %bitcast.25, bf16[4096,128]{1,0:T(8,128)(2,1)} %bitcast.17, bf16[512,128]{1,0:T(8,128)(2,1)} %sh_down.1), custom_call_target="tpu_custom_call" | custom-call | tf_op jit(solution)/shard_map/side_down/pallas_call | solution.py:305
  172.9 4.2 %all-gather.10.cloned.1.call-done = bf16[13056,256]{1,0:T(8,128)(2,1)} async-done(((bf16[816,256]{1,0:T(8,128)(2,1)}), bf16[13056,256]{1,0:T(8,128)(2,1)}) %all-gather.10.cloned.1.call-update) | async-done | bytes 6684688 | tf_op jit(solution)/shard_map/all_gather | solution.py:416
  177.2 5.7 %down.1 = bf16[816,128]{1,0:T(8,128)(2,1)} custom-call(bf16[16,816,256]{2,1,0:T(8,128)(2,1)} %bitcast.16, bf16[4096,128]{1,0:T(8,128)(2,1)} %bitcast.18), custom_call_target="tpu_custom_call" | custom-call | tf_op jit(solution)/shard_map/down/pallas_call | solution.py:323
  182.8 0.0 copy-done.5
  182.8 0.9 pad_maximum_fusion
  183.8 21.6 %all_to_all.15 = bf16[32,32,128]{2,1,0:T(8,128)(2,1)} all-to-all(bf16[32,32,128]{2,1,0:T(8,128)(2,1)S(1)} %bitcast.29), channel_id=1, replica_groups=mesh['sp'=32,'tp'=16] {'sp'}, dimensions={0} | all-to-all | bytes 524288 | tf_op jit(solution)/shard_map/all_to_all | solution.py:423
  205.4 2.2 %combine.1 = bf16[128,128]{1,0:T(8,128)(2,1)} custom-call(bf16[1024,128]{1,0:T(8,128)(2,1)} %bitcast.30, bf16[3,128,1024]{2,1,0:T(8,128)(2,1)} %table.1, bf16[128,128]{1,0:T(8,128)(2,1)} %get-tuple-element.29.middle, f32[128,128]{1,0:T(8,128)} %get-tuple-element.40.shared), custom_call_target="tpu_custom_call" | custom-call | tf_op jit(solution)/shard_map/combine/pallas_call | solution.py:345
  (3 shorter events, 0.0 us)
Async XLA Ops:
  6.5 21.5 %copy-start = (bf16[128,2048]{1,0:T(8,128)(2,1)S(1)}, bf16[128,2048]{1,0:T(8,128)(2,1)}, u32[]{:S(2)}) copy-start(bf16[128,2048]{1,0:T(8,128)(2,1)} %param.17) | copy-start | bytes 1572868
  6.5 74.8 %copy-start.4 = (bf16[2048,32]{0,1:T(8,128)(2,1)S(1)}, bf16[2048,32]{0,1:T(8,128)(2,1)}, u32[]{:S(2)}) copy-start(bf16[2048,32]{0,1:T(8,128)(2,1)} %param.32) | copy-start | bytes 393220
  7.4 5.6 %copy-start.2 = (bf16[128,64]{1,0:T(8,128)(2,1)}, bf16[128,64]{1,0:T(8,128)(2,1)S(1)}, u32[]{:S(2)}) copy-start(bf16[128,64]{1,0:T(8,128)(2,1)S(1)} %copy.18.a_val) | copy-start | bytes 49156
  8.3 4.8 %copy-start.3 = (bf16[128,64]{1,0:T(8,128)(2,1)}, bf16[128,64]{1,0:T(8,128)(2,1)S(1)}, u32[]{:S(2)}) copy-start(bf16[128,64]{1,0:T(8,128)(2,1)S(1)} %copy.19.a_gate) | copy-start | bytes 49156
  8.3 4.7 %collective-permute-start = (bf16[30,64]{1,0:T(8,128)(2,1)S(1)}, bf16[30,64]{1,0:T(8,128)(2,1)S(1)}, u32[]{:S(2)}, u32[]{:S(2)}) collective-permute-start(bf16[30,64]{1,0:T(8,128)(2,1)S(1)} %multiply_convert_fusion), channel_id=1, source_target_pairs={{0,16},{16,32},{32,48},{48,64},{64,80},{80,96},{96,112},{112,128},... | collective-permute-start | bytes 11528 | tf_op jit(solution)/shard_map/ppermute | solution.py:385
  13.0 0.6 copy-start.6
  15.7 30.0 %all-to-all-start = ((bf16[16,176,128]{2,1,0:T(8,128)(2,1)}), bf16[16,176,128]{2,1,0:T(8,128)(2,1)S(1)}, u32[]{:S(2)}, u32[]{:S(2)}) async-start(bf16[16,176,128]{2,1,0:T(8,128)(2,1)} %pack.1), calls=%async_computation | async-start | bytes 1441792 | tf_op jit(solution)/shard_map/all_to_all | solution.py:389
  45.7 0.9 copy-start.1
  52.0 26.7 %all-to-all-start.1 = ((bf16[32,32,128]{2,1,0:T(8,128)(2,1)}), bf16[32,32,128]{2,1,0:T(8,128)(2,1)S(1)}, u32[]{:S(2)}, u32[]{:S(2)}) async-start(bf16[32,32,128]{2,1,0:T(8,128)(2,1)} %bitcast.31), calls=%async_computation.1 | async-start | bytes 524288 | tf_op jit(solution)/shard_map/all_to_all | solution.py:397
  66.5 50.8 %all-gather.8.cloned.1.call-start = ((), (), s32[]{:S(2)}) async-start(), calls=%async_computation.3 | async-start | bytes 4038656 | tf_op jit(solution)/shard_map/all_gather | solution.py:410
  79.4 97.8 %all-gather.10.cloned.1.call-start = ((), (), s32[]{:S(2)}) async-start(), calls=%async_computation.4 | async-start | bytes 7102464 | tf_op jit(solution)/shard_map/all_gather | solution.py:416
  172.9 9.9 %copy-start.5 = (bf16[208,128]{1,0:T(8,128)(2,1)S(1)}, bf16[208,128]{1,0:T(8,128)(2,1)}, u32[]{:S(2)}) copy-start(bf16[208,128]{1,0:T(8,128)(2,1)} %get-tuple-element.37) | copy-start | bytes 159748
Sparse Core Ops, SparseCore 0:
  79.5 37.7 all-gather.7
  123.4 53.7 all-gather.9

commit v6 on v5

--- a/solution.py
+++ b/solution.py
@@ -12,19 +12,26 @@
 BF16 = jnp.bfloat16
 
 
+def near(v):
+    return pltpu.with_memory_space_constraint(v, pltpu.VMEM)
+
+
 def silu(v):
     return v / (1.0 + jnp.exp(-v))
 
 
-def pack_kernel(before, a_val, a_gate, taps, bias, gain, shift, w_out, out, win, params):
+def pack_kernel(before, a_val, a_gate, taps, bias, gain, shift, w_out, out, win, params, wide):
     peers, _, lanes = out.shape
-    halo, half = before.shape
+    half, halo = before.shape
+    tok_rows = a_val.shape[1]
     rows = win.shape[0]
     win[...] = jnp.zeros(win.shape, F32)
     params[...] = jnp.zeros(params.shape, F32)
     gate = 1.0 / (1.0 + jnp.exp(-a_gate[...].astype(F32)))
-    win[0:halo, :] = before[...].astype(F32)
-    win[halo : halo + a_val.shape[0], :] = a_val[...].astype(F32) * gate
+    wide[...] = jnp.zeros(wide.shape, F32)
+    wide[:, 0:halo] = before[...].astype(F32)
+    win[0:halo, :] = wide[...].T[0:halo, :]
+    win[halo : halo + tok_rows, :] = (a_val[...].astype(F32) * gate).T
     span = taps.shape[0]
     params[0:span, :] = taps[...].astype(F32)
     for n, vector in enumerate((bias, gain, shift)):
@@ -58,18 +65,20 @@
 
 
 def pack(before, a_val, a_gate, taps, bias, gain, shift, w_out, peers):
-    rows = window_rows(taps.shape[0], a_val.shape[0])
+    half, tok_rows = a_val.shape
+    rows = window_rows(taps.shape[0], tok_rows)
     lanes = w_out.shape[1] // peers
     total = rows // 2 + PARAM_ROWS // 2 + w_out.shape[0]
     return pl.pallas_call(
         pack_kernel,
         out_shape=jax.ShapeDtypeStruct((peers, total, lanes), BF16),
         scratch_shapes=[
-            pltpu.VMEM((rows, a_val.shape[1]), F32),
-            pltpu.VMEM((PARAM_ROWS, a_val.shape[1]), F32),
+            pltpu.VMEM((rows, half), F32),
+            pltpu.VMEM((PARAM_ROWS, half), F32),
+            pltpu.VMEM((half, LANES), F32),
         ],
         name="pack",
-    )(before, a_val, a_gate, taps, bias, gain, shift, w_out)
+    )(near(before), a_val, a_gate, taps, bias, gain, shift, near(w_out))
 
 
 def routing_kernel(capacity, routes, slots_out, pick_out):
@@ -198,7 +207,7 @@
             pltpu.VMEM((tok_rows, channels), F32),
         ],
         name="front",
-    )(packed, resid, pick)
+    )(near(packed), resid, near(pick))
 
 
 def normed_rows(pieces, width, gain):
@@ -245,8 +254,8 @@
         in_specs=[
             pl.BlockSpec((pieces, block, lanes), lambda i: (0, i, 0)),
             pl.BlockSpec((1, width), lambda i: (0, 0)),
-            pl.BlockSpec((width, units), lambda i: (0, 0)),
-            pl.BlockSpec((width, units), lambda i: (0, 0)),
+            pl.BlockSpec(memory_space=pltpu.VMEM),
+            pl.BlockSpec(memory_space=pltpu.VMEM),
         ],
         out_specs=[
             pl.BlockSpec((aside, units), lambda i: (0, 0)),
@@ -257,7 +266,7 @@
             jax.ShapeDtypeStruct((rows - aside, units), BF16),
         ),
         name="hidden",
-    )(rows_in, gain, wg, wu)
+    )(rows_in, gain, near(wg), near(wu))
 
 
 def side_hidden_kernel(one, gain, wg, wu, sg, su, out):
@@ -325,12 +334,12 @@
         grid=(blocks,),
         in_specs=[
             pl.BlockSpec((pieces, block, units), lambda i: (0, i, 0)),
-            pl.BlockSpec(wd.shape, lambda i: (0, 0)),
+            pl.BlockSpec(memory_space=pltpu.VMEM),
         ],
         out_specs=pl.BlockSpec((block, wd.shape[1]), lambda i: (i, 0)),
         out_shape=jax.ShapeDtypeStruct((rows, wd.shape[1]), BF16),
         name="down",
-    )(hidden, wd)
+    )(hidden, near(wd))
 
 
 def combine_kernel(returned, table, middle, shared, out):
@@ -346,7 +355,7 @@
         combine_kernel,
         out_shape=jax.ShapeDtypeStruct(middle.shape, BF16),
         name="combine",
-    )(returned, table, middle, shared)
+    )(near(returned), near(table), middle, shared)
 
 
 def body(
@@ -385,7 +394,7 @@
     before = lax.ppermute((late_val * jax.nn.sigmoid(late_gate)).astype(BF16), "sp", pairs)
 
     vectors = [v[None, :] for v in (conv_bias, ln_gain, ln_bias)]
-    packed = pack(before, a_val, a_gate, conv_kernel, *vectors, w_out, tp_count)
+    packed = pack(before.T, a_val.T, a_gate.T, conv_kernel, *vectors, w_out, tp_count)
     spread = lax.all_to_all(packed, "tp", split_axis=0, concat_axis=0, tiled=True)
 
     routes_late, _ = lax.optimization_barrier((routes, packed[0, :1]))

time: 215 us -> 214 us (level)
    unnamed x18 -> x20, local copies, waits for them, and re-layouts: 6.15 us -> 6.05 us
where the time goes in v6:
time: 214 us
  blocking collectives  90.5 us (42%)
  waiting for transfers between devices  38.4 us (18%)
  Pallas kernels  31 us (14%)
  starting transfers between devices  27.3 us (13%)
  between operations  13.5 us (6%)
  local copies, waits for them, and re-layouts  10.2 us (5%)
  other arithmetic  2.65 us (1%)
    all_gather x1, blocking collectives, body(): lax.all_gather(two, 'tp')  24.5 us
    all_gather x1, blocking collectives, body(): lax.all_gather(jnp.concatenate([landed[:first], middle], axis=0), 'tp')  22.4 us
    all_gather x1, blocking collectives, body(): lax.all_gather(one, 'tp')  22.2 us
    all_to_all x1, blocking collectives, body(): lax.all_to_all(expert_out.reshape(sp_count, slot_count // sp_count, col_w...  21.4 us
    all_to_all x1, waiting for transfers between devices, body(): lax.all_to_all(packed, 'tp', split_axis=0, concat_axis=0, tiled=True)  17.1 us
    all_to_all x1, starting transfers between devices, body(): lax.all_to_all(send.reshape(sp_count, slot_count // sp_count, col_width),...  14.6 us
    all_to_all x1, starting transfers between devices, body(): lax.all_to_all(packed, 'tp', split_axis=0, concat_axis=0, tiled=True)  8.64 us
    all_to_all x1, waiting for transfers between devices, body(): lax.all_to_all(send.reshape(sp_count, slot_count // sp_count, col_width),...  8.33 us
  transfers between devices with their start and end apart: 5, of which 5 were waited for; matrix products, arithmetic and copies ran while one was open for 3% of the time, Pallas kernels for 5%

profile of v6, /device:TPU:1, one launch (start us, length us, event | category | flops | bytes accessed | tf_op | source)
XLA Modules:
  0.0 213.5 jit_solution(12192070721197181688)
XLA Ops:
  6.5 0.0 copy-start
  6.5 0.0 copy-start.3
  6.5 0.9 multiply_convert_fusion
  7.5 3.9 %collective-permute-start = (bf16[30,64]{0,1:T(8,128)(2,1)S(1)}, bf16[30,64]{0,1:T(8,128)(2,1)S(1)}, u32[]{:S(2)}, u32[]{:S(2)}) collective-permute-start(bf16[30,64]{0,1:T(8,128)(2,1)S(1)} %multiply_convert_fusion), channel_id=1, source_target_pairs={{0,16},{16,32},{32,48},{48,64},{64,80},{80,96},{96,112},{112,128},... | collective-permute-start | bytes 11528 | tf_op jit(solution)/shard_map/ppermute | solution.py:394
  11.4 0.9 collective-permute-done
  12.3 0.0 copy-start.5
  12.3 0.9 copy-done.5
  13.2 0.0 copy-start.7
  13.2 1.9 pack.1
  15.1 8.6 %all-to-all-start = ((bf16[16,176,128]{2,1,0:T(8,128)(2,1)}), bf16[16,176,128]{2,1,0:T(8,128)(2,1)S(1)}, u32[]{:S(2)}, u32[]{:S(2)}) async-start(bf16[16,176,128]{2,1,0:T(8,128)(2,1)} %pack.1), calls=%async_computation | async-start | bytes 1441792 | tf_op jit(solution)/shard_map/all_to_all | solution.py:398
  23.8 1.4 copy.18.refs_0_
  25.2 2.2 %routing.1 = (s32[128,4]{1,0:T(8,128)}, bf16[1024,128]{1,0:T(8,128)(2,1)}) custom-call(s32[128,4]{1,0:T(8,128)} %copy.18.refs_0_), custom_call_target="tpu_custom_call" | custom-call | tf_op jit(solution)/shard_map/routing/pallas_call | solution.py:114
  27.4 0.0 copy-done
  27.4 0.6 constant_dynamic-slice_fusion.refs_1_
  28.0 17.1 %all-to-all-done.refs_0_ = bf16[16,176,128]{2,1,0:T(8,128)(2,1)S(1)} async-done(((bf16[16,176,128]{2,1,0:T(8,128)(2,1)}), bf16[16,176,128]{2,1,0:T(8,128)(2,1)S(1)}, u32[]{:S(2)}, u32[]{:S(2)}) %all-to-all-start) | async-done | bytes 720928 | tf_op jit(solution)/shard_map/all_to_all | solution.py:398
  45.1 0.0 copy-start.6
  45.1 0.9 copy-done.6
  46.0 4.9 %front.1 = (bf16[128,128]{1,0:T(8,128)(2,1)}, bf16[1024,128]{1,0:T(8,128)(2,1)}) custom-call(bf16[16,176,128]{2,1,0:T(8,128)(2,1)S(1)} %all-to-all-done.refs_0_, bf16[128,128]{1,0:T(8,128)(2,1)} %constant_dynamic-slice_fusion.refs_1_, bf16[1024,128]{1,0:T(8,128)(2,1)S(1)} %copy-done.6), custom_call_target="tpu_custom_call" | custom-call | tf_op jit(solution)/shard_map/front/pallas_call | solution.py:198
  51.0 14.6 %all-to-all-start.1 = ((bf16[32,32,128]{2,1,0:T(8,128)(2,1)}), bf16[32,32,128]{2,1,0:T(8,128)(2,1)S(1)}, u32[]{:S(2)}, u32[]{:S(2)}) async-start(bf16[32,32,128]{2,1,0:T(8,128)(2,1)} %bitcast.35), calls=%async_computation.1 | async-start | bytes 524288 | tf_op jit(solution)/shard_map/all_to_all | solution.py:406
  65.6 0.0 all-gather.8.cloned.1.call-start
  65.7 1.4 copy.19.weights
  67.1 2.3 %table.1 = bf16[3,128,1024]{2,1,0:T(8,128)(2,1)} custom-call(s32[128,4]{1,0:T(8,128)} %get-tuple-element.26.slots, f32[128,4]{1,0:T(8,128)} %copy.19.weights), custom_call_target="tpu_custom_call" | custom-call | tf_op jit(solution)/shard_map/table/pallas_call | solution.py:137
  69.4 8.3 %all-to-all-done.1 = bf16[32,32,128]{2,1,0:T(8,128)(2,1)S(1)} async-done(((bf16[32,32,128]{2,1,0:T(8,128)(2,1)}), bf16[32,32,128]{2,1,0:T(8,128)(2,1)S(1)}, u32[]{:S(2)}, u32[]{:S(2)}) %all-to-all-start.1) | async-done | bytes 262176 | tf_op jit(solution)/shard_map/all_to_all | solution.py:406
  77.8 0.7 slice.16
  78.5 0.0 all-gather.8.cloned.1.call-update
  78.5 0.0 all-gather.10.cloned.1.call-start
  78.5 1.9 copy.20.sg
  80.4 0.0 copy-done.7
  80.4 1.0 copy.21.su
  81.4 0.8 pad_maximum_fusion.1
  82.2 22.4 %all-gather.1 = bf16[3584,128]{1,0:T(8,128)(2,1)} all-gather(bf16[224,128]{1,0:T(8,128)(2,1)S(1)} %pad_maximum_fusion.1), channel_id=3, replica_groups=mesh['sp'=32,'tp'=16] {'tp'}, dimensions={0}, use_global_device_ids=true | all-gather | bytes 974848 | tf_op jit(solution)/shard_map/all_gather | solution.py:420
  104.6 3.7 %side_hidden.1 = bf16[112,256]{1,0:T(8,128)(2,1)} custom-call(bf16[16,224,128]{2,1,0:T(8,128)(2,1)} %bitcast.31, f32[1,2048]{1,0:T(1,128)} %bitcast.38, bf16[2048,256]{1,0:T(8,128)(2,1)} %bitcast.21, bf16[2048,256]{1,0:T(8,128)(2,1)} %bitcast.23, bf16[2048,32]{1,0:T(8,128)(2,1)} %copy.20.sg, bf16[2048,32]{1,0:T(8,128)(2,1)} %copy.21.su), custom_call_target="tpu_custom_call" | custom-call | tf_op jit(solution)/shard_map/side_hidden/pallas_call | solution.py:285
  108.4 8.0 %all-gather.8.cloned.1.call-done = bf16[14848,128]{1,0:T(8,128)(2,1)} async-done(((bf16[928,128]{1,0:T(8,128)(2,1)}), bf16[14848,128]{1,0:T(8,128)(2,1)}) %all-gather.8.cloned.1.call-update) | async-done | bytes 3801104 | tf_op jit(solution)/shard_map/all_gather | solution.py:419
  116.3 0.0 copy-done.3
  116.3 0.0 copy-done.2
  116.3 5.3 %hidden.1 = (bf16[112,256]{1,0:T(8,128)(2,1)}, bf16[816,256]{1,0:T(8,128)(2,1)}) custom-call(bf16[16,928,128]{2,1,0:T(8,128)(2,1)} %bitcast.28, f32[1,2048]{1,0:T(1,128)} %bitcast.39, bf16[2048,256]{1,0:T(8,128)(2,1)S(1)} %bitcast.22, bf16[2048,256]{1,0:T(8,128)(2,1)S(1)} %bitcast.24), custom_call_target="tpu_custom_call" | custom-call | tf_op jit(solution)/shard_map/hidden/pallas_call | solution.py:251
  121.6 0.0 all-gather.10.cloned.1.call-update
  121.7 22.2 %all-gather.3 = bf16[1792,256]{1,0:T(8,128)(2,1)} all-gather(bf16[112,256]{1,0:T(8,128)(2,1)} %side_hidden.1), channel_id=5, replica_groups=mesh['sp'=32,'tp'=16] {'tp'}, dimensions={0}, use_global_device_ids=true | all-gather | bytes 974848 | tf_op jit(solution)/shard_map/all_gather | solution.py:428
  143.9 24.5 %all-gather.4 = bf16[1792,256]{1,0:T(8,128)(2,1)} all-gather(bf16[112,256]{1,0:T(8,128)(2,1)} %get-tuple-element.35), channel_id=6, replica_groups=mesh['sp'=32,'tp'=16] {'tp'}, dimensions={0}, use_global_device_ids=true | all-gather | bytes 974848 | tf_op jit(solution)/shard_map/all_gather | solution.py:428
  168.4 3.3 %side_down.1 = (bf16[208,128]{1,0:T(8,128)(2,1)}, f32[128,128]{1,0:T(8,128)}) custom-call(bf16[16,112,256]{2,1,0:T(8,128)(2,1)} %bitcast.29, bf16[16,112,256]{2,1,0:T(8,128)(2,1)} %bitcast.30, bf16[4096,128]{1,0:T(8,128)(2,1)} %bitcast.19, bf16[512,128]{1,0:T(8,128)(2,1)} %sh_down.1), custom_call_target="tpu_custom_call" | custom-call | tf_op jit(solution)/shard_map/side_down/pallas_call | solution.py:314
  171.7 4.2 %all-gather.10.cloned.1.call-done = bf16[13056,256]{1,0:T(8,128)(2,1)} async-done(((bf16[816,256]{1,0:T(8,128)(2,1)}), bf16[13056,256]{1,0:T(8,128)(2,1)}) %all-gather.10.cloned.1.call-update) | async-done | bytes 6684688 | tf_op jit(solution)/shard_map/all_gather | solution.py:425
  175.9 1.2 copy-done.1
  177.1 5.4 %down.1 = bf16[816,128]{1,0:T(8,128)(2,1)} custom-call(bf16[16,816,256]{2,1,0:T(8,128)(2,1)} %bitcast.27, bf16[4096,128]{1,0:T(8,128)(2,1)S(1)} %bitcast.20), custom_call_target="tpu_custom_call" | custom-call | tf_op jit(solution)/shard_map/down/pallas_call | solution.py:332
  182.5 0.0 copy-done.8
  182.5 0.9 pad_maximum_fusion
  183.5 21.4 %all_to_all.15 = bf16[32,32,128]{2,1,0:T(8,128)(2,1)S(1)} all-to-all(bf16[32,32,128]{2,1,0:T(8,128)(2,1)S(1)} %bitcast.34), channel_id=1, replica_groups=mesh['sp'=32,'tp'=16] {'sp'}, dimensions={0} | all-to-all | bytes 524288 | tf_op jit(solution)/shard_map/all_to_all | solution.py:432
  204.9 0.0 copy-done.4
  204.9 1.8 combine.1
  (5 shorter events, 0.0 us)
Async XLA Ops:
  6.5 20.9 %copy-start = (bf16[128,2048]{1,0:T(8,128)(2,1)S(1)}, bf16[128,2048]{1,0:T(8,128)(2,1)}, u32[]{:S(2)}) copy-start(bf16[128,2048]{1,0:T(8,128)(2,1)} %param.17) | copy-start | bytes 1572868
  6.5 109.8 %copy-start.3 = (bf16[1,2048,256]{2,1,0:T(8,128)(2,1)S(1)}, bf16[1,2048,256]{2,1,0:T(8,128)(2,1)}, u32[]{:S(2)}) copy-start(bf16[1,2048,256]{2,1,0:T(8,128)(2,1)} %param.29) | copy-start | bytes 3145732
  7.5 4.8 %collective-permute-start = (bf16[30,64]{0,1:T(8,128)(2,1)S(1)}, bf16[30,64]{0,1:T(8,128)(2,1)S(1)}, u32[]{:S(2)}, u32[]{:S(2)}) collective-permute-start(bf16[30,64]{0,1:T(8,128)(2,1)S(1)} %multiply_convert_fusion), channel_id=1, source_target_pairs={{0,16},{16,32},{32,48},{48,64},{64,80},{80,96},{96,112},{112,128},... | collective-permute-start | bytes 11528 | tf_op jit(solution)/shard_map/ppermute | solution.py:394
  12.3 0.9 copy-start.5
  13.2 67.2 %copy-start.7 = (bf16[2048,32]{0,1:T(8,128)(2,1)S(1)}, bf16[2048,32]{0,1:T(8,128)(2,1)}, u32[]{:S(2)}) copy-start(bf16[2048,32]{0,1:T(8,128)(2,1)} %param.32) | copy-start | bytes 393220
  15.1 30.0 %all-to-all-start = ((bf16[16,176,128]{2,1,0:T(8,128)(2,1)}), bf16[16,176,128]{2,1,0:T(8,128)(2,1)S(1)}, u32[]{:S(2)}, u32[]{:S(2)}) async-start(bf16[16,176,128]{2,1,0:T(8,128)(2,1)} %pack.1), calls=%async_computation | async-start | bytes 1441792 | tf_op jit(solution)/shard_map/all_to_all | solution.py:398
  45.1 1.0 copy-start.6
  51.0 65.3 %copy-start.2 = (bf16[1,2048,256]{2,1,0:T(8,128)(2,1)S(1)}, bf16[1,2048,256]{2,1,0:T(8,128)(2,1)}, u32[]{:S(2)}) copy-start(bf16[1,2048,256]{2,1,0:T(8,128)(2,1)} %param.28) | copy-start | bytes 3145732
  51.0 26.8 %all-to-all-start.1 = ((bf16[32,32,128]{2,1,0:T(8,128)(2,1)}), bf16[32,32,128]{2,1,0:T(8,128)(2,1)S(1)}, u32[]{:S(2)}, u32[]{:S(2)}) async-start(bf16[32,32,128]{2,1,0:T(8,128)(2,1)} %bitcast.35), calls=%async_computation.1 | async-start | bytes 524288 | tf_op jit(solution)/shard_map/all_to_all | solution.py:406
  65.6 50.7 %all-gather.8.cloned.1.call-start = ((), (), s32[]{:S(2)}) async-start(), calls=%async_computation.3 | async-start | bytes 4038656 | tf_op jit(solution)/shard_map/all_gather | solution.py:419
  78.5 97.4 %all-gather.10.cloned.1.call-start = ((), (), s32[]{:S(2)}) async-start(), calls=%async_computation.4 | async-start | bytes 7102464 | tf_op jit(solution)/shard_map/all_gather | solution.py:425
  143.9 61.0 %copy-start.4 = (bf16[3,128,1024]{2,1,0:T(8,128)(2,1)S(1)}, bf16[3,128,1024]{2,1,0:T(8,128)(2,1)}, u32[]{:S(2)}) copy-start(bf16[3,128,1024]{2,1,0:T(8,128)(2,1)} %table.1) | copy-start | bytes 2359300
  175.9 1.2 copy-start.1
  177.1 5.4 %copy-start.8 = (bf16[208,128]{1,0:T(8,128)(2,1)S(1)}, bf16[208,128]{1,0:T(8,128)(2,1)}, u32[]{:S(2)}) copy-start(bf16[208,128]{1,0:T(8,128)(2,1)} %get-tuple-element.37) | copy-start | bytes 159748
Sparse Core Ops, SparseCore 0:
  78.6 37.6 all-gather.7
  121.8 54.0 all-gather.9

commit v7 on v6

--- a/solution.py
+++ b/solution.py
@@ -207,7 +207,7 @@
             pltpu.VMEM((tok_rows, channels), F32),
         ],
         name="front",
-    )(near(packed), resid, near(pick))
+    )(near(packed), resid, pick)
 
 
 def normed_rows(pieces, width, gain):
@@ -321,25 +321,41 @@
     )(one, two, wd, sh_down)
 
 
-def down_kernel(hidden, wd, out):
-    whole = jnp.concatenate([hidden[t] for t in range(hidden.shape[0])], axis=1)
-    out[...] = jnp.dot(whole, wd[...], preferred_element_type=F32).astype(BF16)
-
-
-def down(hidden, wd, blocks):
+def down_kernel(hidden, wd, aside, out, total):
+    step = pl.program_id(0)
+    pair = jnp.concatenate([hidden[n] for n in range(hidden.shape[0])], axis=1)
+    part = jnp.dot(pair, wd[...], preferred_element_type=F32)
+
+    @pl.when(step == 0)
+    def _():
+        out[0 : aside.shape[0], :] = aside[...]
+        total[...] = part
+
+    @pl.when(step > 0)
+    def _():
+        total[...] = total[...] + part
+
+    @pl.when(step == pl.num_programs(0) - 1)
+    def _():
+        out[aside.shape[0] :, :] = total[...].astype(BF16)
+
+
+def down(hidden, wd, aside):
     pieces, rows, units = hidden.shape
-    block = rows // blocks
+    cols = wd.shape[1]
     return pl.pallas_call(
         down_kernel,
-        grid=(blocks,),
+        grid=(pieces // 2,),
         in_specs=[
-            pl.BlockSpec((pieces, block, units), lambda i: (0, i, 0)),
-            pl.BlockSpec(memory_space=pltpu.VMEM),
+            pl.BlockSpec((2, rows, units), lambda i: (i, 0, 0)),
+            pl.BlockSpec((2 * units, cols), lambda i: (i, 0)),
+            pl.BlockSpec(aside.shape, lambda i: (0, 0)),
         ],
-        out_specs=pl.BlockSpec((block, wd.shape[1]), lambda i: (i, 0)),
-        out_shape=jax.ShapeDtypeStruct((rows, wd.shape[1]), BF16),
+        out_specs=pl.BlockSpec((aside.shape[0] + rows, cols), lambda i: (0, 0)),
+        out_shape=jax.ShapeDtypeStruct((aside.shape[0] + rows, cols), BF16),
+        scratch_shapes=[pltpu.VMEM((rows, cols), F32)],
         name="down",
-    )(hidden, near(wd))
+    )(hidden, wd, aside)
 
 
 def combine_kernel(returned, table, middle, shared, out):
@@ -428,7 +444,7 @@
         lax.all_gather(one, "tp"), lax.all_gather(two, "tp"), exp_down[0], sh_down, tok_rows
     )
     hidden_all, side_out = lax.optimization_barrier((hidden_all, side_out))
-    expert_out = jnp.concatenate([side_out, down(hidden_all, exp_down[0], 3)], axis=0)
+    expert_out = down(hidden_all, exp_down[0], side_out)
     returned = lax.all_to_all(
         expert_out.reshape(sp_count, slot_count // sp_count, col_width),
         "sp",

time: 214 us -> 214 us (level)
  Pallas kernels: 31 us -> 33.7 us
    pallas_call x1, Pallas kernels: 5.42 us -> 7.86 us  [down(): pl.pallas_call(down_kernel, grid=(pieces // 2,), in_specs=[pl.BlockSpec((...]
    unnamed x20 -> x14, local copies, waits for them, and re-layouts: 6.05 us -> 3.91 us
where the time goes in v7:
time: 214 us; the launch traced here: 213 us
  blocking collectives  90.5 us (42%)
  waiting for transfers between devices  38.5 us (18%)
  Pallas kernels  33.7 us (16%)
  starting transfers between devices  27.3 us (13%)
  between operations  13.5 us (6%)
  local copies, waits for them, and re-layouts  8.07 us (4%)
    all_gather x1, blocking collectives, body(): lax.all_gather(two, 'tp')  24.3 us
    all_gather x1, blocking collectives, body(): lax.all_gather(jnp.concatenate([landed[:first], middle], axis=0), 'tp')  22.3 us
    all_gather x1, blocking collectives, body(): lax.all_gather(one, 'tp')  22.2 us
    all_to_all x1, blocking collectives, body(): lax.all_to_all(expert_out.reshape(sp_count, slot_count // sp_count, col_w...  21.7 us
    all_to_all x1, waiting for transfers between devices, body(): lax.all_to_all(packed, 'tp', split_axis=0, concat_axis=0, tiled=True)  17.1 us
    all_to_all x1, starting transfers between devices, body(): lax.all_to_all(send.reshape(sp_count, slot_count // sp_count, col_width),...  14.6 us
    all_to_all x1, starting transfers between devices, body(): lax.all_to_all(packed, 'tp', split_axis=0, concat_axis=0, tiled=True)  8.64 us
    all_to_all x1, waiting for transfers between devices, body(): lax.all_to_all(send.reshape(sp_count, slot_count // sp_count, col_width),...  8.31 us
  transfers between devices with their start and end apart: 5, of which 5 were waited for; matrix products, arithmetic and copies ran while one was open for 3% of the time, Pallas kernels for 5%

profile of v7, /device:TPU:1, one launch (start us, length us, event | category | flops | bytes accessed | tf_op | source)
XLA Modules:
  0.0 213.3 jit_solution(14169373803215118300)
XLA Ops:
  6.5 0.0 copy-start
  6.5 0.0 copy-start.2
  6.5 0.9 multiply_convert_fusion
  7.5 3.9 %collective-permute-start = (bf16[30,64]{0,1:T(8,128)(2,1)S(1)}, bf16[30,64]{0,1:T(8,128)(2,1)S(1)}, u32[]{:S(2)}, u32[]{:S(2)}) collective-permute-start(bf16[30,64]{0,1:T(8,128)(2,1)S(1)} %multiply_convert_fusion), channel_id=1, source_target_pairs={{0,16},{16,32},{32,48},{48,64},{64,80},{80,96},{96,112},{112,128},... | collective-permute-start | bytes 11528 | tf_op jit(solution)/shard_map/ppermute | solution.py:410
  11.4 0.9 collective-permute-done
  12.3 0.0 copy-start.4
  12.3 0.9 copy-done.4
  13.2 0.0 copy-start.5
  13.2 1.9 pack.1
  15.1 8.6 %all-to-all-start = ((bf16[16,176,128]{2,1,0:T(8,128)(2,1)}), bf16[16,176,128]{2,1,0:T(8,128)(2,1)S(1)}, u32[]{:S(2)}, u32[]{:S(2)}) async-start(bf16[16,176,128]{2,1,0:T(8,128)(2,1)} %pack.1), calls=%async_computation | async-start | bytes 1441792 | tf_op jit(solution)/shard_map/all_to_all | solution.py:414
  23.8 1.4 copy.18.refs_0_
  25.2 2.2 %routing.1 = (s32[128,4]{1,0:T(8,128)}, bf16[1024,128]{1,0:T(8,128)(2,1)}) custom-call(s32[128,4]{1,0:T(8,128)} %copy.18.refs_0_), custom_call_target="tpu_custom_call" | custom-call | tf_op jit(solution)/shard_map/routing/pallas_call | solution.py:114
  27.4 0.0 copy-done
  27.4 0.6 constant_dynamic-slice_fusion.refs_1_
  28.1 17.1 %all-to-all-done.refs_0_ = bf16[16,176,128]{2,1,0:T(8,128)(2,1)S(1)} async-done(((bf16[16,176,128]{2,1,0:T(8,128)(2,1)}), bf16[16,176,128]{2,1,0:T(8,128)(2,1)S(1)}, u32[]{:S(2)}, u32[]{:S(2)}) %all-to-all-start) | async-done | bytes 720928 | tf_op jit(solution)/shard_map/all_to_all | solution.py:414
  45.1 5.1 %front.1 = (bf16[128,128]{1,0:T(8,128)(2,1)}, bf16[1024,128]{1,0:T(8,128)(2,1)}) custom-call(bf16[16,176,128]{2,1,0:T(8,128)(2,1)S(1)} %all-to-all-done.refs_0_, bf16[128,128]{1,0:T(8,128)(2,1)} %constant_dynamic-slice_fusion.refs_1_, bf16[1024,128]{1,0:T(8,128)(2,1)} %get-tuple-element.23.refs_2_), custom_call_target="tpu_custom_call" | custom-call | tf_op jit(solution)/shard_map/front/pallas_call | solution.py:198
  50.3 0.0 copy-start.1
  50.3 14.6 %all-to-all-start.1 = ((bf16[32,32,128]{2,1,0:T(8,128)(2,1)}), bf16[32,32,128]{2,1,0:T(8,128)(2,1)S(1)}, u32[]{:S(2)}, u32[]{:S(2)}) async-start(bf16[32,32,128]{2,1,0:T(8,128)(2,1)} %bitcast.35), calls=%async_computation.1 | async-start | bytes 524288 | tf_op jit(solution)/shard_map/all_to_all | solution.py:422
  64.9 0.0 all-gather.8.cloned.1.call-start
  65.0 1.4 copy.19.weights
  66.4 2.4 %table.1 = bf16[3,128,1024]{2,1,0:T(8,128)(2,1)} custom-call(s32[128,4]{1,0:T(8,128)} %get-tuple-element.26.slots, f32[128,4]{1,0:T(8,128)} %copy.19.weights), custom_call_target="tpu_custom_call" | custom-call | tf_op jit(solution)/shard_map/table/pallas_call | solution.py:137
  68.7 8.3 %all-to-all-done.1 = bf16[32,32,128]{2,1,0:T(8,128)(2,1)S(1)} async-done(((bf16[32,32,128]{2,1,0:T(8,128)(2,1)}), bf16[32,32,128]{2,1,0:T(8,128)(2,1)S(1)}, u32[]{:S(2)}, u32[]{:S(2)}) %all-to-all-start.1) | async-done | bytes 262176 | tf_op jit(solution)/shard_map/all_to_all | solution.py:422
  77.0 0.7 slice.16
  77.8 0.0 all-gather.8.cloned.1.call-update
  77.8 0.0 all-gather.10.cloned.1.call-start
  77.8 1.9 copy.20.sg
  79.7 0.0 copy-done.5
  79.7 1.0 copy.21.su
  80.8 0.8 pad_maximum_fusion
  81.5 22.3 %all-gather.1 = bf16[3584,128]{1,0:T(8,128)(2,1)} all-gather(bf16[224,128]{1,0:T(8,128)(2,1)S(1)} %pad_maximum_fusion), channel_id=3, replica_groups=mesh['sp'=32,'tp'=16] {'tp'}, dimensions={0}, use_global_device_ids=true | all-gather | bytes 974848 | tf_op jit(solution)/shard_map/all_gather | solution.py:436
  103.9 3.7 %side_hidden.1 = bf16[112,256]{1,0:T(8,128)(2,1)} custom-call(bf16[16,224,128]{2,1,0:T(8,128)(2,1)} %bitcast.31, f32[1,2048]{1,0:T(1,128)} %bitcast.38, bf16[2048,256]{1,0:T(8,128)(2,1)} %bitcast.19, bf16[2048,256]{1,0:T(8,128)(2,1)} %bitcast.21, bf16[2048,32]{1,0:T(8,128)(2,1)} %copy.20.sg, bf16[2048,32]{1,0:T(8,128)(2,1)} %copy.21.su), custom_call_target="tpu_custom_call" | custom-call | tf_op jit(solution)/shard_map/side_hidden/pallas_call | solution.py:285
  107.6 8.1 %all-gather.8.cloned.1.call-done = bf16[14848,128]{1,0:T(8,128)(2,1)} async-done(((bf16[928,128]{1,0:T(8,128)(2,1)}), bf16[14848,128]{1,0:T(8,128)(2,1)}) %all-gather.8.cloned.1.call-update) | async-done | bytes 3801104 | tf_op jit(solution)/shard_map/all_gather | solution.py:435
  115.7 0.0 copy-done.2
  115.7 0.0 copy-done.1
  115.7 5.3 %hidden.1 = (bf16[112,256]{1,0:T(8,128)(2,1)}, bf16[816,256]{1,0:T(8,128)(2,1)}) custom-call(bf16[16,928,128]{2,1,0:T(8,128)(2,1)} %bitcast.28, f32[1,2048]{1,0:T(1,128)} %bitcast.39, bf16[2048,256]{1,0:T(8,128)(2,1)S(1)} %bitcast.20, bf16[2048,256]{1,0:T(8,128)(2,1)S(1)} %bitcast.22), custom_call_target="tpu_custom_call" | custom-call | tf_op jit(solution)/shard_map/hidden/pallas_call | solution.py:251
  120.9 0.0 all-gather.10.cloned.1.call-update
  121.0 0.0 copy-start.3
  121.0 22.2 %all-gather.3 = bf16[1792,256]{1,0:T(8,128)(2,1)} all-gather(bf16[112,256]{1,0:T(8,128)(2,1)} %side_hidden.1), channel_id=5, replica_groups=mesh['sp'=32,'tp'=16] {'tp'}, dimensions={0}, use_global_device_ids=true | all-gather | bytes 974848 | tf_op jit(solution)/shard_map/all_gather | solution.py:444
  143.2 24.3 %all-gather.4 = bf16[1792,256]{1,0:T(8,128)(2,1)} all-gather(bf16[112,256]{1,0:T(8,128)(2,1)} %get-tuple-element.35), channel_id=6, replica_groups=mesh['sp'=32,'tp'=16] {'tp'}, dimensions={0}, use_global_device_ids=true | all-gather | bytes 974848 | tf_op jit(solution)/shard_map/all_gather | solution.py:444
  167.5 3.4 %side_down.1 = (bf16[208,128]{1,0:T(8,128)(2,1)}, f32[128,128]{1,0:T(8,128)}) custom-call(bf16[16,112,256]{2,1,0:T(8,128)(2,1)} %bitcast.29, bf16[16,112,256]{2,1,0:T(8,128)(2,1)} %bitcast.30, bf16[4096,128]{1,0:T(8,128)(2,1)} %bitcast.26, bf16[512,128]{1,0:T(8,128)(2,1)} %sh_down.1), custom_call_target="tpu_custom_call" | custom-call | tf_op jit(solution)/shard_map/side_down/pallas_call | solution.py:314
  170.9 4.2 %all-gather.10.cloned.1.call-done = bf16[13056,256]{1,0:T(8,128)(2,1)} async-done(((bf16[816,256]{1,0:T(8,128)(2,1)}), bf16[13056,256]{1,0:T(8,128)(2,1)}) %all-gather.10.cloned.1.call-update) | async-done | bytes 6684688 | tf_op jit(solution)/shard_map/all_gather | solution.py:441
  175.1 7.9 %down.1 = bf16[1024,128]{1,0:T(8,128)(2,1)} custom-call(bf16[16,816,256]{2,1,0:T(8,128)(2,1)} %bitcast.25, bf16[4096,128]{1,0:T(8,128)(2,1)} %bitcast.27, bf16[208,128]{1,0:T(8,128)(2,1)} %get-tuple-element.38.aside), custom_call_target="tpu_custom_call" | custom-call | tf_op jit(solution)/shard_map/down/pallas_call | solution.py:346
  182.9 21.7 %all_to_all.15 = bf16[32,32,128]{2,1,0:T(8,128)(2,1)S(1)} all-to-all(bf16[32,32,128]{2,1,0:T(8,128)(2,1)} %bitcast.32), channel_id=1, replica_groups=mesh['sp'=32,'tp'=16] {'sp'}, dimensions={0} | all-to-all | bytes 524288 | tf_op jit(solution)/shard_map/all_to_all | solution.py:448
  204.6 0.0 copy-done.3
  204.6 1.8 combine.1
  (1 shorter events, 0.0 us)
Async XLA Ops:
  6.5 20.9 %copy-start = (bf16[128,2048]{1,0:T(8,128)(2,1)S(1)}, bf16[128,2048]{1,0:T(8,128)(2,1)}, u32[]{:S(2)}) copy-start(bf16[128,2048]{1,0:T(8,128)(2,1)} %param.17) | copy-start | bytes 1572868
  6.5 109.1 %copy-start.2 = (bf16[1,2048,256]{2,1,0:T(8,128)(2,1)S(1)}, bf16[1,2048,256]{2,1,0:T(8,128)(2,1)}, u32[]{:S(2)}) copy-start(bf16[1,2048,256]{2,1,0:T(8,128)(2,1)} %param.29) | copy-start | bytes 3145732
  7.5 4.8 %collective-permute-start = (bf16[30,64]{0,1:T(8,128)(2,1)S(1)}, bf16[30,64]{0,1:T(8,128)(2,1)S(1)}, u32[]{:S(2)}, u32[]{:S(2)}) collective-permute-start(bf16[30,64]{0,1:T(8,128)(2,1)S(1)} %multiply_convert_fusion), channel_id=1, source_target_pairs={{0,16},{16,32},{32,48},{48,64},{64,80},{80,96},{96,112},{112,128},... | collective-permute-start | bytes 11528 | tf_op jit(solution)/shard_map/ppermute | solution.py:410
  12.3 0.9 copy-start.4
  13.2 66.5 %copy-start.5 = (bf16[2048,32]{0,1:T(8,128)(2,1)S(1)}, bf16[2048,32]{0,1:T(8,128)(2,1)}, u32[]{:S(2)}) copy-start(bf16[2048,32]{0,1:T(8,128)(2,1)} %param.32) | copy-start | bytes 393220
  15.1 30.0 %all-to-all-start = ((bf16[16,176,128]{2,1,0:T(8,128)(2,1)}), bf16[16,176,128]{2,1,0:T(8,128)(2,1)S(1)}, u32[]{:S(2)}, u32[]{:S(2)}) async-start(bf16[16,176,128]{2,1,0:T(8,128)(2,1)} %pack.1), calls=%async_computation | async-start | bytes 1441792 | tf_op jit(solution)/shard_map/all_to_all | solution.py:414
  50.3 65.4 %copy-start.1 = (bf16[1,2048,256]{2,1,0:T(8,128)(2,1)S(1)}, bf16[1,2048,256]{2,1,0:T(8,128)(2,1)}, u32[]{:S(2)}) copy-start(bf16[1,2048,256]{2,1,0:T(8,128)(2,1)} %param.28) | copy-start | bytes 3145732
  50.3 26.8 %all-to-all-start.1 = ((bf16[32,32,128]{2,1,0:T(8,128)(2,1)}), bf16[32,32,128]{2,1,0:T(8,128)(2,1)S(1)}, u32[]{:S(2)}, u32[]{:S(2)}) async-start(bf16[32,32,128]{2,1,0:T(8,128)(2,1)} %bitcast.35), calls=%async_computation.1 | async-start | bytes 524288 | tf_op jit(solution)/shard_map/all_to_all | solution.py:422
  64.9 50.7 %all-gather.8.cloned.1.call-start = ((), (), s32[]{:S(2)}) async-start(), calls=%async_computation.3 | async-start | bytes 4038656 | tf_op jit(solution)/shard_map/all_gather | solution.py:435
  77.8 97.3 %all-gather.10.cloned.1.call-start = ((), (), s32[]{:S(2)}) async-start(), calls=%async_computation.4 | async-start | bytes 7102464 | tf_op jit(solution)/shard_map/all_gather | solution.py:441
  121.0 83.7 %copy-start.3 = (bf16[3,128,1024]{2,1,0:T(8,128)(2,1)S(1)}, bf16[3,128,1024]{2,1,0:T(8,128)(2,1)}, u32[]{:S(2)}) copy-start(bf16[3,128,1024]{2,1,0:T(8,128)(2,1)} %table.1) | copy-start | bytes 2359300
Sparse Core Ops, SparseCore 0:
  77.9 37.7 all-gather.7
  121.1 53.9 all-gather.9

commit v8 on v6

--- a/solution.py
+++ b/solution.py
@@ -78,7 +78,7 @@
             pltpu.VMEM((half, LANES), F32),
         ],
         name="pack",
-    )(near(before), a_val, a_gate, taps, bias, gain, shift, near(w_out))
+    )(near(before), a_val, a_gate, taps, bias, gain, shift, w_out)
 
 
 def routing_kernel(capacity, routes, slots_out, pick_out):
@@ -207,7 +207,7 @@
             pltpu.VMEM((tok_rows, channels), F32),
         ],
         name="front",
-    )(near(packed), resid, near(pick))
+    )(near(packed), resid, pick)
 
 
 def normed_rows(pieces, width, gain):
@@ -321,25 +321,36 @@
     )(one, two, wd, sh_down)
 
 
-def down_kernel(hidden, wd, out):
+def down_kernel(hidden, wd, aside, out):
+    slots = aside.shape[0]
+    block = hidden.shape[1]
+    step = pl.program_id(0)
+
+    @pl.when(step == 0)
+    def _():
+        out[0:slots, :] = aside[...]
+
     whole = jnp.concatenate([hidden[t] for t in range(hidden.shape[0])], axis=1)
-    out[...] = jnp.dot(whole, wd[...], preferred_element_type=F32).astype(BF16)
-
-
-def down(hidden, wd, blocks):
+    at = pl.ds(pl.multiple_of(slots + step * block, 16), block)
+    out[at, :] = jnp.dot(whole, wd[...], preferred_element_type=F32).astype(BF16)
+
+
+def down(hidden, wd, aside, blocks):
     pieces, rows, units = hidden.shape
     block = rows // blocks
+    total = (aside.shape[0] + rows, wd.shape[1])
     return pl.pallas_call(
         down_kernel,
         grid=(blocks,),
         in_specs=[
             pl.BlockSpec((pieces, block, units), lambda i: (0, i, 0)),
-            pl.BlockSpec(memory_space=pltpu.VMEM),
+            pl.BlockSpec(wd.shape, lambda i: (0, 0)),
+            pl.BlockSpec(aside.shape, lambda i: (0, 0)),
         ],
-        out_specs=pl.BlockSpec((block, wd.shape[1]), lambda i: (i, 0)),
-        out_shape=jax.ShapeDtypeStruct((rows, wd.shape[1]), BF16),
+        out_specs=pl.BlockSpec(total, lambda i: (0, 0)),
+        out_shape=jax.ShapeDtypeStruct(total, BF16),
         name="down",
-    )(hidden, near(wd))
+    )(hidden, wd, aside)
 
 
 def combine_kernel(returned, table, middle, shared, out):
@@ -428,7 +439,7 @@
         lax.all_gather(one, "tp"), lax.all_gather(two, "tp"), exp_down[0], sh_down, tok_rows
     )
     hidden_all, side_out = lax.optimization_barrier((hidden_all, side_out))
-    expert_out = jnp.concatenate([side_out, down(hidden_all, exp_down[0], 3)], axis=0)
+    expert_out = down(hidden_all, exp_down[0], side_out, 3)
     returned = lax.all_to_all(
         expert_out.reshape(sp_count, slot_count // sp_count, col_width),
         "sp",

time: 214 us -> 211 us (0.986)
  local copies, waits for them, and re-layouts: 10.2 us -> 7.13 us
    unnamed x20 -> x12, local copies, waits for them, and re-layouts: 6.05 us -> 2.98 us
  transfers between devices with their start and end apart: 5 -> 5, of which waited for: 5 -> 5; matrix products, arithmetic and copies ran while one was open for 3% -> 3% of each run, Pallas kernels for 5% -> 6%
where the time goes in v8:
time: 211 us; the launch traced here: 210 us
  blocking collectives  90.5 us (43%)
  waiting for transfers between devices  38.5 us (18%)
  Pallas kernels  31.9 us (15%)
  starting transfers between devices  27.3 us (13%)
  between operations  13.5 us (6%)
  local copies, waits for them, and re-layouts  7.13 us (3%)
    all_gather x1, blocking collectives, body(): lax.all_gather(two, 'tp')  24.3 us
    all_gather x1, blocking collectives, body(): lax.all_gather(one, 'tp')  22.3 us
    all_gather x1, blocking collectives, body(): lax.all_gather(jnp.concatenate([landed[:first], middle], axis=0), 'tp')  22.3 us
    all_to_all x1, blocking collectives, body(): lax.all_to_all(expert_out.reshape(sp_count, slot_count // sp_count, col_w...  21.6 us
    all_to_all x1, waiting for transfers between devices, body(): lax.all_to_all(packed, 'tp', split_axis=0, concat_axis=0, tiled=True)  17 us
    all_to_all x1, starting transfers between devices, body(): lax.all_to_all(send.reshape(sp_count, slot_count // sp_count, col_width),...  14.6 us
    all_to_all x1, starting transfers between devices, body(): lax.all_to_all(packed, 'tp', split_axis=0, concat_axis=0, tiled=True)  8.64 us
    all_to_all x1, waiting for transfers between devices, body(): lax.all_to_all(send.reshape(sp_count, slot_count // sp_count, col_width),...  8.32 us
  transfers between devices with their start and end apart: 5, of which 5 were waited for; matrix products, arithmetic and copies ran while one was open for 3% of the time, Pallas kernels for 6%

profile of v8, /device:TPU:1, one launch (start us, length us, event | category | flops | bytes accessed | tf_op | source)
XLA Modules:
  0.0 210.5 jit_solution(4743720865006049342)
XLA Ops:
  6.5 0.0 copy-start
  6.5 0.0 copy-start.4
  6.5 0.0 copy-start.2
  6.5 0.9 multiply_convert_fusion
  7.5 3.9 %collective-permute-start = (bf16[30,64]{0,1:T(8,128)(2,1)S(1)}, bf16[30,64]{0,1:T(8,128)(2,1)S(1)}, u32[]{:S(2)}, u32[]{:S(2)}) collective-permute-start(bf16[30,64]{0,1:T(8,128)(2,1)S(1)} %multiply_convert_fusion), channel_id=1, source_target_pairs={{0,16},{16,32},{32,48},{48,64},{64,80},{80,96},{96,112},{112,128},... | collective-permute-start | bytes 11528 | tf_op jit(solution)/shard_map/ppermute | solution.py:405
  11.4 0.9 collective-permute-done
  12.3 2.2 %pack.1 = bf16[16,176,128]{2,1,0:T(8,128)(2,1)} custom-call(bf16[64,30]{1,0:T(8,128)(2,1)S(1)} %bitcast.24, bf16[64,128]{1,0:T(8,128)(2,1)} %bitcast.37, bf16[64,128]{1,0:T(8,128)(2,1)} %bitcast.36, bf16[31,64]{1,0:T(8,128)(2,1)} %taps.1, f32[1,64]{1,0:T(1,128)} %bitcast.40, f32[1,64]{1,0:T(1,128)} %bitcast.41, f32[1,64]{1,0:T(1,128)} %bitcast.42, ...), custom_call_target="tpu_custom_call" | custom-call | tf_op jit(solution)/shard_map/pack/pallas_call | solution.py:72
  14.4 8.6 %all-to-all-start = ((bf16[16,176,128]{2,1,0:T(8,128)(2,1)}), bf16[16,176,128]{2,1,0:T(8,128)(2,1)S(1)}, u32[]{:S(2)}, u32[]{:S(2)}) async-start(bf16[16,176,128]{2,1,0:T(8,128)(2,1)} %pack.1), calls=%async_computation | async-start | bytes 1441792 | tf_op jit(solution)/shard_map/all_to_all | solution.py:409
  23.1 1.4 copy.18.refs_0_
  24.5 2.3 %routing.1 = (s32[128,4]{1,0:T(8,128)}, bf16[1024,128]{1,0:T(8,128)(2,1)}) custom-call(s32[128,4]{1,0:T(8,128)} %copy.18.refs_0_), custom_call_target="tpu_custom_call" | custom-call | tf_op jit(solution)/shard_map/routing/pallas_call | solution.py:114
  26.8 0.0 copy-done
  26.8 0.6 constant_dynamic-slice_fusion.refs_1_
  27.4 17.0 %all-to-all-done.refs_0_ = bf16[16,176,128]{2,1,0:T(8,128)(2,1)S(1)} async-done(((bf16[16,176,128]{2,1,0:T(8,128)(2,1)}), bf16[16,176,128]{2,1,0:T(8,128)(2,1)S(1)}, u32[]{:S(2)}, u32[]{:S(2)}) %all-to-all-start) | async-done | bytes 720928 | tf_op jit(solution)/shard_map/all_to_all | solution.py:409
  44.4 5.1 %front.1 = (bf16[128,128]{1,0:T(8,128)(2,1)}, bf16[1024,128]{1,0:T(8,128)(2,1)}) custom-call(bf16[16,176,128]{2,1,0:T(8,128)(2,1)S(1)} %all-to-all-done.refs_0_, bf16[128,128]{1,0:T(8,128)(2,1)} %constant_dynamic-slice_fusion.refs_1_, bf16[1024,128]{1,0:T(8,128)(2,1)} %get-tuple-element.23.refs_2_), custom_call_target="tpu_custom_call" | custom-call | tf_op jit(solution)/shard_map/front/pallas_call | solution.py:198
  49.6 0.0 copy-start.1
  49.6 14.6 %all-to-all-start.1 = ((bf16[32,32,128]{2,1,0:T(8,128)(2,1)}), bf16[32,32,128]{2,1,0:T(8,128)(2,1)S(1)}, u32[]{:S(2)}, u32[]{:S(2)}) async-start(bf16[32,32,128]{2,1,0:T(8,128)(2,1)} %bitcast.35), calls=%async_computation.1 | async-start | bytes 524288 | tf_op jit(solution)/shard_map/all_to_all | solution.py:417
  64.2 0.0 all-gather.8.cloned.1.call-start
  64.3 1.4 copy.19.weights
  65.7 2.4 %table.1 = bf16[3,128,1024]{2,1,0:T(8,128)(2,1)} custom-call(s32[128,4]{1,0:T(8,128)} %get-tuple-element.26.slots, f32[128,4]{1,0:T(8,128)} %copy.19.weights), custom_call_target="tpu_custom_call" | custom-call | tf_op jit(solution)/shard_map/table/pallas_call | solution.py:137
  68.0 8.3 %all-to-all-done.1 = bf16[32,32,128]{2,1,0:T(8,128)(2,1)S(1)} async-done(((bf16[32,32,128]{2,1,0:T(8,128)(2,1)}), bf16[32,32,128]{2,1,0:T(8,128)(2,1)S(1)}, u32[]{:S(2)}, u32[]{:S(2)}) %all-to-all-start.1) | async-done | bytes 262176 | tf_op jit(solution)/shard_map/all_to_all | solution.py:417
  76.4 0.7 slice.16
  77.1 0.0 all-gather.8.cloned.1.call-update
  77.1 0.0 all-gather.10.cloned.1.call-start
  77.1 1.9 copy.20.sg
  79.1 0.0 copy-done.4
  79.1 1.0 copy.21.su
  80.1 0.8 pad_maximum_fusion
  80.9 22.3 %all-gather.1 = bf16[3584,128]{1,0:T(8,128)(2,1)} all-gather(bf16[224,128]{1,0:T(8,128)(2,1)S(1)} %pad_maximum_fusion), channel_id=3, replica_groups=mesh['sp'=32,'tp'=16] {'tp'}, dimensions={0}, use_global_device_ids=true | all-gather | bytes 974848 | tf_op jit(solution)/shard_map/all_gather | solution.py:431
  103.2 3.7 %side_hidden.1 = bf16[112,256]{1,0:T(8,128)(2,1)} custom-call(bf16[16,224,128]{2,1,0:T(8,128)(2,1)} %bitcast.31, f32[1,2048]{1,0:T(1,128)} %bitcast.38, bf16[2048,256]{1,0:T(8,128)(2,1)} %bitcast.19, bf16[2048,256]{1,0:T(8,128)(2,1)} %bitcast.21, bf16[2048,32]{1,0:T(8,128)(2,1)} %copy.20.sg, bf16[2048,32]{1,0:T(8,128)(2,1)} %copy.21.su), custom_call_target="tpu_custom_call" | custom-call | tf_op jit(solution)/shard_map/side_hidden/pallas_call | solution.py:285
  106.9 8.1 %all-gather.8.cloned.1.call-done = bf16[14848,128]{1,0:T(8,128)(2,1)} async-done(((bf16[928,128]{1,0:T(8,128)(2,1)}), bf16[14848,128]{1,0:T(8,128)(2,1)}) %all-gather.8.cloned.1.call-update) | async-done | bytes 3801104 | tf_op jit(solution)/shard_map/all_gather | solution.py:430
  115.0 0.0 copy-done.2
  115.0 0.0 copy-done.1
  115.0 5.3 %hidden.1 = (bf16[112,256]{1,0:T(8,128)(2,1)}, bf16[816,256]{1,0:T(8,128)(2,1)}) custom-call(bf16[16,928,128]{2,1,0:T(8,128)(2,1)} %bitcast.28, f32[1,2048]{1,0:T(1,128)} %bitcast.39, bf16[2048,256]{1,0:T(8,128)(2,1)S(1)} %bitcast.20, bf16[2048,256]{1,0:T(8,128)(2,1)S(1)} %bitcast.22), custom_call_target="tpu_custom_call" | custom-call | tf_op jit(solution)/shard_map/hidden/pallas_call | solution.py:251
  120.3 0.0 all-gather.10.cloned.1.call-update
  120.3 0.0 copy-start.3
  120.4 22.3 %all-gather.3 = bf16[1792,256]{1,0:T(8,128)(2,1)} all-gather(bf16[112,256]{1,0:T(8,128)(2,1)} %side_hidden.1), channel_id=5, replica_groups=mesh['sp'=32,'tp'=16] {'tp'}, dimensions={0}, use_global_device_ids=true | all-gather | bytes 974848 | tf_op jit(solution)/shard_map/all_gather | solution.py:439
  142.7 24.3 %all-gather.4 = bf16[1792,256]{1,0:T(8,128)(2,1)} all-gather(bf16[112,256]{1,0:T(8,128)(2,1)} %get-tuple-element.35), channel_id=6, replica_groups=mesh['sp'=32,'tp'=16] {'tp'}, dimensions={0}, use_global_device_ids=true | all-gather | bytes 974848 | tf_op jit(solution)/shard_map/all_gather | solution.py:439
  167.0 3.3 %side_down.1 = (bf16[208,128]{1,0:T(8,128)(2,1)}, f32[128,128]{1,0:T(8,128)}) custom-call(bf16[16,112,256]{2,1,0:T(8,128)(2,1)} %bitcast.29, bf16[16,112,256]{2,1,0:T(8,128)(2,1)} %bitcast.30, bf16[4096,128]{1,0:T(8,128)(2,1)} %bitcast.26, bf16[512,128]{1,0:T(8,128)(2,1)} %sh_down.1), custom_call_target="tpu_custom_call" | custom-call | tf_op jit(solution)/shard_map/side_down/pallas_call | solution.py:314
  170.4 4.1 %all-gather.10.cloned.1.call-done = bf16[13056,256]{1,0:T(8,128)(2,1)} async-done(((bf16[816,256]{1,0:T(8,128)(2,1)}), bf16[13056,256]{1,0:T(8,128)(2,1)}) %all-gather.10.cloned.1.call-update) | async-done | bytes 6684688 | tf_op jit(solution)/shard_map/all_gather | solution.py:436
  174.5 5.7 %down.1 = bf16[1024,128]{1,0:T(8,128)(2,1)} custom-call(bf16[16,816,256]{2,1,0:T(8,128)(2,1)} %bitcast.25, bf16[4096,128]{1,0:T(8,128)(2,1)} %bitcast.27, bf16[208,128]{1,0:T(8,128)(2,1)} %get-tuple-element.38.aside), custom_call_target="tpu_custom_call" | custom-call | tf_op jit(solution)/shard_map/down/pallas_call | solution.py:342
  180.2 21.6 %all_to_all.15 = bf16[32,32,128]{2,1,0:T(8,128)(2,1)S(1)} all-to-all(bf16[32,32,128]{2,1,0:T(8,128)(2,1)} %bitcast.32), channel_id=1, replica_groups=mesh['sp'=32,'tp'=16] {'sp'}, dimensions={0} | all-to-all | bytes 524288 | tf_op jit(solution)/shard_map/all_to_all | solution.py:443
  201.8 0.0 copy-done.3
  201.8 1.8 combine.1
  (1 shorter events, 0.0 us)
Async XLA Ops:
  6.5 20.2 %copy-start = (bf16[128,2048]{1,0:T(8,128)(2,1)S(1)}, bf16[128,2048]{1,0:T(8,128)(2,1)}, u32[]{:S(2)}) copy-start(bf16[128,2048]{1,0:T(8,128)(2,1)} %param.17) | copy-start | bytes 1572868
  6.5 72.5 %copy-start.4 = (bf16[2048,32]{0,1:T(8,128)(2,1)S(1)}, bf16[2048,32]{0,1:T(8,128)(2,1)}, u32[]{:S(2)}) copy-start(bf16[2048,32]{0,1:T(8,128)(2,1)} %param.32) | copy-start | bytes 393220
  6.5 108.5 %copy-start.2 = (bf16[1,2048,256]{2,1,0:T(8,128)(2,1)S(1)}, bf16[1,2048,256]{2,1,0:T(8,128)(2,1)}, u32[]{:S(2)}) copy-start(bf16[1,2048,256]{2,1,0:T(8,128)(2,1)} %param.29) | copy-start | bytes 3145732
  7.5 4.8 %collective-permute-start = (bf16[30,64]{0,1:T(8,128)(2,1)S(1)}, bf16[30,64]{0,1:T(8,128)(2,1)S(1)}, u32[]{:S(2)}, u32[]{:S(2)}) collective-permute-start(bf16[30,64]{0,1:T(8,128)(2,1)S(1)} %multiply_convert_fusion), channel_id=1, source_target_pairs={{0,16},{16,32},{32,48},{48,64},{64,80},{80,96},{96,112},{112,128},... | collective-permute-start | bytes 11528 | tf_op jit(solution)/shard_map/ppermute | solution.py:405
  14.4 30.0 %all-to-all-start = ((bf16[16,176,128]{2,1,0:T(8,128)(2,1)}), bf16[16,176,128]{2,1,0:T(8,128)(2,1)S(1)}, u32[]{:S(2)}, u32[]{:S(2)}) async-start(bf16[16,176,128]{2,1,0:T(8,128)(2,1)} %pack.1), calls=%async_computation | async-start | bytes 1441792 | tf_op jit(solution)/shard_map/all_to_all | solution.py:409
  49.6 65.4 %copy-start.1 = (bf16[1,2048,256]{2,1,0:T(8,128)(2,1)S(1)}, bf16[1,2048,256]{2,1,0:T(8,128)(2,1)}, u32[]{:S(2)}) copy-start(bf16[1,2048,256]{2,1,0:T(8,128)(2,1)} %param.28) | copy-start | bytes 3145732
  49.6 26.8 %all-to-all-start.1 = ((bf16[32,32,128]{2,1,0:T(8,128)(2,1)}), bf16[32,32,128]{2,1,0:T(8,128)(2,1)S(1)}, u32[]{:S(2)}, u32[]{:S(2)}) async-start(bf16[32,32,128]{2,1,0:T(8,128)(2,1)} %bitcast.35), calls=%async_computation.1 | async-start | bytes 524288 | tf_op jit(solution)/shard_map/all_to_all | solution.py:417
  64.2 50.8 %all-gather.8.cloned.1.call-start = ((), (), s32[]{:S(2)}) async-start(), calls=%async_computation.3 | async-start | bytes 4038656 | tf_op jit(solution)/shard_map/all_gather | solution.py:430
  77.1 97.4 %all-gather.10.cloned.1.call-start = ((), (), s32[]{:S(2)}) async-start(), calls=%async_computation.4 | async-start | bytes 7102464 | tf_op jit(solution)/shard_map/all_gather | solution.py:436
  120.3 81.5 %copy-start.3 = (bf16[3,128,1024]{2,1,0:T(8,128)(2,1)S(1)}, bf16[3,128,1024]{2,1,0:T(8,128)(2,1)}, u32[]{:S(2)}) copy-start(bf16[3,128,1024]{2,1,0:T(8,128)(2,1)} %table.1) | copy-start | bytes 2359300
Sparse Core Ops, SparseCore 0:
  77.2 37.7 all-gather.7
  120.5 53.9 all-gather.9

commit v9 on v8

--- a/solution.py
+++ b/solution.py
@@ -146,14 +146,14 @@
     tok_rows = resid.shape[0]
     half = LANES // 2
     channels = peers * half
-    top = win.shape[0] // 2
+    top = win.shape[1] // 2
     fold = PARAM_ROWS // 2
     for pair in range(peers // 2):
         at = slice(pair * LANES, (pair + 1) * LANES)
         one, two = packed[2 * pair, 0 : top + fold, :], packed[2 * pair + 1, 0 : top + fold, :]
         left = jnp.concatenate([one[:, :half], two[:, :half]], axis=1).astype(F32)
         right = jnp.concatenate([one[:, half:], two[:, half:]], axis=1).astype(F32)
-        win[0:top, at], win[top : 2 * top, at] = left[0:top], right[0:top]
+        win[pair, 0:top, :], win[pair, top : 2 * top, :] = left[0:top], right[0:top]
         params[0:fold, at], params[fold : 2 * fold, at] = left[top:], right[top:]
 
     def vector(first, cols=slice(None)):
@@ -168,7 +168,7 @@
         for r in range(0, tok_rows, conv_rows):
             acc = jnp.broadcast_to(b, (conv_rows, LANES))
             for j in range(span):
-                acc = acc + taps[j : j + 1, :] * win[r + j : r + j + conv_rows, cols]
+                acc = acc + taps[j : j + 1, :] * win[i, r + j : r + j + conv_rows, :]
             conv[r : r + conv_rows, cols] = acc
         return 0
 
@@ -202,7 +202,7 @@
             jax.ShapeDtypeStruct((pick.shape[0], cols), BF16),
         ),
         scratch_shapes=[
-            pltpu.VMEM((window_rows(span, tok_rows), channels), F32),
+            pltpu.VMEM((channels // LANES, window_rows(span, tok_rows), LANES), F32),
             pltpu.VMEM((PARAM_ROWS, channels), F32),
             pltpu.VMEM((tok_rows, channels), F32),
         ],

time: 211 us -> 210 us (level)
  no operation moved by 1% of the time
where the time goes in v9:
time: 210 us; the launch traced here: 209 us
  blocking collectives  90.5 us (43%)
  waiting for transfers between devices  38.5 us (18%)
  Pallas kernels  30.4 us (14%)
  starting transfers between devices  27.3 us (13%)
  between operations  13.5 us (6%)
  local copies, waits for them, and re-layouts  7.13 us (3%)
    all_gather x1, blocking collectives, body(): lax.all_gather(two, 'tp')  24.3 us
    all_gather x1, blocking collectives, body(): lax.all_gather(jnp.concatenate([landed[:first], middle], axis=0), 'tp')  22.3 us
    all_gather x1, blocking collectives, body(): lax.all_gather(one, 'tp')  22.3 us
    all_to_all x1, blocking collectives, body(): lax.all_to_all(expert_out.reshape(sp_count, slot_count // sp_count, col_w...  21.6 us
    all_to_all x1, waiting for transfers between devices, body(): lax.all_to_all(packed, 'tp', split_axis=0, concat_axis=0, tiled=True)  17 us
    all_to_all x1, starting transfers between devices, body(): lax.all_to_all(send.reshape(sp_count, slot_count // sp_count, col_width),...  14.6 us
    all_to_all x1, starting transfers between devices, body(): lax.all_to_all(packed, 'tp', split_axis=0, concat_axis=0, tiled=True)  8.64 us
    all_to_all x1, waiting for transfers between devices, body(): lax.all_to_all(send.reshape(sp_count, slot_count // sp_count, col_width),...  8.31 us
  transfers between devices with their start and end apart: 5, of which 5 were waited for; matrix products, arithmetic and copies ran while one was open for 3% of the time, Pallas kernels for 6%

profile of v9, /device:TPU:1, one launch (start us, length us, event | category | flops | bytes accessed | tf_op | source)
XLA Modules:
  0.0 209.0 jit_solution(15759760713762776127)
XLA Ops:
  6.5 0.0 copy-start
  6.5 0.0 copy-start.4
  6.5 0.0 copy-start.2
  6.5 0.9 multiply_convert_fusion
  7.5 3.9 %collective-permute-start = (bf16[30,64]{0,1:T(8,128)(2,1)S(1)}, bf16[30,64]{0,1:T(8,128)(2,1)S(1)}, u32[]{:S(2)}, u32[]{:S(2)}) collective-permute-start(bf16[30,64]{0,1:T(8,128)(2,1)S(1)} %multiply_convert_fusion), channel_id=1, source_target_pairs={{0,16},{16,32},{32,48},{48,64},{64,80},{80,96},{96,112},{112,128},... | collective-permute-start | bytes 11528 | tf_op jit(solution)/shard_map/ppermute | solution.py:405
  11.4 0.9 collective-permute-done
  12.3 2.2 %pack.1 = bf16[16,176,128]{2,1,0:T(8,128)(2,1)} custom-call(bf16[64,30]{1,0:T(8,128)(2,1)S(1)} %bitcast.24, bf16[64,128]{1,0:T(8,128)(2,1)} %bitcast.37, bf16[64,128]{1,0:T(8,128)(2,1)} %bitcast.36, bf16[31,64]{1,0:T(8,128)(2,1)} %taps.1, f32[1,64]{1,0:T(1,128)} %bitcast.40, f32[1,64]{1,0:T(1,128)} %bitcast.41, f32[1,64]{1,0:T(1,128)} %bitcast.42, ...), custom_call_target="tpu_custom_call" | custom-call | tf_op jit(solution)/shard_map/pack/pallas_call | solution.py:72
  14.4 8.6 %all-to-all-start = ((bf16[16,176,128]{2,1,0:T(8,128)(2,1)}), bf16[16,176,128]{2,1,0:T(8,128)(2,1)S(1)}, u32[]{:S(2)}, u32[]{:S(2)}) async-start(bf16[16,176,128]{2,1,0:T(8,128)(2,1)} %pack.1), calls=%async_computation | async-start | bytes 1441792 | tf_op jit(solution)/shard_map/all_to_all | solution.py:409
  23.1 1.4 copy.18.refs_0_
  24.5 2.3 %routing.1 = (s32[128,4]{1,0:T(8,128)}, bf16[1024,128]{1,0:T(8,128)(2,1)}) custom-call(s32[128,4]{1,0:T(8,128)} %copy.18.refs_0_), custom_call_target="tpu_custom_call" | custom-call | tf_op jit(solution)/shard_map/routing/pallas_call | solution.py:114
  26.8 0.0 copy-done
  26.8 0.6 constant_dynamic-slice_fusion.refs_1_
  27.4 17.0 %all-to-all-done.refs_0_ = bf16[16,176,128]{2,1,0:T(8,128)(2,1)S(1)} async-done(((bf16[16,176,128]{2,1,0:T(8,128)(2,1)}), bf16[16,176,128]{2,1,0:T(8,128)(2,1)S(1)}, u32[]{:S(2)}, u32[]{:S(2)}) %all-to-all-start) | async-done | bytes 720928 | tf_op jit(solution)/shard_map/all_to_all | solution.py:409
  44.4 3.7 %front.1 = (bf16[128,128]{1,0:T(8,128)(2,1)}, bf16[1024,128]{1,0:T(8,128)(2,1)}) custom-call(bf16[16,176,128]{2,1,0:T(8,128)(2,1)S(1)} %all-to-all-done.refs_0_, bf16[128,128]{1,0:T(8,128)(2,1)} %constant_dynamic-slice_fusion.refs_1_, bf16[1024,128]{1,0:T(8,128)(2,1)} %get-tuple-element.23.refs_2_), custom_call_target="tpu_custom_call" | custom-call | tf_op jit(solution)/shard_map/front/pallas_call | solution.py:198
  48.1 0.0 copy-start.1
  48.1 14.6 %all-to-all-start.1 = ((bf16[32,32,128]{2,1,0:T(8,128)(2,1)}), bf16[32,32,128]{2,1,0:T(8,128)(2,1)S(1)}, u32[]{:S(2)}, u32[]{:S(2)}) async-start(bf16[32,32,128]{2,1,0:T(8,128)(2,1)} %bitcast.35), calls=%async_computation.1 | async-start | bytes 524288 | tf_op jit(solution)/shard_map/all_to_all | solution.py:417
  62.8 0.0 all-gather.8.cloned.1.call-start
  62.8 1.4 copy.19.weights
  64.2 2.4 %table.1 = bf16[3,128,1024]{2,1,0:T(8,128)(2,1)} custom-call(s32[128,4]{1,0:T(8,128)} %get-tuple-element.26.slots, f32[128,4]{1,0:T(8,128)} %copy.19.weights), custom_call_target="tpu_custom_call" | custom-call | tf_op jit(solution)/shard_map/table/pallas_call | solution.py:137
  66.6 8.3 %all-to-all-done.1 = bf16[32,32,128]{2,1,0:T(8,128)(2,1)S(1)} async-done(((bf16[32,32,128]{2,1,0:T(8,128)(2,1)}), bf16[32,32,128]{2,1,0:T(8,128)(2,1)S(1)}, u32[]{:S(2)}, u32[]{:S(2)}) %all-to-all-start.1) | async-done | bytes 262176 | tf_op jit(solution)/shard_map/all_to_all | solution.py:417
  74.9 0.7 slice.16
  75.6 0.0 all-gather.8.cloned.1.call-update
  75.6 0.0 all-gather.10.cloned.1.call-start
  75.7 1.9 copy.20.sg
  77.6 0.0 copy-done.4
  77.6 1.0 copy.21.su
  78.6 0.8 pad_maximum_fusion
  79.4 22.3 %all-gather.1 = bf16[3584,128]{1,0:T(8,128)(2,1)} all-gather(bf16[224,128]{1,0:T(8,128)(2,1)S(1)} %pad_maximum_fusion), channel_id=3, replica_groups=mesh['sp'=32,'tp'=16] {'tp'}, dimensions={0}, use_global_device_ids=true | all-gather | bytes 974848 | tf_op jit(solution)/shard_map/all_gather | solution.py:431
  101.7 3.7 %side_hidden.1 = bf16[112,256]{1,0:T(8,128)(2,1)} custom-call(bf16[16,224,128]{2,1,0:T(8,128)(2,1)} %bitcast.31, f32[1,2048]{1,0:T(1,128)} %bitcast.38, bf16[2048,256]{1,0:T(8,128)(2,1)} %bitcast.19, bf16[2048,256]{1,0:T(8,128)(2,1)} %bitcast.21, bf16[2048,32]{1,0:T(8,128)(2,1)} %copy.20.sg, bf16[2048,32]{1,0:T(8,128)(2,1)} %copy.21.su), custom_call_target="tpu_custom_call" | custom-call | tf_op jit(solution)/shard_map/side_hidden/pallas_call | solution.py:285
  105.4 8.1 %all-gather.8.cloned.1.call-done = bf16[14848,128]{1,0:T(8,128)(2,1)} async-done(((bf16[928,128]{1,0:T(8,128)(2,1)}), bf16[14848,128]{1,0:T(8,128)(2,1)}) %all-gather.8.cloned.1.call-update) | async-done | bytes 3801104 | tf_op jit(solution)/shard_map/all_gather | solution.py:430
  113.5 0.0 copy-done.2
  113.5 0.0 copy-done.1
  113.5 5.3 %hidden.1 = (bf16[112,256]{1,0:T(8,128)(2,1)}, bf16[816,256]{1,0:T(8,128)(2,1)}) custom-call(bf16[16,928,128]{2,1,0:T(8,128)(2,1)} %bitcast.28, f32[1,2048]{1,0:T(1,128)} %bitcast.39, bf16[2048,256]{1,0:T(8,128)(2,1)S(1)} %bitcast.20, bf16[2048,256]{1,0:T(8,128)(2,1)S(1)} %bitcast.22), custom_call_target="tpu_custom_call" | custom-call | tf_op jit(solution)/shard_map/hidden/pallas_call | solution.py:251
  118.8 0.0 all-gather.10.cloned.1.call-update
  118.8 0.0 copy-start.3
  118.9 22.3 %all-gather.3 = bf16[1792,256]{1,0:T(8,128)(2,1)} all-gather(bf16[112,256]{1,0:T(8,128)(2,1)} %side_hidden.1), channel_id=5, replica_groups=mesh['sp'=32,'tp'=16] {'tp'}, dimensions={0}, use_global_device_ids=true | all-gather | bytes 974848 | tf_op jit(solution)/shard_map/all_gather | solution.py:439
  141.1 24.3 %all-gather.4 = bf16[1792,256]{1,0:T(8,128)(2,1)} all-gather(bf16[112,256]{1,0:T(8,128)(2,1)} %get-tuple-element.35), channel_id=6, replica_groups=mesh['sp'=32,'tp'=16] {'tp'}, dimensions={0}, use_global_device_ids=true | all-gather | bytes 974848 | tf_op jit(solution)/shard_map/all_gather | solution.py:439
  165.5 3.3 %side_down.1 = (bf16[208,128]{1,0:T(8,128)(2,1)}, f32[128,128]{1,0:T(8,128)}) custom-call(bf16[16,112,256]{2,1,0:T(8,128)(2,1)} %bitcast.29, bf16[16,112,256]{2,1,0:T(8,128)(2,1)} %bitcast.30, bf16[4096,128]{1,0:T(8,128)(2,1)} %bitcast.26, bf16[512,128]{1,0:T(8,128)(2,1)} %sh_down.1), custom_call_target="tpu_custom_call" | custom-call | tf_op jit(solution)/shard_map/side_down/pallas_call | solution.py:314
  168.8 4.2 %all-gather.10.cloned.1.call-done = bf16[13056,256]{1,0:T(8,128)(2,1)} async-done(((bf16[816,256]{1,0:T(8,128)(2,1)}), bf16[13056,256]{1,0:T(8,128)(2,1)}) %all-gather.10.cloned.1.call-update) | async-done | bytes 6684688 | tf_op jit(solution)/shard_map/all_gather | solution.py:436
  173.0 5.7 %down.1 = bf16[1024,128]{1,0:T(8,128)(2,1)} custom-call(bf16[16,816,256]{2,1,0:T(8,128)(2,1)} %bitcast.25, bf16[4096,128]{1,0:T(8,128)(2,1)} %bitcast.27, bf16[208,128]{1,0:T(8,128)(2,1)} %get-tuple-element.38.aside), custom_call_target="tpu_custom_call" | custom-call | tf_op jit(solution)/shard_map/down/pallas_call | solution.py:342
  178.7 21.6 %all_to_all.15 = bf16[32,32,128]{2,1,0:T(8,128)(2,1)S(1)} all-to-all(bf16[32,32,128]{2,1,0:T(8,128)(2,1)} %bitcast.32), channel_id=1, replica_groups=mesh['sp'=32,'tp'=16] {'sp'}, dimensions={0} | all-to-all | bytes 524288 | tf_op jit(solution)/shard_map/all_to_all | solution.py:443
  200.3 0.0 copy-done.3
  200.3 1.8 combine.1
  (1 shorter events, 0.0 us)
Async XLA Ops:
  6.5 20.2 %copy-start = (bf16[128,2048]{1,0:T(8,128)(2,1)S(1)}, bf16[128,2048]{1,0:T(8,128)(2,1)}, u32[]{:S(2)}) copy-start(bf16[128,2048]{1,0:T(8,128)(2,1)} %param.17) | copy-start | bytes 1572868
  6.5 71.1 %copy-start.4 = (bf16[2048,32]{0,1:T(8,128)(2,1)S(1)}, bf16[2048,32]{0,1:T(8,128)(2,1)}, u32[]{:S(2)}) copy-start(bf16[2048,32]{0,1:T(8,128)(2,1)} %param.32) | copy-start | bytes 393220
  6.5 107.0 %copy-start.2 = (bf16[1,2048,256]{2,1,0:T(8,128)(2,1)S(1)}, bf16[1,2048,256]{2,1,0:T(8,128)(2,1)}, u32[]{:S(2)}) copy-start(bf16[1,2048,256]{2,1,0:T(8,128)(2,1)} %param.29) | copy-start | bytes 3145732
  7.5 4.8 %collective-permute-start = (bf16[30,64]{0,1:T(8,128)(2,1)S(1)}, bf16[30,64]{0,1:T(8,128)(2,1)S(1)}, u32[]{:S(2)}, u32[]{:S(2)}) collective-permute-start(bf16[30,64]{0,1:T(8,128)(2,1)S(1)} %multiply_convert_fusion), channel_id=1, source_target_pairs={{0,16},{16,32},{32,48},{48,64},{64,80},{80,96},{96,112},{112,128},... | collective-permute-start | bytes 11528 | tf_op jit(solution)/shard_map/ppermute | solution.py:405
  14.4 30.0 %all-to-all-start = ((bf16[16,176,128]{2,1,0:T(8,128)(2,1)}), bf16[16,176,128]{2,1,0:T(8,128)(2,1)S(1)}, u32[]{:S(2)}, u32[]{:S(2)}) async-start(bf16[16,176,128]{2,1,0:T(8,128)(2,1)} %pack.1), calls=%async_computation | async-start | bytes 1441792 | tf_op jit(solution)/shard_map/all_to_all | solution.py:409
  48.1 65.4 %copy-start.1 = (bf16[1,2048,256]{2,1,0:T(8,128)(2,1)S(1)}, bf16[1,2048,256]{2,1,0:T(8,128)(2,1)}, u32[]{:S(2)}) copy-start(bf16[1,2048,256]{2,1,0:T(8,128)(2,1)} %param.28) | copy-start | bytes 3145732
  48.1 26.8 %all-to-all-start.1 = ((bf16[32,32,128]{2,1,0:T(8,128)(2,1)}), bf16[32,32,128]{2,1,0:T(8,128)(2,1)S(1)}, u32[]{:S(2)}, u32[]{:S(2)}) async-start(bf16[32,32,128]{2,1,0:T(8,128)(2,1)} %bitcast.35), calls=%async_computation.1 | async-start | bytes 524288 | tf_op jit(solution)/shard_map/all_to_all | solution.py:417
  62.8 50.8 %all-gather.8.cloned.1.call-start = ((), (), s32[]{:S(2)}) async-start(), calls=%async_computation.3 | async-start | bytes 4038656 | tf_op jit(solution)/shard_map/all_gather | solution.py:430
  75.6 97.4 %all-gather.10.cloned.1.call-start = ((), (), s32[]{:S(2)}) async-start(), calls=%async_computation.4 | async-start | bytes 7102464 | tf_op jit(solution)/shard_map/all_gather | solution.py:436
  118.8 81.4 %copy-start.3 = (bf16[3,128,1024]{2,1,0:T(8,128)(2,1)S(1)}, bf16[3,128,1024]{2,1,0:T(8,128)(2,1)}, u32[]{:S(2)}) copy-start(bf16[3,128,1024]{2,1,0:T(8,128)(2,1)} %table.1) | copy-start | bytes 2359300
Sparse Core Ops, SparseCore 0:
  75.7 37.7 all-gather.7
  119.0 53.9 all-gather.9

commit v10 on v9

--- a/solution.py
+++ b/solution.py
@@ -159,7 +159,7 @@
     def vector(first, cols=slice(None)):
         return sum(params[first + i : first + i + 1, cols] for i in range(3))
 
-    conv_rows = 64
+    conv_rows = tok_rows
 
     def one_block(i, _):
         cols = pl.ds(pl.multiple_of(i * LANES, LANES), LANES)

time: 210 us -> 210 us (level)
  no operation moved by 1% of the time
where the time goes in v10:
time: 210 us; the launch traced here: 209 us
  blocking collectives  90.5 us (43%)
  waiting for transfers between devices  38.6 us (18%)
  Pallas kernels  30.4 us (14%)
  starting transfers between devices  27.3 us (13%)
  between operations  13.5 us (6%)
  local copies, waits for them, and re-layouts  7.13 us (3%)
    all_gather x1, blocking collectives, body(): lax.all_gather(two, 'tp')  24.3 us
    all_gather x1, blocking collectives, body(): lax.all_gather(jnp.concatenate([landed[:first], middle], axis=0), 'tp')  22.3 us
    all_gather x1, blocking collectives, body(): lax.all_gather(one, 'tp')  22.3 us
    all_to_all x1, blocking collectives, body(): lax.all_to_all(expert_out.reshape(sp_count, slot_count // sp_count, col_w...  21.5 us
    all_to_all x1, waiting for transfers between devices, body(): lax.all_to_all(packed, 'tp', split_axis=0, concat_axis=0, tiled=True)  17 us
    all_to_all x1, starting transfers between devices, body(): lax.all_to_all(send.reshape(sp_count, slot_count // sp_count, col_width),...  14.6 us
    all_to_all x1, starting transfers between devices, body(): lax.all_to_all(packed, 'tp', split_axis=0, concat_axis=0, tiled=True)  8.64 us
    all_to_all x1, waiting for transfers between devices, body(): lax.all_to_all(send.reshape(sp_count, slot_count // sp_count, col_width),...  8.32 us
  transfers between devices with their start and end apart: 5, of which 5 were waited for; matrix products, arithmetic and copies ran while one was open for 3% of the time, Pallas kernels for 6%

profile of v10, /device:TPU:1, one launch (start us, length us, event | category | flops | bytes accessed | tf_op | source)
XLA Modules:
  0.0 209.0 jit_solution(12487204117854315237)
XLA Ops:
  6.5 0.0 copy-start
  6.5 0.0 copy-start.4
  6.5 0.0 copy-start.2
  6.5 0.9 multiply_convert_fusion
  7.5 3.9 %collective-permute-start = (bf16[30,64]{0,1:T(8,128)(2,1)S(1)}, bf16[30,64]{0,1:T(8,128)(2,1)S(1)}, u32[]{:S(2)}, u32[]{:S(2)}) collective-permute-start(bf16[30,64]{0,1:T(8,128)(2,1)S(1)} %multiply_convert_fusion), channel_id=1, source_target_pairs={{0,16},{16,32},{32,48},{48,64},{64,80},{80,96},{96,112},{112,128},... | collective-permute-start | bytes 11528 | tf_op jit(solution)/shard_map/ppermute | solution.py:405
  11.4 0.9 collective-permute-done
  12.3 2.2 %pack.1 = bf16[16,176,128]{2,1,0:T(8,128)(2,1)} custom-call(bf16[64,30]{1,0:T(8,128)(2,1)S(1)} %bitcast.24, bf16[64,128]{1,0:T(8,128)(2,1)} %bitcast.37, bf16[64,128]{1,0:T(8,128)(2,1)} %bitcast.36, bf16[31,64]{1,0:T(8,128)(2,1)} %taps.1, f32[1,64]{1,0:T(1,128)} %bitcast.40, f32[1,64]{1,0:T(1,128)} %bitcast.41, f32[1,64]{1,0:T(1,128)} %bitcast.42, ...), custom_call_target="tpu_custom_call" | custom-call | tf_op jit(solution)/shard_map/pack/pallas_call | solution.py:72
  14.4 8.6 %all-to-all-start = ((bf16[16,176,128]{2,1,0:T(8,128)(2,1)}), bf16[16,176,128]{2,1,0:T(8,128)(2,1)S(1)}, u32[]{:S(2)}, u32[]{:S(2)}) async-start(bf16[16,176,128]{2,1,0:T(8,128)(2,1)} %pack.1), calls=%async_computation | async-start | bytes 1441792 | tf_op jit(solution)/shard_map/all_to_all | solution.py:409
  23.1 1.4 copy.18.refs_0_
  24.5 2.3 %routing.1 = (s32[128,4]{1,0:T(8,128)}, bf16[1024,128]{1,0:T(8,128)(2,1)}) custom-call(s32[128,4]{1,0:T(8,128)} %copy.18.refs_0_), custom_call_target="tpu_custom_call" | custom-call | tf_op jit(solution)/shard_map/routing/pallas_call | solution.py:114
  26.8 0.0 copy-done
  26.8 0.6 constant_dynamic-slice_fusion.refs_1_
  27.4 17.0 %all-to-all-done.refs_0_ = bf16[16,176,128]{2,1,0:T(8,128)(2,1)S(1)} async-done(((bf16[16,176,128]{2,1,0:T(8,128)(2,1)}), bf16[16,176,128]{2,1,0:T(8,128)(2,1)S(1)}, u32[]{:S(2)}, u32[]{:S(2)}) %all-to-all-start) | async-done | bytes 720928 | tf_op jit(solution)/shard_map/all_to_all | solution.py:409
  44.4 3.7 %front.1 = (bf16[128,128]{1,0:T(8,128)(2,1)}, bf16[1024,128]{1,0:T(8,128)(2,1)}) custom-call(bf16[16,176,128]{2,1,0:T(8,128)(2,1)S(1)} %all-to-all-done.refs_0_, bf16[128,128]{1,0:T(8,128)(2,1)} %constant_dynamic-slice_fusion.refs_1_, bf16[1024,128]{1,0:T(8,128)(2,1)} %get-tuple-element.23.refs_2_), custom_call_target="tpu_custom_call" | custom-call | tf_op jit(solution)/shard_map/front/pallas_call | solution.py:198
  48.1 0.0 copy-start.1
  48.1 14.6 %all-to-all-start.1 = ((bf16[32,32,128]{2,1,0:T(8,128)(2,1)}), bf16[32,32,128]{2,1,0:T(8,128)(2,1)S(1)}, u32[]{:S(2)}, u32[]{:S(2)}) async-start(bf16[32,32,128]{2,1,0:T(8,128)(2,1)} %bitcast.35), calls=%async_computation.1 | async-start | bytes 524288 | tf_op jit(solution)/shard_map/all_to_all | solution.py:417
  62.8 0.0 all-gather.8.cloned.1.call-start
  62.8 1.4 copy.19.weights
  64.2 2.4 %table.1 = bf16[3,128,1024]{2,1,0:T(8,128)(2,1)} custom-call(s32[128,4]{1,0:T(8,128)} %get-tuple-element.26.slots, f32[128,4]{1,0:T(8,128)} %copy.19.weights), custom_call_target="tpu_custom_call" | custom-call | tf_op jit(solution)/shard_map/table/pallas_call | solution.py:137
  66.6 8.3 %all-to-all-done.1 = bf16[32,32,128]{2,1,0:T(8,128)(2,1)S(1)} async-done(((bf16[32,32,128]{2,1,0:T(8,128)(2,1)}), bf16[32,32,128]{2,1,0:T(8,128)(2,1)S(1)}, u32[]{:S(2)}, u32[]{:S(2)}) %all-to-all-start.1) | async-done | bytes 262176 | tf_op jit(solution)/shard_map/all_to_all | solution.py:417
  74.9 0.7 slice.16
  75.6 0.0 all-gather.8.cloned.1.call-update
  75.6 0.0 all-gather.10.cloned.1.call-start
  75.7 1.9 copy.20.sg
  77.6 0.0 copy-done.4
  77.6 1.0 copy.21.su
  78.7 0.8 pad_maximum_fusion
  79.4 22.3 %all-gather.1 = bf16[3584,128]{1,0:T(8,128)(2,1)} all-gather(bf16[224,128]{1,0:T(8,128)(2,1)S(1)} %pad_maximum_fusion), channel_id=3, replica_groups=mesh['sp'=32,'tp'=16] {'tp'}, dimensions={0}, use_global_device_ids=true | all-gather | bytes 974848 | tf_op jit(solution)/shard_map/all_gather | solution.py:431
  101.7 3.7 %side_hidden.1 = bf16[112,256]{1,0:T(8,128)(2,1)} custom-call(bf16[16,224,128]{2,1,0:T(8,128)(2,1)} %bitcast.31, f32[1,2048]{1,0:T(1,128)} %bitcast.38, bf16[2048,256]{1,0:T(8,128)(2,1)} %bitcast.19, bf16[2048,256]{1,0:T(8,128)(2,1)} %bitcast.21, bf16[2048,32]{1,0:T(8,128)(2,1)} %copy.20.sg, bf16[2048,32]{1,0:T(8,128)(2,1)} %copy.21.su), custom_call_target="tpu_custom_call" | custom-call | tf_op jit(solution)/shard_map/side_hidden/pallas_call | solution.py:285
  105.5 8.1 %all-gather.8.cloned.1.call-done = bf16[14848,128]{1,0:T(8,128)(2,1)} async-done(((bf16[928,128]{1,0:T(8,128)(2,1)}), bf16[14848,128]{1,0:T(8,128)(2,1)}) %all-gather.8.cloned.1.call-update) | async-done | bytes 3801104 | tf_op jit(solution)/shard_map/all_gather | solution.py:430
  113.6 0.0 copy-done.2
  113.6 0.0 copy-done.1
  113.6 5.3 %hidden.1 = (bf16[112,256]{1,0:T(8,128)(2,1)}, bf16[816,256]{1,0:T(8,128)(2,1)}) custom-call(bf16[16,928,128]{2,1,0:T(8,128)(2,1)} %bitcast.28, f32[1,2048]{1,0:T(1,128)} %bitcast.39, bf16[2048,256]{1,0:T(8,128)(2,1)S(1)} %bitcast.20, bf16[2048,256]{1,0:T(8,128)(2,1)S(1)} %bitcast.22), custom_call_target="tpu_custom_call" | custom-call | tf_op jit(solution)/shard_map/hidden/pallas_call | solution.py:251
  118.8 0.0 all-gather.10.cloned.1.call-update
  118.9 0.0 copy-start.3
  118.9 22.3 %all-gather.3 = bf16[1792,256]{1,0:T(8,128)(2,1)} all-gather(bf16[112,256]{1,0:T(8,128)(2,1)} %side_hidden.1), channel_id=5, replica_groups=mesh['sp'=32,'tp'=16] {'tp'}, dimensions={0}, use_global_device_ids=true | all-gather | bytes 974848 | tf_op jit(solution)/shard_map/all_gather | solution.py:439
  141.2 24.3 %all-gather.4 = bf16[1792,256]{1,0:T(8,128)(2,1)} all-gather(bf16[112,256]{1,0:T(8,128)(2,1)} %get-tuple-element.35), channel_id=6, replica_groups=mesh['sp'=32,'tp'=16] {'tp'}, dimensions={0}, use_global_device_ids=true | all-gather | bytes 974848 | tf_op jit(solution)/shard_map/all_gather | solution.py:439
  165.5 3.3 %side_down.1 = (bf16[208,128]{1,0:T(8,128)(2,1)}, f32[128,128]{1,0:T(8,128)}) custom-call(bf16[16,112,256]{2,1,0:T(8,128)(2,1)} %bitcast.29, bf16[16,112,256]{2,1,0:T(8,128)(2,1)} %bitcast.30, bf16[4096,128]{1,0:T(8,128)(2,1)} %bitcast.26, bf16[512,128]{1,0:T(8,128)(2,1)} %sh_down.1), custom_call_target="tpu_custom_call" | custom-call | tf_op jit(solution)/shard_map/side_down/pallas_call | solution.py:314
  168.8 4.2 %all-gather.10.cloned.1.call-done = bf16[13056,256]{1,0:T(8,128)(2,1)} async-done(((bf16[816,256]{1,0:T(8,128)(2,1)}), bf16[13056,256]{1,0:T(8,128)(2,1)}) %all-gather.10.cloned.1.call-update) | async-done | bytes 6684688 | tf_op jit(solution)/shard_map/all_gather | solution.py:436
  173.0 5.7 %down.1 = bf16[1024,128]{1,0:T(8,128)(2,1)} custom-call(bf16[16,816,256]{2,1,0:T(8,128)(2,1)} %bitcast.25, bf16[4096,128]{1,0:T(8,128)(2,1)} %bitcast.27, bf16[208,128]{1,0:T(8,128)(2,1)} %get-tuple-element.38.aside), custom_call_target="tpu_custom_call" | custom-call | tf_op jit(solution)/shard_map/down/pallas_call | solution.py:342
  178.8 21.5 %all_to_all.15 = bf16[32,32,128]{2,1,0:T(8,128)(2,1)S(1)} all-to-all(bf16[32,32,128]{2,1,0:T(8,128)(2,1)} %bitcast.32), channel_id=1, replica_groups=mesh['sp'=32,'tp'=16] {'sp'}, dimensions={0} | all-to-all | bytes 524288 | tf_op jit(solution)/shard_map/all_to_all | solution.py:443
  200.3 0.0 copy-done.3
  200.3 1.8 combine.1
  (1 shorter events, 0.0 us)
Async XLA Ops:
  6.5 20.2 %copy-start = (bf16[128,2048]{1,0:T(8,128)(2,1)S(1)}, bf16[128,2048]{1,0:T(8,128)(2,1)}, u32[]{:S(2)}) copy-start(bf16[128,2048]{1,0:T(8,128)(2,1)} %param.17) | copy-start | bytes 1572868
  6.5 71.1 %copy-start.4 = (bf16[2048,32]{0,1:T(8,128)(2,1)S(1)}, bf16[2048,32]{0,1:T(8,128)(2,1)}, u32[]{:S(2)}) copy-start(bf16[2048,32]{0,1:T(8,128)(2,1)} %param.32) | copy-start | bytes 393220
  6.5 107.0 %copy-start.2 = (bf16[1,2048,256]{2,1,0:T(8,128)(2,1)S(1)}, bf16[1,2048,256]{2,1,0:T(8,128)(2,1)}, u32[]{:S(2)}) copy-start(bf16[1,2048,256]{2,1,0:T(8,128)(2,1)} %param.29) | copy-start | bytes 3145732
  7.5 4.8 %collective-permute-start = (bf16[30,64]{0,1:T(8,128)(2,1)S(1)}, bf16[30,64]{0,1:T(8,128)(2,1)S(1)}, u32[]{:S(2)}, u32[]{:S(2)}) collective-permute-start(bf16[30,64]{0,1:T(8,128)(2,1)S(1)} %multiply_convert_fusion), channel_id=1, source_target_pairs={{0,16},{16,32},{32,48},{48,64},{64,80},{80,96},{96,112},{112,128},... | collective-permute-start | bytes 11528 | tf_op jit(solution)/shard_map/ppermute | solution.py:405
  14.4 30.0 %all-to-all-start = ((bf16[16,176,128]{2,1,0:T(8,128)(2,1)}), bf16[16,176,128]{2,1,0:T(8,128)(2,1)S(1)}, u32[]{:S(2)}, u32[]{:S(2)}) async-start(bf16[16,176,128]{2,1,0:T(8,128)(2,1)} %pack.1), calls=%async_computation | async-start | bytes 1441792 | tf_op jit(solution)/shard_map/all_to_all | solution.py:409
  48.1 65.5 %copy-start.1 = (bf16[1,2048,256]{2,1,0:T(8,128)(2,1)S(1)}, bf16[1,2048,256]{2,1,0:T(8,128)(2,1)}, u32[]{:S(2)}) copy-start(bf16[1,2048,256]{2,1,0:T(8,128)(2,1)} %param.28) | copy-start | bytes 3145732
  48.1 26.8 %all-to-all-start.1 = ((bf16[32,32,128]{2,1,0:T(8,128)(2,1)}), bf16[32,32,128]{2,1,0:T(8,128)(2,1)S(1)}, u32[]{:S(2)}, u32[]{:S(2)}) async-start(bf16[32,32,128]{2,1,0:T(8,128)(2,1)} %bitcast.35), calls=%async_computation.1 | async-start | bytes 524288 | tf_op jit(solution)/shard_map/all_to_all | solution.py:417
  62.8 50.8 %all-gather.8.cloned.1.call-start = ((), (), s32[]{:S(2)}) async-start(), calls=%async_computation.3 | async-start | bytes 4038656 | tf_op jit(solution)/shard_map/all_gather | solution.py:430
  75.6 97.4 %all-gather.10.cloned.1.call-start = ((), (), s32[]{:S(2)}) async-start(), calls=%async_computation.4 | async-start | bytes 7102464 | tf_op jit(solution)/shard_map/all_gather | solution.py:436
  118.9 81.4 %copy-start.3 = (bf16[3,128,1024]{2,1,0:T(8,128)(2,1)S(1)}, bf16[3,128,1024]{2,1,0:T(8,128)(2,1)}, u32[]{:S(2)}) copy-start(bf16[3,128,1024]{2,1,0:T(8,128)(2,1)} %table.1) | copy-start | bytes 2359300
Sparse Core Ops, SparseCore 0:
  75.8 37.7 all-gather.7
  119.0 53.9 all-gather.9
